TPU v7x, 256 devices: a whole 4x4x8 slice. The times are simulated.
256 devices in a mesh: dp: 4 (over x), kv: 32 (over z, y), tp: 2 (over core).
Axes of the slice: x: 4, y: 4, z: 8, core: 2. Of those that a mesh axis runs over, the one named last changes fastest.
Arguments:
- tokens: bfloat16 [128, 4096], P('dp', ('kv', 'tp')), may hold values from -24 to 24
- rec_state: float32 [128, 16, 128, 128], P(('dp', 'kv'), 'tp'), may hold values from -2 to 2
- norm_gain: float32 [4096], replicated, may hold values from 0.1 to 1.9
- w_query: bfloat16 [4096, 2048], P('kv', 'tp'), may hold values from -0.09375 to 0.09375
- w_forget: bfloat16 [4096, 2048], P('kv', 'tp'), may hold values from -0.09375 to 0.09375
- w_input: bfloat16 [4096, 2048], P('kv', 'tp'), may hold values from -0.09375 to 0.09375
- w_outgate: bfloat16 [4096, 2048], P('kv', 'tp'), may hold values from -0.09375 to 0.09375
- lower_bound: float32 [2048], P('tp'), may hold values from 0 to 0.9
- head_gain: float32 [2048], P('tp'), may hold values from 0.1 to 1.9
- w_heads_out: bfloat16 [2048, 4096], P(None, ('kv', 'tp')), may hold values from -0.125 to 0.125
- mixer_gain: float32 [4096], replicated, may hold values from 0.1 to 1.9
- w_gate: bfloat16 [4096, 11264], P(None, ('kv', 'tp')), may hold values from -0.09375 to 0.09375
- w_up: bfloat16 [4096, 11264], P(None, ('kv', 'tp')), may hold values from -0.09375 to 0.09375
- w_down: bfloat16 [11264, 4096], P(('kv', 'tp')), may hold values from -0.15625 to 0.15625
Outputs:
- result: bfloat16 [128, 4096], P('dp', ('kv', 'tp'))
- new_state: float32 [128, 16, 128, 128], P(('dp', 'kv'), 'tp')
All inputs are finite; a program needn't handle non-finite values.
Results may differ from a plain program's by a relative error of at most 0.012.
Values may be sent and summed in bfloat16 or wider, within the bound.
No kernel may reach another device: no remote copies, remote signals or barrier semaphores. Data moves between devices by JAX's collectives and lax.ppermute only.
A program may use at most 64 MiB of HBM per device.

v0:
```python
import jax
import jax.numpy as jnp
from jax import lax
from jax.sharding import Mesh
from jax.sharding import PartitionSpec as P

HEAD_DIM = 128
KV = ("kv_0", "kv_1")
KV_TP = ("kv_0", "kv_1", "tp")
DP_KV = ("dp", "kv_0", "kv_1")


epsilon = 1e-06


def laid_out(pieces, dim):
    pieces = jnp.moveaxis(pieces, 0, dim)
    dims = pieces.shape
    return pieces.reshape(*dims[:dim], dims[dim] * dims[dim + 1], *dims[dim + 2 :])


def from_everyone(value, axis):
    copies = jnp.broadcast_to(value, (lax.axis_size(axis), *value.shape))
    return lax.all_to_all(copies, axis, split_axis=0, concat_axis=0, tiled=True)


def collect(value, axis, dim):
    return laid_out(from_everyone(value, axis), dim)


def over_copies(value, axis):
    everything = from_everyone(value, axis)
    return jnp.sum(everything, axis=0)


def sum_by_axis(total, axes):
    for axis in axes:
        total = lax.psum_scatter(total, axis, scatter_dimension=0, tiled=True)
    return total


def split_up(value, dim, size):
    before, after = (value.shape[:dim], value.shape[dim + 1 :])
    return jnp.moveaxis(value.reshape(*before, size, -1, *after), dim, 0)


def sent_and_summed(value, axis, dim):
    size = lax.axis_size(axis)
    pieces = lax.all_to_all(split_up(value, dim, size), axis, 0, 0, tiled=True)
    return jnp.sum(pieces.astype(jnp.float32), axis=0)


def channel_mixer(whole_rows, mixer_gain, w_gate, w_up, w_down):
    rows_float = whole_rows.astype(jnp.float32)
    mixer_scale = lax.rsqrt(jnp.mean(rows_float * rows_float, axis=1, keepdims=True) + epsilon)
    normed = (rows_float * mixer_scale * mixer_gain).astype(jnp.bfloat16)
    gate_val = jnp.dot(normed, w_gate, preferred_element_type=jnp.float32)
    up_val = jnp.dot(normed, w_up, preferred_element_type=jnp.float32)
    hidden = (jax.nn.silu(gate_val) * up_val).astype(jnp.bfloat16)
    return jnp.dot(hidden, w_down, preferred_element_type=jnp.float32)


def local(
    tokens,
    rec_state,
    norm_gain,
    w_query,
    w_forget,
    w_input,
    w_outgate,
    lower_bound,
    head_gain,
    w_heads_out,
    mixer_gain,
    w_gate,
    w_up,
    w_down,
):
    kv_count = lax.axis_size(KV)
    tp_count = lax.axis_size("tp")
    kv_index = lax.axis_index(KV)
    row_count = tokens.shape[0]
    seq_count = rec_state.shape[0]
    model_width = norm_gain.shape[0]
    col_block = model_width // kv_count
    tok_float = tokens.astype(jnp.float32)
    own_cols = collect(tokens, "tp", 1).astype(jnp.float32)
    squares = over_copies(jnp.sum(tok_float * tok_float, axis=1), KV_TP)
    gain_block = lax.dynamic_slice_in_dim(norm_gain, kv_index * col_block, col_block, 0)
    scaled = (own_cols * gain_block).astype(jnp.bfloat16)
    projected = sum_by_axis(
        jnp.stack(
            [
                jnp.dot(scaled, weight, preferred_element_type=jnp.float32)
                for weight in (w_query, w_forget, w_input, w_outgate)
            ],
            axis=1,
        ),
        KV,
    )
    my_squares = lax.dynamic_slice_in_dim(squares, kv_index * seq_count, seq_count, 0)
    row_scale = lax.rsqrt(my_squares / model_width + epsilon)[:, None]
    query_pre = row_scale * projected[:, 0]
    forget_pre = row_scale * projected[:, 1]
    value_in = row_scale * projected[:, 2]
    gate_pre = row_scale * projected[:, 3]
    forget = lower_bound + (1.0 - lower_bound) * jax.nn.sigmoid(forget_pre)
    key_in = 1.0 - forget
    query_act = jax.nn.silu(query_pre)
    head_count = rec_state.shape[1]
    shaped = (seq_count, head_count, HEAD_DIM)
    forget = forget.reshape(shaped)
    key_in = key_in.reshape(shaped)
    value_in = value_in.reshape(shaped)
    query_act = query_act.reshape(shaped)
    new_state = forget[:, :, :, None] * rec_state + key_in[:, :, :, None] * value_in[:, :, None, :]
    head_out = jnp.sum(query_act[:, :, :, None] * new_state, axis=2)
    head_out = head_out * lax.rsqrt(jnp.mean(head_out * head_out, axis=2, keepdims=True) + epsilon)
    head_out = head_out * head_gain.reshape(head_count, HEAD_DIM)
    local_width = head_count * HEAD_DIM
    gated = (head_out.reshape(seq_count, local_width) * jax.nn.silu(gate_pre)).astype(jnp.bfloat16)
    every_head = collect(gated[None], KV_TP, 0)
    every_head = every_head.reshape(kv_count, tp_count, seq_count, local_width)
    every_head = every_head.transpose(0, 2, 1, 3).reshape(
        kv_count * seq_count, tp_count * local_width
    )
    mixed_add = jnp.dot(every_head, w_heads_out, preferred_element_type=jnp.float32)
    mixed = (tok_float + mixed_add).astype(jnp.bfloat16)
    gathered = collect(mixed, KV_TP, 1)
    terms = channel_mixer(gathered, mixer_gain, w_gate, w_up, w_down)
    out_block = model_width // (kv_count * tp_count)
    blocked = terms.reshape(row_count, kv_count, tp_count, out_block)
    chip_sum = sent_and_summed(blocked.astype(jnp.bfloat16), "tp", 2)
    down_sum = sent_and_summed(chip_sum.astype(jnp.bfloat16), KV, 1).reshape(row_count, out_block)
    result = (mixed.astype(jnp.float32) + down_sum).astype(jnp.bfloat16)
    return (result, new_state)


def solution(mesh):
    torus = Mesh(
        mesh.devices.reshape(mesh.shape["dp"], 8, 4, mesh.shape["tp"]), ("dp", "kv_0", "kv_1", "tp")
    )
    in_specs = (
        P("dp", KV_TP),
        P(DP_KV, "tp", None, None),
        P(),
        P(KV, "tp"),
        P(KV, "tp"),
        P(KV, "tp"),
        P(KV, "tp"),
        P("tp"),
        P("tp"),
        P(None, KV_TP),
        P(),
        P(None, KV_TP),
        P(None, KV_TP),
        P(KV_TP, None),
    )
    out_specs = (P("dp", KV_TP), P(DP_KV, "tp", None, None))
    return jax.shard_map(local, mesh=torus, in_specs=in_specs, out_specs=out_specs, check_vma=False)
```

profile of v0, /device:TPU:6, one launch (start us, length us, event | category | flops | bytes accessed | tf_op | source)
XLA Modules:
  0.0 222.2 jit_solution(14498625972558857634)
XLA Ops:
  7.2 0.8 broadcast_in_dim.9
  8.7 3.2 %all-to-all-start.1 = ((bf16[2,2,1024]{2,1,0:T(2,128)(2,1)}), bf16[2,2,1024]{2,1,0:T(2,128)(2,1)S(1)}, u32[]{:S(2)}, u32[]{:S(2)}) async-start(bf16[2,2,1024]{2,1,0:T(2,128)(2,1)} %reshape.163), calls=%async_computation.1 | async-start | bytes 16384 | tf_op jit(solution)/shard_map/all_to_all | solution.py:24
  12.0 1.3 all-to-all-done.1
  13.5 0.8 dynamic_slice.7
  14.3 1.1 convolution_bitcast_fusion
  15.4 1.1 convolution_bitcast_fusion.1
  16.6 1.2 convolution_bitcast_fusion.2
  17.9 0.8 pad_maximum_fusion
  20.1 75.5 %all-reduce.5.cloned.1.call-done = f32[32,4,1024]{2,0,1:T(8,128)} async-done(((f32[32,4,1024]{2,0,1:T(8,128)}), f32[32,4,1024]{2,0,1:T(8,128)}) %all-reduce.5.cloned.1.call-update) | async-done | bytes 524304
  95.6 0.9 constant_dynamic-slice_fusion
  98.0 7.5 %all-to-all-start = ((f32[64,1,32]{2,1,0:T(1,128)}), f32[64,1,32]{2,1,0:T(1,128)S(1)}, u32[]{:S(2)}, u32[]{:S(2)}) async-start(f32[64,1,32]{2,1,0:T(1,128)} %broadcast_in_dim.8), calls=%async_computation | async-start | bytes 65536 | tf_op jit(solution)/shard_map/all_to_all | solution.py:24
  106.1 9.0 %all-to-all-done = f32[64,1,32]{2,1,0:T(1,128)S(1)} async-done(((f32[64,1,32]{2,1,0:T(1,128)}), f32[64,1,32]{2,1,0:T(1,128)S(1)}, u32[]{:S(2)}, u32[]{:S(2)}) %all-to-all-start) | async-done | bytes 8224 | tf_op jit(solution)/shard_map/all_to_all | solution.py:24
  116.4 26.7 %all-reduce.7.cloned.1.call-done = f32[4,4,1024]{2,1,0:T(4,128)} async-done(((f32[4,4,1024]{2,1,0:T(4,128)}), f32[4,4,1024]{2,1,0:T(4,128)}) %all-reduce.7.cloned.1.call-update) | async-done | bytes 65552
  143.2 1.5 dynamic-slice_multiply_fusion
  144.8 1.3 multiply_reduce_fusion
  146.9 1.4 reduce.10
  148.4 20.4 %all_to_all.31 = bf16[64,2,512]{2,1,0:T(2,128)(2,1)S(1)} all-to-all(bf16[64,2,512]{2,1,0:T(2,128)(2,1)S(1)} %reshape.165), channel_id=1, replica_groups=mesh['dp'=4,'kv_0'=8,'kv_1'=4,'tp'=2] {'kv_0','kv_1','tp'}, dimensions={0} | all-to-all | bytes 262144 | tf_op jit(solution)/shard_map/all_to_all | solution.py:24
  168.9 0.8 reduce.9
  170.3 16.8 %all_to_all.32 = bf16[64,2,1024]{2,1,0:T(2,128)(2,1)S(1)} all-to-all(bf16[64,2,1024]{2,1,0:T(2,128)(2,1)S(1)} %reshape.167), channel_id=1, replica_groups=mesh['dp'=4,'kv_0'=8,'kv_1'=4,'tp'=2] {'kv_0','kv_1','tp'}, dimensions={0} | all-to-all | bytes 524288 | tf_op jit(solution)/shard_map/all_to_all | solution.py:24
  188.8 2.0 fusion.16
  190.9 1.9 convolution_convert_fusion
  192.8 1.5 convert_element_type.80
  194.8 3.9 %all_to_all.33 = bf16[2,2,32768]{2,1,0:T(2,128)(2,1)S(1)} all-to-all(bf16[2,2,32768]{2,1,0:T(2,128)(2,1)S(1)} %reshape.169), channel_id=1, replica_groups=mesh['dp'=4,'kv_0'=8,'kv_1'=4,'tp'=2] {'tp'}, dimensions={0} | all-to-all | bytes 524288 | tf_op jit(solution)/shard_map/all_to_all | solution.py:49
  199.5 14.9 %all_to_all.34 = bf16[32,2,1024]{2,1,0:T(2,128)(2,1)S(1)} all-to-all(bf16[32,2,1024]{2,1,0:T(2,128)(2,1)S(1)} %reshape.171), channel_id=1, replica_groups=mesh['dp'=4,'kv_0'=8,'kv_1'=4,'tp'=2] {'kv_0','kv_1'}, dimensions={0} | all-to-all | bytes 262144 | tf_op jit(solution)/shard_map/all_to_all | solution.py:49
  (69 shorter events, 10.1 us)
Async XLA Ops:
  7.2 183.7 %copy-start = (bf16[176,4096]{1,0:T(8,128)(2,1)S(1)}, bf16[176,4096]{1,0:T(8,128)(2,1)}, u32[]{:S(2)}) copy-start(bf16[176,4096]{1,0:T(8,128)(2,1)} %param.27) | copy-start | bytes 4325380
  7.2 10.6 %copy-start.3 = (bf16[128,1024]{1,0:T(8,128)(2,1)S(1)}, bf16[128,1024]{1,0:T(8,128)(2,1)}, u32[]{:S(2)}) copy-start(bf16[128,1024]{1,0:T(8,128)(2,1)} %param.17) | copy-start | bytes 786436
  8.7 4.6 %all-to-all-start.1 = ((bf16[2,2,1024]{2,1,0:T(2,128)(2,1)}), bf16[2,2,1024]{2,1,0:T(2,128)(2,1)S(1)}, u32[]{:S(2)}, u32[]{:S(2)}) async-start(bf16[2,2,1024]{2,1,0:T(2,128)(2,1)} %reshape.163), calls=%async_computation.1 | async-start | bytes 16384 | tf_op jit(solution)/shard_map/all_to_all | solution.py:24
  11.9 83.7 %all-reduce.5.cloned.1.call-start = ((), (), s32[]{:S(2)}) async-start(), calls=%async_computation.6 | async-start | bytes 1048576
  15.4 3.4 %copy-start.10 = (u32[256]{0:T(256)S(1)}, u32[256]{0:T(256)}, u32[]{:S(2)}) copy-start(u32[256]{0:T(256)} %constant.52) | copy-start | bytes 3076
  16.5 80.7 %copy-start.5 = (bf16[32,64]{1,0:T(8,128)(2,1)S(1)}, bf16[32,64]{1,0:T(8,128)(2,1)}, u32[]{:S(2)}) copy-start(bf16[32,64]{1,0:T(8,128)(2,1)} %param.14) | copy-start | bytes 12292
  16.5 88.9 %copy-start.9 = (u32[256]{0:T(256)S(1)}, u32[256]{0:T(256)}, u32[]{:S(2)}) copy-start(u32[256]{0:T(256)} %constant.56) | copy-start | bytes 3076
  16.5 128.2 %copy-start.7 = (f32[1024]{0:T(1024)S(1)}, f32[1024]{0:T(1024)}, u32[]{:S(2)}) copy-start(f32[1024]{0:T(1024)} %param.21) | copy-start | bytes 12292
  16.6 128.2 %copy-start.2 = (f32[1,8,128,128]{3,2,1,0:T(8,128)S(1)}, f32[1,8,128,128]{3,2,1,0:T(8,128)}, u32[]{:S(2)}) copy-start(f32[1,8,128,128]{3,2,1,0:T(8,128)} %param.15) | copy-start | bytes 1572868
  17.9 128.3 %copy-start.8 = (f32[1024]{0:T(1024)S(1)}, f32[1024]{0:T(1024)}, u32[]{:S(2)}) copy-start(f32[1024]{0:T(1024)} %param.22) | copy-start | bytes 12292
  18.8 124.4 %all-reduce.7.cloned.1.call-start = ((), (), s32[]{:S(2)}) async-start(), calls=%async_computation.7 | async-start | bytes 131072
  98.0 17.1 %all-to-all-start = ((f32[64,1,32]{2,1,0:T(1,128)}), f32[64,1,32]{2,1,0:T(1,128)S(1)}, u32[]{:S(2)}, u32[]{:S(2)}) async-start(f32[64,1,32]{2,1,0:T(1,128)} %broadcast_in_dim.8), calls=%async_computation | async-start | bytes 65536 | tf_op jit(solution)/shard_map/all_to_all | solution.py:24
  144.7 25.0 %copy-start.4 = (bf16[2048,64]{0,1:T(8,128)(2,1)S(1)}, bf16[2048,64]{0,1:T(8,128)(2,1)}, u32[]{:S(2)}) copy-start(bf16[2048,64]{0,1:T(8,128)(2,1)} %param.23) | copy-start | bytes 786436
  187.8 1.0 copy-start.6
  188.8 2.1 copy-start.1
Sparse Core Ops, SparseCore 0:
  18.9 76.6 all-reduce.4
  98.5 44.6 all-reduce.6
where the time goes:
time: 223 us; the launch traced here: 222 us
  waiting for transfers between devices  113 us (51%)
  blocking collectives  56.1 us (25%)
  between operations  15.7 us (7%)
  local copies, waits for them, and re-layouts  12 us (5%)
  starting transfers between devices  10.8 us (5%)
  matrix products  7.69 us (3%)
  other arithmetic  7.33 us (3%)
    unnamed x4, waiting for transfers between devices  102 us
    all_to_all x2, blocking collectives, from_everyone(): return lax.all_to_all(copies, axis, split_axis=0, concat_axis=0, tiled=True)  37.2 us
    all_to_all x2, blocking collectives, sent_and_summed(): pieces = lax.all_to_all(split_up(value, dim, size), axis, 0, 0, tiled=True)  18.9 us
    all_to_all x2, starting transfers between devices, from_everyone(): return lax.all_to_all(copies, axis, split_axis=0, concat_axis=0, tiled=True)  10.7 us
    all_to_all x2, waiting for transfers between devices, from_everyone(): return lax.all_to_all(copies, axis, split_axis=0, concat_axis=0, tiled=True)  10.3 us
    unnamed x35, local copies, waits for them, and re-layouts  4.91 us
  transfers between devices with their start and end apart: 4, of which 4 were waited for; matrix products, arithmetic and copies ran while one was open for 1% of the time, Pallas kernels for 0%

commit v1 on v0

v1 whole, which is shorter than its diff:
```python
import jax
import jax.numpy as jnp
from jax import lax
from jax.sharding import Mesh
from jax.sharding import PartitionSpec as P

HEAD_DIM = 128
KV = ("kv_0", "kv_1")
KV_TP = ("kv_0", "kv_1", "tp")
DP_KV = ("dp", "kv_0", "kv_1")
SWAP = [(0, 1), (1, 0)]

epsilon = 1e-06


def exchanged(pieces, axis):
    return lax.all_to_all(pieces, axis, split_axis=0, concat_axis=0, tiled=True)


def to_everyone(value, axis):
    return exchanged(jnp.broadcast_to(value, (lax.axis_size(axis), *value.shape)), axis)


def by_core(own, other, core):
    first = jnp.where(core == 0, own, other)
    second = jnp.where(core == 0, other, own)
    return first, second


def local(
    tokens,
    rec_state,
    norm_gain,
    w_query,
    w_forget,
    w_input,
    w_outgate,
    lower_bound,
    head_gain,
    w_heads_out,
    mixer_gain,
    w_gate,
    w_up,
    w_down,
):
    bf16, f32 = jnp.bfloat16, jnp.float32
    kv_count = lax.axis_size(KV)
    core = lax.axis_index("tp")
    kv_index = lax.axis_index(KV)
    rows, cols = tokens.shape
    model_width = norm_gain.shape[0]
    heads = rec_state.shape[1]
    width = heads * HEAD_DIM
    half = rows // 2

    first, second = by_core(tokens, lax.ppermute(tokens, "tp", SWAP), core)
    block = jnp.concatenate([first, second], axis=1).astype(f32)
    gain = lax.dynamic_slice_in_dim(norm_gain, kv_index * 2 * cols, 2 * cols, 0)
    squares = jnp.sum(block * block, axis=1)
    high = squares.astype(bf16)
    low = (squares - high.astype(f32)).astype(bf16)
    scaled = (block * gain).astype(bf16)
    parts = [
        jnp.dot(scaled, w, preferred_element_type=f32).astype(bf16).reshape(rows, heads, HEAD_DIM)
        for w in (w_query, w_forget, w_input, w_outgate)
    ]
    extra = jnp.concatenate([high[:, None], low[:, None], jnp.zeros((rows, HEAD_DIM - 2), bf16)], axis=1)
    extra = jnp.broadcast_to(extra[:, None, :], (rows, heads, HEAD_DIM))
    pieces = jnp.concatenate(parts + [extra], axis=1)
    summed = jnp.sum(exchanged(pieces, KV).astype(f32), axis=0)
    row_scale = lax.rsqrt((summed[4 * heads, 0] + summed[4 * heads, 1]) / model_width + epsilon)
    scaled_sum = row_scale * summed[: 4 * heads].reshape(4, heads, HEAD_DIM)
    query_pre, forget_pre, value_in, gate_pre = [scaled_sum[i] for i in range(4)]

    bound = lower_bound.reshape(heads, HEAD_DIM)
    forget = bound + (1.0 - bound) * jax.nn.sigmoid(forget_pre)
    key_in = 1.0 - forget
    query_act = jax.nn.silu(query_pre)
    new_state = forget[:, :, None] * rec_state[0] + key_in[:, :, None] * value_in[:, None, :]
    head_out = jnp.sum(query_act[:, :, None] * new_state, axis=1)
    head_out = head_out * lax.rsqrt(jnp.mean(head_out * head_out, axis=1, keepdims=True) + epsilon)
    head_out = head_out * head_gain.reshape(heads, HEAD_DIM)
    gated = (head_out * jax.nn.silu(gate_pre)).astype(bf16)

    every_head = to_everyone(gated, KV_TP).reshape(rows, 2 * width)
    mixed = (tokens.astype(f32) + jnp.dot(every_head, w_heads_out, preferred_element_type=f32)).astype(bf16)

    packed = jnp.concatenate([mixed[:half], mixed[half:]], axis=1)
    own = to_everyone(packed, KV)
    first, second = by_core(own, lax.ppermute(own, "tp", SWAP), core)
    top = jnp.concatenate([first[:, :, :cols], second[:, :, :cols]], axis=2)
    bottom = jnp.concatenate([first[:, :, cols:], second[:, :, cols:]], axis=2)
    whole = jnp.concatenate([top, bottom], axis=1).transpose(1, 0, 2).reshape(rows, model_width)

    rows_float = whole.astype(f32)
    mixer_scale = lax.rsqrt(jnp.mean(rows_float * rows_float, axis=1, keepdims=True) + epsilon)
    normed = (rows_float * mixer_scale * mixer_gain).astype(bf16)
    gate_val = jnp.dot(normed, w_gate, preferred_element_type=f32)
    up_val = jnp.dot(normed, w_up, preferred_element_type=f32)
    hidden = (jax.nn.silu(gate_val) * up_val).astype(bf16)
    terms = jnp.dot(hidden, w_down, preferred_element_type=f32)

    terms = terms.reshape(rows, kv_count, 2, cols).transpose(2, 1, 0, 3)
    terms = jnp.concatenate([terms[:, :, :half], terms[:, :, half:]], axis=3)
    mine = lax.dynamic_index_in_dim(terms, core, 0, keepdims=False)
    theirs = lax.dynamic_index_in_dim(terms, 1 - core, 0, keepdims=False).astype(bf16)
    chip_sum = (mine + lax.ppermute(theirs, "tp", SWAP).astype(f32)).astype(bf16)
    down = jnp.sum(exchanged(chip_sum, KV).astype(f32), axis=0)
    down = jnp.concatenate([down[:, :cols], down[:, cols:]], axis=0)
    result = (mixed.astype(f32) + down).astype(bf16)
    return (result, new_state[None])


def solution(mesh):
    torus = Mesh(
        mesh.devices.reshape(mesh.shape["dp"], 8, 4, mesh.shape["tp"]), ("dp", "kv_0", "kv_1", "tp")
    )
    in_specs = (
        P("dp", KV_TP),
        P(DP_KV, "tp", None, None),
        P(),
        P(KV, "tp"),
        P(KV, "tp"),
        P(KV, "tp"),
        P(KV, "tp"),
        P("tp"),
        P("tp"),
        P(None, KV_TP),
        P(),
        P(None, KV_TP),
        P(None, KV_TP),
        P(KV_TP, None),
    )
    out_specs = (P("dp", KV_TP), P(DP_KV, "tp", None, None))
    return jax.shard_map(local, mesh=torus, in_specs=in_specs, out_specs=out_specs, check_vma=False)
```

time: 223 us -> 90.7 us (0.41)
  waiting for transfers between devices: 113 us -> 12.9 us
  between operations: 15.7 us -> 2.37 us
  local copies, waits for them, and re-layouts: 12 us -> 3.79 us
  starting transfers between devices: 10.8 us -> 4.17 us
  other arithmetic: 7.33 us -> 4.78 us
    unnamed x4 -> x0, waiting for transfers between devices: 102 us -> none
    all_to_all x2 -> x1, starting transfers between devices: 10.7 us -> 3.84 us  [exchanged(): return lax.all_to_all(pieces, axis, split_axis=0, concat_axis=0, tiled=True)]
    unnamed x35 -> x30, local copies, waits for them, and re-layouts: 4.91 us -> 0.23 us
    ppermute x0 -> x3, waiting for transfers between devices: none -> 2.95 us  [the longest x1 1.34 us: local(): first, second = by_core(own, lax.ppermute(own, 'tp', SWAP), core)]
    convert_element_type x6 -> x2, local copies, waits for them, and re-layouts: 2.64 us -> 0.2 us  [the longest x1 0.1 us: local(): high = squares.astype(bf16)]
    all_to_all x4 -> x3, blocking collectives: 56.1 us -> 55.3 us  [exchanged(): return lax.all_to_all(pieces, axis, split_axis=0, concat_axis=0, tiled=True)]
    all_to_all x2 -> x1, waiting for transfers between devices: 10.3 us -> 9.99 us  [exchanged(): return lax.all_to_all(pieces, axis, split_axis=0, concat_axis=0, tiled=True)]
  transfers between devices with their start and end apart: 4 -> 4, of which waited for: 4 -> 4; matrix products, arithmetic and copies ran while one was open for 1% -> 2% of each run, Pallas kernels for 0% -> 0%
where the time goes in v1:
time: 90.7 us; the launch traced here: 90.2 us
  blocking collectives  55.3 us (61%)
  waiting for transfers between devices  12.9 us (14%)
  matrix products  6.83 us (8%)
  other arithmetic  4.78 us (5%)
  starting transfers between devices  4.17 us (5%)
  local copies, waits for them, and re-layouts  3.79 us (4%)
  between operations  2.37 us (3%)
    all_to_all x3, blocking collectives, exchanged(): return lax.all_to_all(pieces, axis, split_axis=0, concat_axis=0, tiled=True)  55.3 us
    all_to_all x1, waiting for transfers between devices, exchanged(): return lax.all_to_all(pieces, axis, split_axis=0, concat_axis=0, tiled=True)  9.99 us
    all_to_all x1, starting transfers between devices, exchanged(): return lax.all_to_all(pieces, axis, split_axis=0, concat_axis=0, tiled=True)  3.84 us
    dot_general x4, matrix products, local(): jnp.dot(scaled, w, preferred_element_type=f32).astype(bf16)  3.52 us
    dot_general x1, matrix products, local(): terms = jnp.dot(hidden, w_down, preferred_element_type=f32)  2.55 us
  transfers between devices with their start and end apart: 4, of which 4 were waited for; matrix products, arithmetic and copies ran while one was open for 2% of the time, Pallas kernels for 0%

profile of v1, /device:TPU:6, one launch (start us, length us, event | category | flops | bytes accessed | tf_op | source)
XLA Modules:
  0.0 90.2 jit_solution(3835294606749847234)
XLA Ops:
  0.8 0.9 dynamic_slice.10
  1.7 0.4 collective-permute-done
  2.1 0.7 broadcast_select_fusion.3
  3.0 1.1 %fusion = bf16[4,8,8,128]{3,1,2,0:T(8,128)(2,1)S(1)} fusion(bf16[128,1024]{1,0:T(8,128)(2,1)} %param.17, bf16[32,128]{1,0:T(8,128)(2,1)S(1)} %get-tuple-element.5, f32[128]{0:T(128)S(1)} %dynamic_slice.10), kind=kOutput, calls=%fused_computation.4 | convolution fusion | flops 8433664 | bytes 336384 | tf_op jit(solution)/shard_map/dot_general | solution.py:64
  4.2 1.2 %fusion.1 = bf16[4,8,8,128]{3,1,2,0:T(8,128)(2,1)S(1)} fusion(bf16[128,1024]{1,0:T(8,128)(2,1)} %param.18, bf16[32,128]{1,0:T(8,128)(2,1)S(1)} %get-tuple-element.5, f32[128]{0:T(128)S(1)} %dynamic_slice.10), kind=kOutput, calls=%fused_computation.5 | convolution fusion | flops 8433664 | bytes 336384 | tf_op jit(solution)/shard_map/dot_general | solution.py:64
  5.4 1.1 %fusion.2 = bf16[4,8,8,128]{3,1,2,0:T(8,128)(2,1)S(1)} fusion(bf16[128,1024]{1,0:T(8,128)(2,1)} %param.19, bf16[32,128]{1,0:T(8,128)(2,1)S(1)} %get-tuple-element.5, f32[128]{0:T(128)S(1)} %dynamic_slice.10), kind=kOutput, calls=%fused_computation.6 | convolution fusion | flops 8433664 | bytes 336384 | tf_op jit(solution)/shard_map/dot_general | solution.py:64
  7.2 25.8 %all_to_all.20 = bf16[32,40,128]{2,1,0:T(8,128)(2,1)S(1)} all-to-all(bf16[32,40,128]{2,1,0:T(8,128)(2,1)S(1)} %broadcast_dynamic-update-slice_fusion), channel_id=1, replica_groups=mesh['dp'=4,'kv_0'=8,'kv_1'=4,'tp'=2] {'kv_0','kv_1'}, dimensions={0} | all-to-all | bytes 655360 | tf_op jit(solution)/shard_map/all_to_all | solution.py:17
  33.0 0.6 fusion.50
  35.0 0.5 fusion.12
  35.7 15.5 %all_to_all.21 = bf16[64,8,128]{2,1,0:T(8,128)(2,1)S(1)} all-to-all(bf16[64,8,128]{2,1,0:T(8,128)(2,1)S(1)} %broadcast_in_dim.10), channel_id=1, replica_groups=mesh['dp'=4,'kv_0'=8,'kv_1'=4,'tp'=2] {'kv_0','kv_1','tp'}, dimensions={0} | all-to-all | bytes 262144 | tf_op jit(solution)/shard_map/all_to_all | solution.py:17
  51.6 14.1 %all_to_all.22 = bf16[32,16,128]{2,1,0:T(8,128)(2,1)S(1)} all-to-all(bf16[32,16,128]{2,1,0:T(8,128)(2,1)S(1)} %broadcast_in_dim.11), channel_id=1, replica_groups=mesh['dp'=4,'kv_0'=8,'kv_1'=4,'tp'=2] {'kv_0','kv_1'}, dimensions={0} | all-to-all | bytes 262144 | tf_op jit(solution)/shard_map/all_to_all | solution.py:17
  65.7 1.3 %collective-permute-done.1 = bf16[32,16,128]{2,1,0:T(8,128)(2,1)S(1)} collective-permute-done((bf16[32,16,128]{2,1,0:T(8,128)(2,1)S(1)}, bf16[32,16,128]{2,1,0:T(8,128)(2,1)S(1)}, u32[]{:S(2)}, u32[]{:S(2)}) %collective-permute-start.1) | collective-permute-done | bytes 131104 | tf_op jit(solution)/shard_map/ppermute | solution.py:90
  67.2 0.3 fusion.7
  67.5 0.6 fusion.44
  68.1 2.6 %fusion.5 = f32[32,4096]{1,0:T(8,128)S(1)} fusion(bf16[176,4096]{1,0:T(8,128)(2,1)S(1)} %copy-done, bf16[4096,176]{0,1:T(8,128)(2,1)} %param.26, f32[32,176]{1,0:T(8,128)S(1)} %fusion.44, f32[4096]{0:T(1024)S(1)} %copy-done.7, f32[32]{0:T(128)S(1)} %add_rsqrt_fusion, bf16[32,16,64]{2,1,0:T(8,128)(2,1)S(1)} %get-tuple-element.26, ...), kind=kOutput, calls=%fused_computation.10 | convolution fusion | flops 93750272 | bytes 3709056 | tf_op jit(solution)/shard_map/dot_general | solution.py:101
  70.7 0.8 reshape.147
  71.4 0.6 copy.35
  72.3 0.2 collective-permute-start.2
  72.5 1.2 %collective-permute-done.2 = bf16[32,16,128]{2,1,0:T(8,128)(2,1)S(1)} collective-permute-done((bf16[32,16,128]{2,1,0:T(8,128)(2,1)S(1)}, bf16[32,16,128]{2,1,0:T(8,128)(2,1)S(1)}, u32[]{:S(2)}, u32[]{:S(2)}) %collective-permute-start.2) | collective-permute-done | bytes 131104 | tf_op jit(solution)/shard_map/ppermute | solution.py:107
  73.7 0.8 fusion.18
  74.5 3.8 %all-to-all-start.3 = ((bf16[32,16,128]{2,1,0:T(8,128)(2,1)}), bf16[32,16,128]{2,1,0:T(8,128)(2,1)S(1)}, u32[]{:S(2)}, u32[]{:S(2)}) async-start(bf16[32,16,128]{2,1,0:T(8,128)(2,1)} %fusion.18), calls=%async_computation.3 | async-start | bytes 262144 | tf_op jit(solution)/shard_map/all_to_all | solution.py:17
  78.4 1.1 %multiply_add_fusion = f32[1,8,128,128]{3,2,1,0:T(8,128)} fusion(f32[1,8,128,128]{3,2,1,0:T(8,128)S(1)} %copy-done.1, f32[8,128]{1,0:T(8,128)S(1)} %get-tuple-element.17, f32[8,128]{1,0:T(8,128)S(1)} %get-tuple-element.18, f32[8,128]{1,0:T(8,128)S(1)} %copy-done.5), kind=kLoop, calls=%fused_computation.25 | loop fusion | flops 393216 | bytes 1060864 | tf_op jit(solution)/shard_map/add | solution.py:79
  79.5 10.0 %all-to-all-done.3 = bf16[32,16,128]{2,1,0:T(8,128)(2,1)S(1)} async-done(((bf16[32,16,128]{2,1,0:T(8,128)(2,1)}), bf16[32,16,128]{2,1,0:T(8,128)(2,1)S(1)}, u32[]{:S(2)}, u32[]{:S(2)}) %all-to-all-start.3) | async-done | bytes 131104 | tf_op jit(solution)/shard_map/all_to_all | solution.py:17
  89.6 0.6 fusion.27
  (61 shorter events, 2.2 us)
Async XLA Ops:
  0.6 67.5 %copy-start = (bf16[176,4096]{1,0:T(8,128)(2,1)S(1)}, bf16[176,4096]{1,0:T(8,128)(2,1)}, u32[]{:S(2)}) copy-start(bf16[176,4096]{1,0:T(8,128)(2,1)} %param.27) | copy-start | bytes 4325380
  0.6 5.9 %copy-start.2 = (bf16[128,1024]{1,0:T(8,128)(2,1)S(1)}, bf16[128,1024]{1,0:T(8,128)(2,1)}, u32[]{:S(2)}) copy-start(bf16[128,1024]{1,0:T(8,128)(2,1)} %param.20) | copy-start | bytes 786436
  0.7 1.5 %collective-permute-start = (bf16[32,64]{1,0:T(8,128)(2,1)}, bf16[32,64]{1,0:T(8,128)(2,1)S(1)}, u32[]{:S(2)}, u32[]{:S(2)}) collective-permute-start(bf16[32,64]{1,0:T(8,128)(2,1)} %param.14), channel_id=1, source_target_pairs={{0,1},{1,0},{2,3},{3,2},{4,5},{5,4},{6,7},{7,6},{8,9},{9,8},{10,11... | collective-permute-start | bytes 12296 | tf_op jit(solution)/shard_map/ppermute | solution.py:56
  4.2 30.8 %copy-start.9 = (f32[1024]{0:T(1024)S(1)}, f32[1024]{0:T(1024)}, u32[]{:S(2)}) copy-start(f32[1024]{0:T(1024)} %param.21) | copy-start | bytes 12292
  4.2 30.8 %copy-start.1 = (f32[1,8,128,128]{3,2,1,0:T(8,128)S(1)}, f32[1,8,128,128]{3,2,1,0:T(8,128)}, u32[]{:S(2)}) copy-start(f32[1,8,128,128]{3,2,1,0:T(8,128)} %param.15) | copy-start | bytes 1572868
  6.5 29.1 %copy-start.8 = (f32[1024]{0:T(1024)S(1)}, f32[1024]{0:T(1024)}, u32[]{:S(2)}) copy-start(f32[1024]{0:T(1024)} %param.22) | copy-start | bytes 12292
  6.8 44.5 %copy-start.3 = (bf16[2048,64]{0,1:T(8,128)(2,1)S(1)}, bf16[2048,64]{0,1:T(8,128)(2,1)}, u32[]{:S(2)}) copy-start(bf16[2048,64]{0,1:T(8,128)(2,1)} %param.23) | copy-start | bytes 786436
  6.8 44.5 %copy-start.6 = (bf16[32,64]{1,0:T(8,128)(2,1)S(1)}, bf16[32,64]{1,0:T(8,128)(2,1)}, u32[]{:S(2)}) copy-start(bf16[32,64]{1,0:T(8,128)(2,1)} %param.14) | copy-start | bytes 12292
  35.0 32.2 %copy-start.4 = (f32[8,128]{1,0:T(8,128)}, f32[8,128]{1,0:T(8,128)S(1)}, u32[]{:S(2)}) copy-start(f32[8,128]{1,0:T(8,128)S(1)} %get-tuple-element.19) | copy-start | bytes 12292
  51.3 16.2 %copy-start.7 = (f32[4096]{0:T(1024)S(1)}, f32[4096]{0:T(1024)}, u32[]{:S(2)}) copy-start(f32[4096]{0:T(1024)} %param.24) | copy-start | bytes 49156
  65.7 1.3 %collective-permute-start.1 = (bf16[32,16,128]{2,1,0:T(8,128)(2,1)S(1)}, bf16[32,16,128]{2,1,0:T(8,128)(2,1)S(1)}, u32[]{:S(2)}, u32[]{:S(2)}) collective-permute-start(bf16[32,16,128]{2,1,0:T(8,128)(2,1)S(1)} %all_to_all.22), channel_id=1, source_target_pairs={{0,1},{1,0},{2,3},{3,2},{4,5},{5,4},{6,7},{7,6},{8,9},{9,8},{10,11... | collective-permute-start | bytes 393224 | tf_op jit(solution)/shard_map/ppermute | solution.py:90
  65.7 1.8 %copy-start.10 = (bf16[4096,176]{0,1:T(8,128)(2,1)S(1)}, bf16[4096,176]{0,1:T(8,128)(2,1)}, u32[]{:S(2)}) copy-start(bf16[4096,176]{0,1:T(8,128)(2,1)} %param.25) | copy-start | bytes 4325380
  72.2 6.2 %copy-start.5 = (f32[8,128]{1,0:T(8,128)S(1)}, f32[8,128]{1,0:T(8,128)}, u32[]{:S(2)}) copy-start(f32[8,128]{1,0:T(8,128)} %copy-done.4) | copy-start | bytes 12292
  72.3 1.4 %collective-permute-start.2 = (bf16[32,16,128]{2,1,0:T(8,128)(2,1)S(1)}, bf16[32,16,128]{2,1,0:T(8,128)(2,1)S(1)}, u32[]{:S(2)}, u32[]{:S(2)}) collective-permute-start(bf16[32,16,128]{2,1,0:T(8,128)(2,1)S(1)} %fusion.19), channel_id=1, source_target_pairs={{0,1},{1,0},{2,3},{3,2},{4,5},{5,4},{6,7},{7,6},{8,9},{9,8},{10,11... | collective-permute-start | bytes 393224 | tf_op jit(solution)/shard_map/ppermute | solution.py:107
  74.5 15.0 %all-to-all-start.3 = ((bf16[32,16,128]{2,1,0:T(8,128)(2,1)}), bf16[32,16,128]{2,1,0:T(8,128)(2,1)S(1)}, u32[]{:S(2)}, u32[]{:S(2)}) async-start(bf16[32,16,128]{2,1,0:T(8,128)(2,1)} %fusion.18), calls=%async_computation.3 | async-start | bytes 262144 | tf_op jit(solution)/shard_map/all_to_all | solution.py:17

commit v2 on v1

v2 whole, which is shorter than its diff:
```python
import jax
import jax.numpy as jnp
from jax import lax
from jax.experimental import pallas as pl
from jax.experimental.pallas import tpu as pltpu
from jax.sharding import Mesh
from jax.sharding import PartitionSpec as P

LANES = 128
KV = ("kv_0", "kv_1")
KV_TP = ("kv_0", "kv_1", "tp")
DP_KV = ("dp", "kv_0", "kv_1")
SWAP = [(0, 1), (1, 0)]
NT = (((1,), (1,)), ((), ()))

epsilon = 1e-06
bf16, f32 = jnp.bfloat16, jnp.float32


def exchanged(pieces, axis):
    return lax.all_to_all(pieces, axis, split_axis=0, concat_axis=0, tiled=True)


def lanes_below(core, shape):
    lane = lax.broadcasted_iota(jnp.int32, shape, len(shape) - 1)
    return (lane < LANES // 2) == (core == 0)


def half_turn(x):
    return pltpu.roll(x, LANES // 2, axis=x.ndim - 1)


def in_vmem(count):
    return [pl.BlockSpec(memory_space=pltpu.VMEM)] * count


IN_SMEM = pl.BlockSpec(memory_space=pltpu.SMEM)


def project_kernel(where, own, other, gain, wq, wf, wi, wg, out, rows_scr):
    kv, core = where[0], where[1]
    rows = own.shape[0]
    pair = jnp.concatenate([own[...].astype(f32), other[...].astype(f32)], axis=1)
    block = jnp.where(core == 0, pair, half_turn(pair))
    squares = jnp.sum(block * block, axis=1, keepdims=True)
    high = squares.astype(bf16).astype(f32)
    lane = lax.broadcasted_iota(jnp.int32, (rows, LANES), 1)
    extra = jnp.where(lane == 0, high, jnp.where(lane == 1, squares - high, 0.0))
    scaled = (block * gain[pl.ds(kv, 1), :]).astype(bf16)
    heads = wq.shape[1] // LANES
    step = out.shape[1]
    for index, weight in enumerate((wq, wf, wi, wg)):
        part = jnp.dot(scaled, weight[...], preferred_element_type=f32)
        for head in range(heads):
            rows_scr[pl.ds(index * heads + head, rows, stride=step), :] = part[
                :, head * LANES : (head + 1) * LANES
            ]
    for row in range(4 * heads, step):
        rows_scr[pl.ds(row, rows, stride=step), :] = extra
    for row in range(rows):
        out[row] = rows_scr[pl.ds(row * step, step), :].astype(bf16)


def recur_kernel(pieces, state, bound, gain, gated, forget_out, value_out, width):
    heads = state.shape[0]
    total = jnp.sum(pieces[...].astype(f32), axis=0)
    squares = total[4 * heads : 4 * heads + 1, 0:1] + total[4 * heads : 4 * heads + 1, 1:2]
    row_scale = lax.rsqrt(squares / width + epsilon)
    query_pre, forget_pre, value_in, gate_pre = [
        row_scale * total[i * heads : (i + 1) * heads] for i in range(4)
    ]
    forget = bound[...] + (1.0 - bound[...]) * jax.nn.sigmoid(forget_pre)
    key_in = 1.0 - forget
    query_act = jax.nn.silu(query_pre)
    forget_out[...] = forget
    value_out[...] = value_in
    fresh = jnp.sum(query_act * key_in, axis=1, keepdims=True) * value_in
    reads = jnp.transpose(query_act * forget)
    kept = jnp.concatenate(
        [
            jnp.sum(reads[:, head : head + 1] * state[head], axis=0, keepdims=True)
            for head in range(heads)
        ],
        axis=0,
    )
    head_out = kept + fresh
    head_out = head_out * lax.rsqrt(
        jnp.mean(head_out * head_out, axis=1, keepdims=True) + epsilon
    )
    value = (head_out * gain[...] * jax.nn.silu(gate_pre)).astype(bf16)
    for peer in range(gated.shape[0]):
        gated[peer] = value


def mix_kernel(where, every, tokens, weight, out, rows_scr, whole_scr):
    core = where[1]
    rows = tokens.shape[0]
    peers, heads, _ = every.shape
    per_row = peers * heads // rows
    rows_scr[...] = every[...].astype(f32).reshape(peers * heads, LANES)
    for head in range(per_row):
        whole_scr[:, head * LANES : (head + 1) * LANES] = rows_scr[
            pl.ds(head, rows, stride=per_row), :
        ].astype(bf16)
    added = lax.dot_general(whole_scr[...], weight[...], NT, preferred_element_type=f32)
    mixed = tokens[...].astype(f32) + added
    half = rows // 2
    packed = jnp.concatenate([mixed[:half], mixed[half:]], axis=1)
    packed = jnp.where(core == 0, packed, half_turn(packed)).astype(bf16)
    for peer in range(out.shape[0]):
        out[peer] = packed


def feed_kernel(where, own, other, gain, w_gate, w_up, w_down, mine, theirs, scr):
    core = where[1]
    blocks, half, _ = own.shape
    rows = 2 * half
    mask = lanes_below(core, (half, LANES))
    squares = jnp.zeros((rows, LANES), f32)
    for block in range(blocks):
        a, b = own[block].astype(f32), other[block].astype(f32)
        top = jnp.where(mask, a, b)
        bottom = half_turn(jnp.where(mask, b, a))
        value = jnp.concatenate([top, bottom], axis=0)
        squares = squares + value * value
        scr[:, block * LANES : (block + 1) * LANES] = (value * gain[pl.ds(block, 1), :]).astype(bf16)
    mean = jnp.sum(squares, axis=1, keepdims=True) / (blocks * LANES)
    scale = lax.rsqrt(mean + epsilon)
    normed = scr[...]
    gate = scale * lax.dot_general(normed, w_gate[...], NT, preferred_element_type=f32)
    up = scale * lax.dot_general(normed, w_up[...], NT, preferred_element_type=f32)
    hidden = (jax.nn.silu(gate) * up).astype(bf16)
    terms = jnp.dot(hidden, w_down[...], preferred_element_type=f32)
    for block in range(blocks):
        term = terms[:, block * LANES : (block + 1) * LANES]
        top, bottom = term[:half], half_turn(term[half:])
        mine[block] = jnp.where(mask, top, bottom)
        theirs[block] = jnp.where(mask, bottom, top).astype(bf16)


def sum_kernel(mine, theirs, out):
    out[...] = (mine[...] + theirs[...].astype(f32)).astype(bf16)


def finish_kernel(where, pieces, mixed, out):
    core = where[1]
    half = mixed.shape[1]
    total = mixed[0].astype(f32) + jnp.sum(pieces[...].astype(f32), axis=0)
    total = jnp.where(core == 0, total, half_turn(total))
    out[:half] = total[:, : LANES // 2].astype(bf16)
    out[half:] = half_turn(total)[:, : LANES // 2].astype(bf16)


def local(
    tokens,
    rec_state,
    norm_gain,
    w_query,
    w_forget,
    w_input,
    w_outgate,
    lower_bound,
    head_gain,
    w_heads_out,
    mixer_gain,
    w_gate,
    w_up,
    w_down,
):
    kv_count = lax.axis_size(KV)
    where = jnp.stack([lax.axis_index(KV), lax.axis_index("tp")]).astype(jnp.int32)
    rows, cols = tokens.shape
    width = norm_gain.shape[0]
    heads = rec_state.shape[1]
    half = rows // 2
    blocks = width // LANES
    shape = jax.ShapeDtypeStruct
    piece_rows = 5 * heads

    other = lax.ppermute(tokens, "tp", SWAP)
    pieces = pl.pallas_call(
        project_kernel,
        out_shape=shape((rows, piece_rows, LANES), bf16),
        in_specs=[IN_SMEM] + in_vmem(7),
        out_specs=in_vmem(1)[0],
        scratch_shapes=[pltpu.VMEM((rows * piece_rows, LANES), f32)],
        name="project",
    )(where, tokens, other, norm_gain.reshape(blocks, LANES), w_query, w_forget, w_input, w_outgate)
    pieces = exchanged(pieces, KV)

    per_head = shape((heads, LANES), f32)
    gated, forget, value_in = pl.pallas_call(
        lambda *refs: recur_kernel(*refs, width),
        out_shape=(shape((2 * kv_count, heads, LANES), bf16), per_head, per_head),
        in_specs=in_vmem(4),
        out_specs=tuple(in_vmem(3)),
        name="recur",
    )(pieces, rec_state[0], lower_bound.reshape(heads, LANES), head_gain.reshape(heads, LANES))
    new_state = forget[:, :, None] * rec_state[0] + (1.0 - forget)[:, :, None] * value_in[:, None, :]

    every = exchanged(gated, KV_TP)
    mixed = pl.pallas_call(
        mix_kernel,
        out_shape=shape((kv_count, half, LANES), bf16),
        in_specs=[IN_SMEM] + in_vmem(3),
        out_specs=in_vmem(1)[0],
        scratch_shapes=[
            pltpu.VMEM((2 * kv_count * heads, LANES), f32),
            pltpu.VMEM((rows, 2 * heads * LANES), bf16),
        ],
        name="mix",
    )(where, every, tokens, w_heads_out.T)

    own = exchanged(mixed, KV)
    other = lax.ppermute(own, "tp", SWAP)
    mine, theirs = pl.pallas_call(
        feed_kernel,
        out_shape=(shape((kv_count, half, LANES), f32), shape((kv_count, half, LANES), bf16)),
        in_specs=[IN_SMEM] + in_vmem(6),
        out_specs=tuple(in_vmem(2)),
        scratch_shapes=[pltpu.VMEM((rows, width), bf16)],
        name="feed",
    )(where, own, other, mixer_gain.reshape(blocks, LANES), w_gate.T, w_up.T, w_down)
    theirs = lax.ppermute(theirs, "tp", SWAP)
    chip_sum = pl.pallas_call(
        sum_kernel,
        out_shape=shape((kv_count, half, LANES), bf16),
        in_specs=in_vmem(2),
        out_specs=in_vmem(1)[0],
        name="chip_sum",
    )(mine, theirs)
    down = exchanged(chip_sum, KV)
    result = pl.pallas_call(
        finish_kernel,
        out_shape=shape((rows, cols), bf16),
        in_specs=[IN_SMEM] + in_vmem(2),
        out_specs=in_vmem(1)[0],
        name="finish",
    )(where, down, mixed)
    return (result, new_state[None])


def solution(mesh):
    torus = Mesh(
        mesh.devices.reshape(mesh.shape["dp"], 8, 4, mesh.shape["tp"]), ("dp", "kv_0", "kv_1", "tp")
    )
    in_specs = (
        P("dp", KV_TP),
        P(DP_KV, "tp", None, None),
        P(),
        P(KV, "tp"),
        P(KV, "tp"),
        P(KV, "tp"),
        P(KV, "tp"),
        P("tp"),
        P("tp"),
        P(None, KV_TP),
        P(),
        P(None, KV_TP),
        P(None, KV_TP),
        P(KV_TP, None),
    )
    out_specs = (P("dp", KV_TP), P(DP_KV, "tp", None, None))
    return jax.shard_map(local, mesh=torus, in_specs=in_specs, out_specs=out_specs, check_vma=False)
```

time: 90.7 us -> 95.4 us (1.052)
  Pallas kernels: 0 us -> 14.9 us
  matrix products: 6.83 us -> 0 us
  other arithmetic: 4.78 us -> 1.79 us
  blocking collectives: 55.3 us -> 57.6 us
  between operations: 2.37 us -> 0.7 us
  local copies, waits for them, and re-layouts: 3.79 us -> 2.56 us
    pallas_call x0 -> x6, Pallas kernels: none -> 14.9 us  [the longest x1 4.6 us: local(): pl.pallas_call(feed_kernel, out_shape=(shape((kv_count, half, LANES), f32...]
    dot_general x7 -> x0, matrix products: 6.83 us -> none  [the longest x4 3.52 us: local(): jnp.dot(scaled, w, preferred_element_type=f32).astype(bf16)]
    unnamed x30 -> x16, local copies, waits for them, and re-layouts: 0.23 us -> 2.56 us
    all_to_all x3, blocking collectives: 55.3 us -> 57.6 us  [exchanged(): return lax.all_to_all(pieces, axis, split_axis=0, concat_axis=0, tiled=True)]
    convert_element_type x6 -> x0, other arithmetic: 1.59 us -> none  [the longest x1 0.79 us: local(): (mine + lax.ppermute(theirs, 'tp', SWAP).astype(f32)).astype(bf16)]
    reshape x3 -> x0, local copies, waits for them, and re-layouts: 1.44 us -> none  [the longest x2 1.38 us: local(): terms = terms.reshape(rows, kv_count, 2, cols).transpose(2, 1, 0, 3)]
    reduce_sum x6 -> x0, other arithmetic: 1.14 us -> none  [the longest x1 0.48 us: local(): head_out = jnp.sum(query_act[:, :, None] * new_state, axis=1)]
where the time goes in v2:
time: 95.4 us; the launch traced here: 95 us
  blocking collectives  57.6 us (60%)
  Pallas kernels  14.9 us (16%)
  waiting for transfers between devices  13.4 us (14%)
  starting transfers between devices  4.1 us (4%)
  local copies, waits for them, and re-layouts  2.56 us (3%)
  other arithmetic  1.79 us (2%)
    all_to_all x3, blocking collectives, exchanged(): return lax.all_to_all(pieces, axis, split_axis=0, concat_axis=0, tiled=True)  57.6 us
    all_to_all x1, waiting for transfers between devices, exchanged(): return lax.all_to_all(pieces, axis, split_axis=0, concat_axis=0, tiled=True)  9.96 us
    pallas_call x1, Pallas kernels, local(): pl.pallas_call(feed_kernel, out_shape=(shape((kv_count, half, LANES), f32...  4.6 us
    all_to_all x1, starting transfers between devices, exchanged(): return lax.all_to_all(pieces, axis, split_axis=0, concat_axis=0, tiled=True)  3.85 us
    unnamed x16, local copies, waits for them, and re-layouts  2.56 us
    pallas_call x1, Pallas kernels, local(): pl.pallas_call(project_kernel, out_shape=shape((rows, piece_rows, LANES),...  2.39 us
    pallas_call x1, Pallas kernels, local(): pl.pallas_call(lambda *refs: recur_kernel(*refs, width), out_shape=(shape...  2.37 us
    pallas_call x1, Pallas kernels, local(): pl.pallas_call(mix_kernel, out_shape=shape((kv_count, half, LANES), bf16)...  2.09 us
  transfers between devices with their start and end apart: 4, of which 4 were waited for; matrix products, arithmetic and copies ran while one was open for 2% of the time, Pallas kernels for 0%

profile of v2, /device:TPU:6, one launch (start us, length us, event | category | flops | bytes accessed | tf_op | source)
XLA Modules:
  0.0 95.0 jit_solution(4011665783161594465)
XLA Ops:
  0.6 0.1 collective-permute-start
  0.7 0.6 pad_add_fusion.where
  1.4 0.7 collective-permute-done.other
  2.1 0.6 copy-done.6
  2.7 2.4 %project.1 = bf16[32,40,128]{2,1,0:T(8,128)(2,1)} custom-call(s32[2]{0:T(128)} %pad_add_fusion.where, bf16[32,64]{1,0:T(8,128)(2,1)} %tokens.1, bf16[32,64]{1,0:T(8,128)(2,1)} %copy-done.6, f32[32,128]{1,0:T(8,128)} %bitcast.14, bf16[128,1024]{1,0:T(8,128)(2,1)} %wq.1, bf16[128,1024]{1,0:T(8,128)(2,1)} %wf.1, bf16[128,1024]{1,0:T(8,128)(2,1)} %wi.1, ...), custom_call_target="tpu_custom_call" | custom-call | tf_op jit(solution)/shard_map/project/pallas_call | solution.py:181
  5.1 26.1 %all_to_all.20.refs_0_ = bf16[32,40,128]{2,1,0:T(8,128)(2,1)} all-to-all(bf16[32,40,128]{2,1,0:T(8,128)(2,1)} %project.1), channel_id=1, replica_groups=mesh['dp'=4,'kv_0'=8,'kv_1'=4,'tp'=2] {'kv_0','kv_1'}, dimensions={0} | all-to-all | bytes 655360 | tf_op jit(solution)/shard_map/all_to_all | solution.py:21
  31.2 2.4 %recur.1 = (bf16[64,8,128]{2,1,0:T(8,128)(2,1)}, f32[8,128]{1,0:T(8,128)}, f32[8,128]{1,0:T(8,128)}) custom-call(bf16[32,40,128]{2,1,0:T(8,128)(2,1)} %all_to_all.20.refs_0_, f32[8,128,128]{2,1,0:T(8,128)} %bitcast.10, f32[8,128]{1,0:T(8,128)} %bitcast.16, f32[8,128]{1,0:T(8,128)} %bitcast.17), custom_call_target="tpu_custom_call" | custom-call | tf_op jit(solution)/shard_map/recur/pallas_call | solution.py:192
  33.6 16.5 %all_to_all.21.every = bf16[64,8,128]{2,1,0:T(8,128)(2,1)} all-to-all(bf16[64,8,128]{2,1,0:T(8,128)(2,1)} %get-tuple-element.7), channel_id=1, replica_groups=mesh['dp'=4,'kv_0'=8,'kv_1'=4,'tp'=2] {'kv_0','kv_1','tp'}, dimensions={0} | all-to-all | bytes 262144 | tf_op jit(solution)/shard_map/all_to_all | solution.py:21
  50.1 2.1 %mix.1.mixed = bf16[32,16,128]{2,1,0:T(8,128)(2,1)} custom-call(s32[2]{0:T(128)} %pad_add_fusion.where, bf16[64,8,128]{2,1,0:T(8,128)(2,1)} %all_to_all.21.every, bf16[32,64]{1,0:T(8,128)(2,1)} %tokens.1, bf16[64,2048]{1,0:T(8,128)(2,1)} %bitcast.13), custom_call_target="tpu_custom_call" | custom-call | tf_op jit(solution)/shard_map/mix/pallas_call | solution.py:202
  52.2 14.9 %all_to_all.22.own = bf16[32,16,128]{2,1,0:T(8,128)(2,1)S(1)} all-to-all(bf16[32,16,128]{2,1,0:T(8,128)(2,1)} %mix.1.mixed), channel_id=1, replica_groups=mesh['dp'=4,'kv_0'=8,'kv_1'=4,'tp'=2] {'kv_0','kv_1'}, dimensions={0} | all-to-all | bytes 262144 | tf_op jit(solution)/shard_map/all_to_all | solution.py:21
  67.1 0.0 collective-permute-start.1
  67.1 1.3 %collective-permute-done.1.other = bf16[32,16,128]{2,1,0:T(8,128)(2,1)S(1)} collective-permute-done((bf16[32,16,128]{2,1,0:T(8,128)(2,1)S(1)}, bf16[32,16,128]{2,1,0:T(8,128)(2,1)S(1)}, u32[]{:S(2)}, u32[]{:S(2)}) %collective-permute-start.1) | collective-permute-done | bytes 131104 | tf_op jit(solution)/shard_map/ppermute | solution.py:215
  68.5 0.0 copy-done.1
  68.5 0.6 copy-done.3
  69.1 4.6 %feed.1 = (f32[32,16,128]{2,1,0:T(8,128)}, bf16[32,16,128]{2,1,0:T(8,128)(2,1)}) custom-call(s32[2]{0:T(128)} %pad_add_fusion.where, bf16[32,16,128]{2,1,0:T(8,128)(2,1)} %copy-done.1, bf16[32,16,128]{2,1,0:T(8,128)(2,1)} %copy-done.3, f32[32,128]{1,0:T(8,128)} %bitcast.15, bf16[176,4096]{1,0:T(8,128)(2,1)} %bitcast.11, bf16[176,4096]{1,0:T(8,128)(2,1)} %bitcast.12, ...), custom_call_target="tpu_custom_call" | custom-call | tf_op jit(solution)/shard_map/feed/pallas_call | solution.py:216
  73.7 0.1 collective-permute-start.2
  73.9 1.4 %collective-permute-done.2.theirs = bf16[32,16,128]{2,1,0:T(8,128)(2,1)S(1)} collective-permute-done((bf16[32,16,128]{2,1,0:T(8,128)(2,1)}, bf16[32,16,128]{2,1,0:T(8,128)(2,1)S(1)}, u32[]{:S(2)}, u32[]{:S(2)}) %collective-permute-start.2) | collective-permute-done | bytes 131104 | tf_op jit(solution)/shard_map/ppermute | solution.py:224
  75.3 0.6 copy-done.4
  75.9 1.7 %chip_sum.1 = bf16[32,16,128]{2,1,0:T(8,128)(2,1)} custom-call(f32[32,16,128]{2,1,0:T(8,128)} %get-tuple-element.8.mine, bf16[32,16,128]{2,1,0:T(8,128)(2,1)} %copy-done.4), custom_call_target="tpu_custom_call" | custom-call | tf_op jit(solution)/shard_map/chip_sum/pallas_call | solution.py:225
  77.6 3.9 %all-to-all-start.3 = ((bf16[32,16,128]{2,1,0:T(8,128)(2,1)}), bf16[32,16,128]{2,1,0:T(8,128)(2,1)S(1)}, u32[]{:S(2)}, u32[]{:S(2)}) async-start(bf16[32,16,128]{2,1,0:T(8,128)(2,1)} %chip_sum.1), calls=%async_computation.3 | async-start | bytes 262144 | tf_op jit(solution)/shard_map/all_to_all | solution.py:21
  81.5 1.1 %multiply_add_fusion = f32[1,8,128,128]{3,2,1,0:T(8,128)} fusion(f32[1,8,128,128]{3,2,1,0:T(8,128)S(1)} %copy-done, f32[8,128]{1,0:T(8,128)S(1)} %copy-done.7, f32[8,128]{1,0:T(8,128)S(1)} %broadcast_subtract_fusion, f32[8,128]{1,0:T(8,128)S(1)} %copy-done.5), kind=kLoop, calls=%fused_computation | loop fusion | flops 393216 | bytes 1060864 | tf_op jit(solution)/shard_map/add | solution.py:199
  82.6 10.0 %all-to-all-done.3.pieces = bf16[32,16,128]{2,1,0:T(8,128)(2,1)S(1)} async-done(((bf16[32,16,128]{2,1,0:T(8,128)(2,1)}), bf16[32,16,128]{2,1,0:T(8,128)(2,1)S(1)}, u32[]{:S(2)}, u32[]{:S(2)}) %all-to-all-start.3) | async-done | bytes 131104 | tf_op jit(solution)/shard_map/all_to_all | solution.py:21
  92.6 0.6 copy-done.2
  93.2 1.8 %finish.1 = bf16[32,64]{1,0:T(8,128)(2,1)} custom-call(s32[2]{0:T(128)} %pad_add_fusion.where, bf16[32,16,128]{2,1,0:T(8,128)(2,1)} %copy-done.2, bf16[32,16,128]{2,1,0:T(8,128)(2,1)} %mix.1.mixed), custom_call_target="tpu_custom_call" | custom-call | tf_op jit(solution)/shard_map/finish/pallas_call | solution.py:233
  (12 shorter events, 0.0 us)
Async XLA Ops:
  0.6 1.5 %collective-permute-start = (bf16[32,64]{1,0:T(8,128)(2,1)}, bf16[32,64]{1,0:T(8,128)(2,1)S(1)}, u32[]{:S(2)}, u32[]{:S(2)}) collective-permute-start(bf16[32,64]{1,0:T(8,128)(2,1)} %tokens.1), channel_id=1, source_target_pairs={{0,1},{1,0},{2,3},{3,2},{4,5},{5,4},{6,7},{7,6},{8,9},{9,8},{10,11... | collective-permute-start | bytes 12296 | tf_op jit(solution)/shard_map/ppermute | solution.py:180
  2.1 0.6 copy-start.6
  67.1 1.4 %copy-start.1 = (bf16[32,16,128]{2,1,0:T(8,128)(2,1)}, bf16[32,16,128]{2,1,0:T(8,128)(2,1)S(1)}, u32[]{:S(2)}) copy-start(bf16[32,16,128]{2,1,0:T(8,128)(2,1)S(1)} %all_to_all.22.own) | copy-start | bytes 393220
  67.1 1.3 %collective-permute-start.1 = (bf16[32,16,128]{2,1,0:T(8,128)(2,1)S(1)}, bf16[32,16,128]{2,1,0:T(8,128)(2,1)S(1)}, u32[]{:S(2)}, u32[]{:S(2)}) collective-permute-start(bf16[32,16,128]{2,1,0:T(8,128)(2,1)S(1)} %all_to_all.22.own), channel_id=1, source_target_pairs={{0,1},{1,0},{2,3},{3,2},{4,5},{5,4},{6,7},{7,6},{8,9},{9,8},{10,11... | collective-permute-start | bytes 393224 | tf_op jit(solution)/shard_map/ppermute | solution.py:215
  68.5 0.7 copy-start.3
  69.1 12.3 %copy-start.5 = (f32[8,128]{1,0:T(8,128)S(1)}, f32[8,128]{1,0:T(8,128)}, u32[]{:S(2)}) copy-start(f32[8,128]{1,0:T(8,128)} %get-tuple-element.10) | copy-start | bytes 12292
  69.1 12.4 %copy-start = (f32[1,8,128,128]{3,2,1,0:T(8,128)S(1)}, f32[1,8,128,128]{3,2,1,0:T(8,128)}, u32[]{:S(2)}) copy-start(f32[1,8,128,128]{3,2,1,0:T(8,128)} %param.15) | copy-start | bytes 1572868
  69.1 12.4 %copy-start.7 = (f32[8,128]{1,0:T(8,128)S(1)}, f32[8,128]{1,0:T(8,128)}, u32[]{:S(2)}) copy-start(f32[8,128]{1,0:T(8,128)} %get-tuple-element.11) | copy-start | bytes 12292
  73.7 1.6 %collective-permute-start.2 = (bf16[32,16,128]{2,1,0:T(8,128)(2,1)}, bf16[32,16,128]{2,1,0:T(8,128)(2,1)S(1)}, u32[]{:S(2)}, u32[]{:S(2)}) collective-permute-start(bf16[32,16,128]{2,1,0:T(8,128)(2,1)} %get-tuple-element.9), channel_id=1, source_target_pairs={{0,1},{1,0},{2,3},{3,2},{4,5},{5,4},{6,7},{7,6},{8,9},{9,8},{10,11... | collective-permute-start | bytes 393224 | tf_op jit(solution)/shard_map/ppermute | solution.py:224
  75.3 0.7 copy-start.4
  77.6 15.0 %all-to-all-start.3 = ((bf16[32,16,128]{2,1,0:T(8,128)(2,1)}), bf16[32,16,128]{2,1,0:T(8,128)(2,1)S(1)}, u32[]{:S(2)}, u32[]{:S(2)}) async-start(bf16[32,16,128]{2,1,0:T(8,128)(2,1)} %chip_sum.1), calls=%async_computation.3 | async-start | bytes 262144 | tf_op jit(solution)/shard_map/all_to_all | solution.py:21
  92.6 0.6 copy-start.2

commit v3 on v2

--- a/solution.py
+++ b/solution.py
@@ -34,11 +34,33 @@
     return [pl.BlockSpec(memory_space=pltpu.VMEM)] * count
 
 
-IN_SMEM = pl.BlockSpec(memory_space=pltpu.SMEM)
-
-
-def project_kernel(where, own, other, gain, wq, wf, wi, wg, out, rows_scr):
-    kv, core = where[0], where[1]
+def held(*arrays):
+    return [pltpu.with_memory_space_constraint(array, pltpu.VMEM) for array in arrays]
+
+
+def far(*arrays):
+    return [pltpu.with_memory_space_constraint(array, pltpu.HBM) for array in arrays]
+
+
+LIMIT = pltpu.CompilerParams(vmem_limit_bytes=8 * 1024 * 1024)
+IN_HBM = pl.BlockSpec(memory_space=pltpu.HBM)
+
+
+def load_kernel(*refs):
+    count = len(refs) // 2
+    sources, targets, sems = refs[:count], refs[count : 2 * count], refs[-1]
+    copies = [
+        pltpu.make_async_copy(source, target, sems.at[index])
+        for index, (source, target) in enumerate(zip(sources, targets))
+    ]
+    for copy in copies:
+        copy.start()
+    for copy in copies:
+        copy.wait()
+
+
+def project_kernel(own, other, gain, wq, wf, wi, wg, out, rows_scr):
+    kv, core = lax.axis_index(KV), lax.axis_index("tp")
     rows = own.shape[0]
     pair = jnp.concatenate([own[...].astype(f32), other[...].astype(f32)], axis=1)
     block = jnp.where(core == 0, pair, half_turn(pair))
@@ -92,8 +114,8 @@
         gated[peer] = value
 
 
-def mix_kernel(where, every, tokens, weight, out, rows_scr, whole_scr):
-    core = where[1]
+def mix_kernel(every, tokens, weight, out, rows_scr, whole_scr):
+    core = lax.axis_index("tp")
     rows = tokens.shape[0]
     peers, heads, _ = every.shape
     per_row = peers * heads // rows
@@ -111,8 +133,10 @@
         out[peer] = packed
 
 
-def feed_kernel(where, own, other, gain, w_gate, w_up, w_down, mine, theirs, scr):
-    core = where[1]
+def feed_kernel(own, other, gain, w_gate, w_up, w_down_hbm, mine, theirs, scr, w_down, sem):
+    fetch = pltpu.make_async_copy(w_down_hbm, w_down, sem)
+    fetch.start()
+    core = lax.axis_index("tp")
     blocks, half, _ = own.shape
     rows = 2 * half
     mask = lanes_below(core, (half, LANES))
@@ -130,6 +154,7 @@
     gate = scale * lax.dot_general(normed, w_gate[...], NT, preferred_element_type=f32)
     up = scale * lax.dot_general(normed, w_up[...], NT, preferred_element_type=f32)
     hidden = (jax.nn.silu(gate) * up).astype(bf16)
+    fetch.wait()
     terms = jnp.dot(hidden, w_down[...], preferred_element_type=f32)
     for block in range(blocks):
         term = terms[:, block * LANES : (block + 1) * LANES]
@@ -142,8 +167,8 @@
     out[...] = (mine[...] + theirs[...].astype(f32)).astype(bf16)
 
 
-def finish_kernel(where, pieces, mixed, out):
-    core = where[1]
+def finish_kernel(pieces, mixed, out):
+    core = lax.axis_index("tp")
     half = mixed.shape[1]
     total = mixed[0].astype(f32) + jnp.sum(pieces[...].astype(f32), axis=0)
     total = jnp.where(core == 0, total, half_turn(total))
@@ -168,24 +193,47 @@
     w_down,
 ):
     kv_count = lax.axis_size(KV)
-    where = jnp.stack([lax.axis_index(KV), lax.axis_index("tp")]).astype(jnp.int32)
     rows, cols = tokens.shape
     width = norm_gain.shape[0]
     heads = rec_state.shape[1]
     half = rows // 2
     blocks = width // LANES
-    shape = jax.ShapeDtypeStruct
+    shape = pltpu.VMEM
     piece_rows = 5 * heads
 
     other = lax.ppermute(tokens, "tp", SWAP)
+    loads = (
+        tokens,
+        norm_gain.reshape(blocks, LANES),
+        lower_bound.reshape(heads, LANES),
+        head_gain.reshape(heads, LANES),
+        mixer_gain.reshape(blocks, LANES),
+        w_heads_out.T,
+        w_query,
+        w_forget,
+        w_input,
+        w_outgate,
+    )
+    tokens_here, first_gain, bound, gain, second_gain, heads_out, *projections = pl.pallas_call(
+        load_kernel,
+        out_shape=tuple(shape(x.shape, x.dtype) for x in loads),
+        in_specs=[IN_HBM] * len(loads),
+        out_specs=tuple(in_vmem(len(loads))),
+        scratch_shapes=[pltpu.SemaphoreType.DMA((len(loads),))],
+        compiler_params=LIMIT,
+        name="load",
+    )(*far(*loads))
     pieces = pl.pallas_call(
         project_kernel,
         out_shape=shape((rows, piece_rows, LANES), bf16),
-        in_specs=[IN_SMEM] + in_vmem(7),
+        in_specs=in_vmem(7),
         out_specs=in_vmem(1)[0],
         scratch_shapes=[pltpu.VMEM((rows * piece_rows, LANES), f32)],
+        compiler_params=LIMIT,
         name="project",
-    )(where, tokens, other, norm_gain.reshape(blocks, LANES), w_query, w_forget, w_input, w_outgate)
+    )(
+        *held(tokens_here, other, first_gain, *projections)
+    )
     pieces = exchanged(pieces, KV)
 
     per_head = shape((heads, LANES), f32)
@@ -194,49 +242,60 @@
         out_shape=(shape((2 * kv_count, heads, LANES), bf16), per_head, per_head),
         in_specs=in_vmem(4),
         out_specs=tuple(in_vmem(3)),
+        compiler_params=LIMIT,
         name="recur",
-    )(pieces, rec_state[0], lower_bound.reshape(heads, LANES), head_gain.reshape(heads, LANES))
+    )(*held(pieces, rec_state[0], bound, gain))
     new_state = forget[:, :, None] * rec_state[0] + (1.0 - forget)[:, :, None] * value_in[:, None, :]
 
     every = exchanged(gated, KV_TP)
     mixed = pl.pallas_call(
         mix_kernel,
         out_shape=shape((kv_count, half, LANES), bf16),
-        in_specs=[IN_SMEM] + in_vmem(3),
+        in_specs=in_vmem(3),
         out_specs=in_vmem(1)[0],
         scratch_shapes=[
             pltpu.VMEM((2 * kv_count * heads, LANES), f32),
             pltpu.VMEM((rows, 2 * heads * LANES), bf16),
         ],
+        compiler_params=LIMIT,
         name="mix",
-    )(where, every, tokens, w_heads_out.T)
+    )(*held(every, tokens_here, heads_out))
 
     own = exchanged(mixed, KV)
     other = lax.ppermute(own, "tp", SWAP)
     mine, theirs = pl.pallas_call(
         feed_kernel,
         out_shape=(shape((kv_count, half, LANES), f32), shape((kv_count, half, LANES), bf16)),
-        in_specs=[IN_SMEM] + in_vmem(6),
+        in_specs=in_vmem(5) + [IN_HBM],
         out_specs=tuple(in_vmem(2)),
-        scratch_shapes=[pltpu.VMEM((rows, width), bf16)],
+        scratch_shapes=[
+            pltpu.VMEM((rows, width), bf16),
+            pltpu.VMEM(w_down.shape, bf16),
+            pltpu.SemaphoreType.DMA,
+        ],
+        compiler_params=LIMIT,
         name="feed",
-    )(where, own, other, mixer_gain.reshape(blocks, LANES), w_gate.T, w_up.T, w_down)
+    )(
+        *held(own, other, second_gain, w_gate.T, w_up.T), *far(w_down)
+    )
     theirs = lax.ppermute(theirs, "tp", SWAP)
     chip_sum = pl.pallas_call(
         sum_kernel,
         out_shape=shape((kv_count, half, LANES), bf16),
         in_specs=in_vmem(2),
         out_specs=in_vmem(1)[0],
+        compiler_params=LIMIT,
         name="chip_sum",
-    )(mine, theirs)
+    )(*held(mine, theirs))
     down = exchanged(chip_sum, KV)
     result = pl.pallas_call(
         finish_kernel,
-        out_shape=shape((rows, cols), bf16),
-        in_specs=[IN_SMEM] + in_vmem(2),
+        out_shape=jax.ShapeDtypeStruct((rows, cols), bf16),
+        in_specs=in_vmem(2),
         out_specs=in_vmem(1)[0],
+        compiler_params=LIMIT,
         name="finish",
-    )(where, down, mixed)
+    )(*held(down, mixed))
     return (result, new_state[None])
 
 

time: 95.4 us -> 81.7 us (0.86)
  Pallas kernels: 14.9 us -> 7.02 us
  local copies, waits for them, and re-layouts: 2.56 us -> 0.02 us
  blocking collectives: 57.6 us -> 55.8 us
    unnamed x16 -> x6, local copies, waits for them, and re-layouts: 2.56 us -> 0.02 us
    pallas_call x1, Pallas kernels: 2.39 us -> 0.43 us  [local(): pl.pallas_call(project_kernel, out_shape=shape((rows, piece_rows, LANES),...]
    pallas_call x1, Pallas kernels: 4.6 us -> 2.68 us  [local(): pl.pallas_call(feed_kernel, out_shape=(shape((kv_count, half, LANES), f32...]
    pallas_call x1, Pallas kernels: 2.37 us -> 0.57 us  [local(): pl.pallas_call(lambda *refs: recur_kernel(*refs, width), out_shape=(shape...]
    all_to_all x3, blocking collectives: 57.6 us -> 55.8 us  [exchanged(): return lax.all_to_all(pieces, axis, split_axis=0, concat_axis=0, tiled=True)]
    pallas_call x1, Pallas kernels: 2.09 us -> 0.4 us  [local(): pl.pallas_call(mix_kernel, out_shape=shape((kv_count, half, LANES), bf16)...]
    pallas_call x1, Pallas kernels: 1.66 us -> 0.67 us  [local(): pl.pallas_call(sum_kernel, out_shape=shape((kv_count, half, LANES), bf16)...]
    pallas_call x1 -> x2, Pallas kernels: 1.75 us -> 2.27 us  [the longest x1 1.5 us: local(): pl.pallas_call(load_kernel, out_shape=tuple((shape(x.shape, x.dtype) for...]
  transfers between devices with their start and end apart: 4 -> 4, of which waited for: 4 -> 3; matrix products, arithmetic and copies ran while one was open for 2% -> 1% of each run, Pallas kernels for 0% -> 2%
where the time goes in v3:
time: 81.7 us; the launch traced here: 81.4 us
  blocking collectives  55.8 us (68%)
  waiting for transfers between devices  12.5 us (15%)
  Pallas kernels  7.02 us (9%)
  starting transfers between devices  4.18 us (5%)
  other arithmetic  1.14 us (1%)
    all_to_all x3, blocking collectives, exchanged(): return lax.all_to_all(pieces, axis, split_axis=0, concat_axis=0, tiled=True)  55.8 us
    all_to_all x1, waiting for transfers between devices, exchanged(): return lax.all_to_all(pieces, axis, split_axis=0, concat_axis=0, tiled=True)  9.99 us
    all_to_all x1, starting transfers between devices, exchanged(): return lax.all_to_all(pieces, axis, split_axis=0, concat_axis=0, tiled=True)  3.85 us
    pallas_call x1, Pallas kernels, local(): pl.pallas_call(feed_kernel, out_shape=(shape((kv_count, half, LANES), f32...  2.68 us
  transfers between devices with their start and end apart: 4, of which 3 were waited for; matrix products, arithmetic and copies ran while one was open for 1% of the time, Pallas kernels for 2%

profile of v3, /device:TPU:6, one launch (start us, length us, event | category | flops | bytes accessed | tf_op | source)
XLA Modules:
  0.0 81.4 jit_solution(8526686625072590419)
XLA Ops:
  0.6 0.1 collective-permute-start
  0.7 0.0 copy-start
  0.7 1.5 %load.1 = (bf16[32,64]{1,0:T(8,128)(2,1)S(1)}, f32[32,128]{1,0:T(8,128)S(1)}, f32[8,128]{1,0:T(8,128)S(1)}, f32[8,128]{1,0:T(8,128)S(1)}, f32[32,128]{1,0:T(8,12...) custom-call(bf16[32,64]{1,0:T(8,128)(2,1)} %refs_0_.1, ...), custom_call_target="tpu_custom_call" | custom-call | tf_op jit(solution)/shard_map/load/pallas_call | solution.py:217
  2.2 0.0 collective-permute-done.other
  2.3 0.0 copy-start.2
  2.3 0.4 project.1
  2.7 0.0 copy-start.1
  2.7 26.2 %all_to_all.20.refs_0_ = bf16[32,40,128]{2,1,0:T(8,128)(2,1)S(1)} all-to-all(bf16[32,40,128]{2,1,0:T(8,128)(2,1)S(1)} %project.1), channel_id=1, replica_groups=mesh['dp'=4,'kv_0'=8,'kv_1'=4,'tp'=2] {'kv_0','kv_1'}, dimensions={0} | all-to-all | bytes 655360 | tf_op jit(solution)/shard_map/all_to_all | solution.py:21
  28.9 0.0 copy-done
  28.9 0.6 recur.1
  29.5 15.5 %all_to_all.21.every = bf16[64,8,128]{2,1,0:T(8,128)(2,1)S(1)} all-to-all(bf16[64,8,128]{2,1,0:T(8,128)(2,1)S(1)} %get-tuple-element.25), channel_id=1, replica_groups=mesh['dp'=4,'kv_0'=8,'kv_1'=4,'tp'=2] {'kv_0','kv_1','tp'}, dimensions={0} | all-to-all | bytes 262144 | tf_op jit(solution)/shard_map/all_to_all | solution.py:21
  45.0 0.4 mix.1.mixed
  45.4 14.1 %all_to_all.22.own = bf16[32,16,128]{2,1,0:T(8,128)(2,1)S(1)} all-to-all(bf16[32,16,128]{2,1,0:T(8,128)(2,1)S(1)} %mix.1.mixed), channel_id=1, replica_groups=mesh['dp'=4,'kv_0'=8,'kv_1'=4,'tp'=2] {'kv_0','kv_1'}, dimensions={0} | all-to-all | bytes 262144 | tf_op jit(solution)/shard_map/all_to_all | solution.py:21
  59.5 0.0 collective-permute-start.1
  59.5 1.3 %collective-permute-done.1.other = bf16[32,16,128]{2,1,0:T(8,128)(2,1)S(1)} collective-permute-done((bf16[32,16,128]{2,1,0:T(8,128)(2,1)S(1)}, bf16[32,16,128]{2,1,0:T(8,128)(2,1)S(1)}, u32[]{:S(2)}, u32[]{:S(2)}) %collective-permute-start.1) | collective-permute-done | bytes 131104 | tf_op jit(solution)/shard_map/ppermute | solution.py:265
  60.8 0.0 copy-done.2
  60.8 2.7 %feed.1 = (f32[32,16,128]{2,1,0:T(8,128)S(1)}, bf16[32,16,128]{2,1,0:T(8,128)(2,1)S(1)}) custom-call(bf16[32,16,128]{2,1,0:T(8,128)(2,1)S(1)} %all_to_all.22.own, bf16[32,16,128]{2,1,0:T(8,128)(2,1)S(1)} %collective-permute-done.1.other, f32[32,128]{1,0:T(8,128)S(1)} %get-tuple-element.27.gain, bf16[176,4096]{1,0:T(8,128)(2,1)S(1)} %bitcast.9, ...), custom_call_target="tpu_custom_call" | custom-call | tf_op jit(solution)/shard_map/feed/pallas_call | solution.py:266
  63.5 0.2 collective-permute-start.2
  63.8 1.2 %collective-permute-done.2.theirs = bf16[32,16,128]{2,1,0:T(8,128)(2,1)S(1)} collective-permute-done((bf16[32,16,128]{2,1,0:T(8,128)(2,1)S(1)}, bf16[32,16,128]{2,1,0:T(8,128)(2,1)S(1)}, u32[]{:S(2)}, u32[]{:S(2)}) %collective-permute-start.2) | collective-permute-done | bytes 131104 | tf_op jit(solution)/shard_map/ppermute | solution.py:281
  65.0 0.7 chip_sum.1
  65.6 3.8 %all-to-all-start.3 = ((bf16[32,16,128]{2,1,0:T(8,128)(2,1)}), bf16[32,16,128]{2,1,0:T(8,128)(2,1)S(1)}, u32[]{:S(2)}, u32[]{:S(2)}) async-start(bf16[32,16,128]{2,1,0:T(8,128)(2,1)} %chip_sum.1), calls=%async_computation.3 | async-start | bytes 262144 | tf_op jit(solution)/shard_map/all_to_all | solution.py:21
  69.5 1.1 %multiply_add_fusion = f32[1,8,128,128]{3,2,1,0:T(8,128)} fusion(f32[1,8,128,128]{3,2,1,0:T(8,128)S(1)} %copy-done, f32[8,128]{1,0:T(8,128)S(1)} %get-tuple-element.31, f32[8,128]{1,0:T(8,128)S(1)} %broadcast_subtract_fusion, f32[8,128]{1,0:T(8,128)S(1)} %get-tuple-element.30), kind=kLoop, calls=%fused_computation | loop fusion | flops 393216 | bytes 1060864 | tf_op jit(solution)/shard_map/add | solution.py:248
  70.6 10.0 %all-to-all-done.3.pieces = bf16[32,16,128]{2,1,0:T(8,128)(2,1)S(1)} async-done(((bf16[32,16,128]{2,1,0:T(8,128)(2,1)}), bf16[32,16,128]{2,1,0:T(8,128)(2,1)S(1)}, u32[]{:S(2)}, u32[]{:S(2)}) %all-to-all-start.3) | async-done | bytes 131104 | tf_op jit(solution)/shard_map/all_to_all | solution.py:21
  80.6 0.8 finish.1
  (2 shorter events, 0.0 us)
Async XLA Ops:
  0.6 1.6 %collective-permute-start = (bf16[32,64]{1,0:T(8,128)(2,1)}, bf16[32,64]{1,0:T(8,128)(2,1)S(1)}, u32[]{:S(2)}, u32[]{:S(2)}) collective-permute-start(bf16[32,64]{1,0:T(8,128)(2,1)} %refs_0_.1), channel_id=1, source_target_pairs={{0,1},{1,0},{2,3},{3,2},{4,5},{5,4},{6,7},{7,6},{8,9},{9,8},{10,11... | collective-permute-start | bytes 12296 | tf_op jit(solution)/shard_map/ppermute | solution.py:204
  0.7 28.2 %copy-start = (f32[1,8,128,128]{3,2,1,0:T(8,128)S(1)}, f32[1,8,128,128]{3,2,1,0:T(8,128)}, u32[]{:S(2)}) copy-start(f32[1,8,128,128]{3,2,1,0:T(8,128)} %param.15) | copy-start | bytes 1572868
  2.3 58.6 %copy-start.2 = (bf16[4096,176]{0,1:T(8,128)(2,1)S(1)}, bf16[4096,176]{0,1:T(8,128)(2,1)}, u32[]{:S(2)}) copy-start(bf16[4096,176]{0,1:T(8,128)(2,1)} %param.26) | copy-start | bytes 4325380
  2.7 58.1 %copy-start.1 = (bf16[4096,176]{0,1:T(8,128)(2,1)S(1)}, bf16[4096,176]{0,1:T(8,128)(2,1)}, u32[]{:S(2)}) copy-start(bf16[4096,176]{0,1:T(8,128)(2,1)} %param.25) | copy-start | bytes 4325380
  59.5 1.3 %collective-permute-start.1 = (bf16[32,16,128]{2,1,0:T(8,128)(2,1)S(1)}, bf16[32,16,128]{2,1,0:T(8,128)(2,1)S(1)}, u32[]{:S(2)}, u32[]{:S(2)}) collective-permute-start(bf16[32,16,128]{2,1,0:T(8,128)(2,1)S(1)} %all_to_all.22.own), channel_id=1, source_target_pairs={{0,1},{1,0},{2,3},{3,2},{4,5},{5,4},{6,7},{7,6},{8,9},{9,8},{10,11... | collective-permute-start | bytes 393224 | tf_op jit(solution)/shard_map/ppermute | solution.py:265
  63.5 1.4 %collective-permute-start.2 = (bf16[32,16,128]{2,1,0:T(8,128)(2,1)S(1)}, bf16[32,16,128]{2,1,0:T(8,128)(2,1)S(1)}, u32[]{:S(2)}, u32[]{:S(2)}) collective-permute-start(bf16[32,16,128]{2,1,0:T(8,128)(2,1)S(1)} %get-tuple-element.29), channel_id=1, source_target_pairs={{0,1},{1,0},{2,3},{3,2},{4,5},{5,4},{6,7},{7,6},{8,9},{9,8},{10,11... | collective-permute-start | bytes 393224 | tf_op jit(solution)/shard_map/ppermute | solution.py:281
  65.6 15.0 %all-to-all-start.3 = ((bf16[32,16,128]{2,1,0:T(8,128)(2,1)}), bf16[32,16,128]{2,1,0:T(8,128)(2,1)S(1)}, u32[]{:S(2)}, u32[]{:S(2)}) async-start(bf16[32,16,128]{2,1,0:T(8,128)(2,1)} %chip_sum.1), calls=%async_computation.3 | async-start | bytes 262144 | tf_op jit(solution)/shard_map/all_to_all | solution.py:21

commit v4 on v3

--- a/solution.py
+++ b/solution.py
@@ -83,7 +83,7 @@
         out[row] = rows_scr[pl.ds(row * step, step), :].astype(bf16)
 
 
-def recur_kernel(pieces, state, bound, gain, gated, forget_out, value_out, width):
+def recur_kernel(pieces, state, bound, gain, gated, new_state, width):
     heads = state.shape[0]
     total = jnp.sum(pieces[...].astype(f32), axis=0)
     squares = total[4 * heads : 4 * heads + 1, 0:1] + total[4 * heads : 4 * heads + 1, 1:2]
@@ -92,20 +92,15 @@
         row_scale * total[i * heads : (i + 1) * heads] for i in range(4)
     ]
     forget = bound[...] + (1.0 - bound[...]) * jax.nn.sigmoid(forget_pre)
-    key_in = 1.0 - forget
-    query_act = jax.nn.silu(query_pre)
-    forget_out[...] = forget
-    value_out[...] = value_in
-    fresh = jnp.sum(query_act * key_in, axis=1, keepdims=True) * value_in
-    reads = jnp.transpose(query_act * forget)
-    kept = jnp.concatenate(
-        [
-            jnp.sum(reads[:, head : head + 1] * state[head], axis=0, keepdims=True)
-            for head in range(heads)
-        ],
-        axis=0,
-    )
-    head_out = kept + fresh
+    forget_down = jnp.transpose(forget)
+    query_down = jnp.transpose(jax.nn.silu(query_pre))
+    reads = []
+    for head in range(heads):
+        keep = jnp.broadcast_to(forget_down[:, head : head + 1], state.shape[1:])
+        fresh = keep * state[head] + (1.0 - keep) * value_in[head : head + 1]
+        new_state[head] = fresh
+        reads.append(jnp.sum(query_down[:, head : head + 1] * fresh, axis=0, keepdims=True))
+    head_out = jnp.concatenate(reads, axis=0)
     head_out = head_out * lax.rsqrt(
         jnp.mean(head_out * head_out, axis=1, keepdims=True) + epsilon
     )
@@ -114,16 +109,19 @@
         gated[peer] = value
 
 
-def mix_kernel(every, tokens, weight, out, rows_scr, whole_scr):
+def mix_kernel(own, other, tokens, weight, out, rows_scr, whole_scr):
     core = lax.axis_index("tp")
     rows = tokens.shape[0]
-    peers, heads, _ = every.shape
-    per_row = peers * heads // rows
-    rows_scr[...] = every[...].astype(f32).reshape(peers * heads, LANES)
-    for head in range(per_row):
-        whole_scr[:, head * LANES : (head + 1) * LANES] = rows_scr[
-            pl.ds(head, rows, stride=per_row), :
-        ].astype(bf16)
+    heads = own.shape[1]
+    rows_scr[0] = own[...].astype(f32).reshape(rows * heads, LANES)
+    rows_scr[1] = other[...].astype(f32).reshape(rows * heads, LANES)
+    for side in range(2):
+        source = (core + side) % 2
+        for head in range(heads):
+            column = (side * heads + head) * LANES
+            whole_scr[:, column : column + LANES] = rows_scr[
+                source, pl.ds(head, rows, stride=heads), :
+            ].astype(bf16)
     added = lax.dot_general(whole_scr[...], weight[...], NT, preferred_element_type=f32)
     mixed = tokens[...].astype(f32) + added
     half = rows // 2
@@ -133,9 +131,13 @@
         out[peer] = packed
 
 
-def feed_kernel(own, other, gain, w_gate, w_up, w_down_hbm, mine, theirs, scr, w_down, sem):
-    fetch = pltpu.make_async_copy(w_down_hbm, w_down, sem)
+def feed_kernel(
+    own, other, gain, w_gate, w_up, state, w_down_hbm, mine, theirs, state_hbm, scr, w_down, sems
+):
+    fetch = pltpu.make_async_copy(w_down_hbm, w_down, sems.at[0])
     fetch.start()
+    store = pltpu.make_async_copy(state, state_hbm, sems.at[1])
+    store.start()
     core = lax.axis_index("tp")
     blocks, half, _ = own.shape
     rows = 2 * half
@@ -161,6 +163,7 @@
         top, bottom = term[:half], half_turn(term[half:])
         mine[block] = jnp.where(mask, top, bottom)
         theirs[block] = jnp.where(mask, bottom, top).astype(bf16)
+    store.wait()
 
 
 def sum_kernel(mine, theirs, out):
@@ -236,47 +239,50 @@
     )
     pieces = exchanged(pieces, KV)
 
-    per_head = shape((heads, LANES), f32)
-    gated, forget, value_in = pl.pallas_call(
+    gated, new_state = pl.pallas_call(
         lambda *refs: recur_kernel(*refs, width),
-        out_shape=(shape((2 * kv_count, heads, LANES), bf16), per_head, per_head),
+        out_shape=(shape((kv_count, heads, LANES), bf16), shape(rec_state.shape[1:], f32)),
         in_specs=in_vmem(4),
-        out_specs=tuple(in_vmem(3)),
+        out_specs=tuple(in_vmem(2)),
         compiler_params=LIMIT,
         name="recur",
     )(*held(pieces, rec_state[0], bound, gain))
-    new_state = forget[:, :, None] * rec_state[0] + (1.0 - forget)[:, :, None] * value_in[:, None, :]
-
-    every = exchanged(gated, KV_TP)
+
+    own = exchanged(gated, KV)
+    other = lax.ppermute(own, "tp", SWAP)
     mixed = pl.pallas_call(
         mix_kernel,
         out_shape=shape((kv_count, half, LANES), bf16),
-        in_specs=in_vmem(3),
+        in_specs=in_vmem(4),
         out_specs=in_vmem(1)[0],
         scratch_shapes=[
-            pltpu.VMEM((2 * kv_count * heads, LANES), f32),
+            pltpu.VMEM((2, rows * heads, LANES), f32),
             pltpu.VMEM((rows, 2 * heads * LANES), bf16),
         ],
         compiler_params=LIMIT,
         name="mix",
-    )(*held(every, tokens_here, heads_out))
+    )(*held(own, other, tokens_here, heads_out))
 
     own = exchanged(mixed, KV)
     other = lax.ppermute(own, "tp", SWAP)
-    mine, theirs = pl.pallas_call(
+    mine, theirs, new_state = pl.pallas_call(
         feed_kernel,
-        out_shape=(shape((kv_count, half, LANES), f32), shape((kv_count, half, LANES), bf16)),
-        in_specs=in_vmem(5) + [IN_HBM],
-        out_specs=tuple(in_vmem(2)),
+        out_shape=(
+            shape((kv_count, half, LANES), f32),
+            shape((kv_count, half, LANES), bf16),
+            pltpu.HBM(new_state.shape, f32),
+        ),
+        in_specs=in_vmem(6) + [IN_HBM],
+        out_specs=tuple(in_vmem(2) + [IN_HBM]),
         scratch_shapes=[
             pltpu.VMEM((rows, width), bf16),
             pltpu.VMEM(w_down.shape, bf16),
-            pltpu.SemaphoreType.DMA,
+            pltpu.SemaphoreType.DMA((2,)),
         ],
         compiler_params=LIMIT,
         name="feed",
     )(
-        *held(own, other, second_gain, w_gate.T, w_up.T), *far(w_down)
+        *held(own, other, second_gain, w_gate.T, w_up.T, new_state), *far(w_down)
     )
     theirs = lax.ppermute(theirs, "tp", SWAP)
     chip_sum = pl.pallas_call(

time: 81.7 us -> 80.2 us (0.982)
  blocking collectives: 55.8 us -> 68.3 us
  waiting for transfers between devices: 12.5 us -> 3.8 us
  starting transfers between devices: 4.18 us -> 0.33 us
  other arithmetic: 1.14 us -> 0 us
    all_to_all x3 -> x4, blocking collectives: 55.8 us -> 68.3 us  [exchanged(): return lax.all_to_all(pieces, axis, split_axis=0, concat_axis=0, tiled=True)]
    all_to_all x1 -> x0, waiting for transfers between devices: 9.99 us -> none  [exchanged(): return lax.all_to_all(pieces, axis, split_axis=0, concat_axis=0, tiled=True)]
    all_to_all x1 -> x0, starting transfers between devices: 3.85 us -> none  [exchanged(): return lax.all_to_all(pieces, axis, split_axis=0, concat_axis=0, tiled=True)]
    ppermute x1 -> x2, waiting for transfers between devices: 1.35 us -> 2.6 us  [local(): other = lax.ppermute(own, 'tp', SWAP)]
    add x1 -> x0, other arithmetic: 1.13 us -> none  [local(): forget[:, :, None] * rec_state[0]]
  transfers between devices with their start and end apart: 4 -> 4, of which waited for: 3 -> 3; matrix products, arithmetic and copies ran while one was open for 1% -> 0% of each run, Pallas kernels for 2% -> 2%
where the time goes in v4:
time: 80.2 us; the launch traced here: 79.9 us
  blocking collectives  68.3 us (85%)
  Pallas kernels  6.73 us (8%)
  waiting for transfers between devices  3.8 us (5%)
    all_to_all x4, blocking collectives, exchanged(): return lax.all_to_all(pieces, axis, split_axis=0, concat_axis=0, tiled=True)  68.3 us
    pallas_call x1, Pallas kernels, local(): pl.pallas_call(feed_kernel, out_shape=(shape((kv_count, half, LANES), f32...  2.88 us
    ppermute x2, waiting for transfers between devices, local(): other = lax.ppermute(own, 'tp', SWAP)  2.6 us
  transfers between devices with their start and end apart: 4, of which 3 were waited for; matrix products, arithmetic and copies ran while one was open for 0% of the time, Pallas kernels for 2%

profile of v4, /device:TPU:6, one launch (start us, length us, event | category | flops | bytes accessed | tf_op | source)
XLA Modules:
  0.0 79.9 jit_solution(15899110127724388462)
XLA Ops:
  0.6 0.1 collective-permute-start
  0.7 0.0 copy-start.2
  0.7 1.5 %load.1 = (bf16[32,64]{1,0:T(8,128)(2,1)S(1)}, f32[32,128]{1,0:T(8,128)S(1)}, f32[8,128]{1,0:T(8,128)S(1)}, f32[8,128]{1,0:T(8,128)S(1)}, f32[32,128]{1,0:T(8,12...) custom-call(bf16[32,64]{1,0:T(8,128)(2,1)} %refs_0_.1, ...), custom_call_target="tpu_custom_call" | custom-call | tf_op jit(solution)/shard_map/load/pallas_call | solution.py:220
  2.2 0.0 collective-permute-done.other
  2.3 0.0 copy-start.1
  2.3 0.4 project.1
  2.7 0.0 copy-start
  2.7 26.2 %all_to_all.20.refs_0_ = bf16[32,40,128]{2,1,0:T(8,128)(2,1)S(1)} all-to-all(bf16[32,40,128]{2,1,0:T(8,128)(2,1)S(1)} %project.1), channel_id=1, replica_groups=mesh['dp'=4,'kv_0'=8,'kv_1'=4,'tp'=2] {'kv_0','kv_1'}, dimensions={0} | all-to-all | bytes 655360 | tf_op jit(solution)/shard_map/all_to_all | solution.py:21
  28.9 0.0 copy-done.2
  28.9 0.7 recur.1
  29.7 13.8 %all_to_all.21.own = bf16[32,8,128]{2,1,0:T(8,128)(2,1)S(1)} all-to-all(bf16[32,8,128]{2,1,0:T(8,128)(2,1)S(1)} %get-tuple-element.25), channel_id=1, replica_groups=mesh['dp'=4,'kv_0'=8,'kv_1'=4,'tp'=2] {'kv_0','kv_1'}, dimensions={0} | all-to-all | bytes 131072 | tf_op jit(solution)/shard_map/all_to_all | solution.py:21
  43.5 0.0 collective-permute-start.1
  43.5 1.3 %collective-permute-done.1.other = bf16[32,8,128]{2,1,0:T(8,128)(2,1)S(1)} collective-permute-done((bf16[32,8,128]{2,1,0:T(8,128)(2,1)S(1)}, bf16[32,8,128]{2,1,0:T(8,128)(2,1)S(1)}, u32[]{:S(2)}, u32[]{:S(2)}) %collective-permute-start.1) | collective-permute-done | bytes 65568 | tf_op jit(solution)/shard_map/ppermute | solution.py:252
  44.7 0.4 mix.1.mixed
  45.1 14.1 %all_to_all.22.own = bf16[32,16,128]{2,1,0:T(8,128)(2,1)S(1)} all-to-all(bf16[32,16,128]{2,1,0:T(8,128)(2,1)S(1)} %mix.1.mixed), channel_id=1, replica_groups=mesh['dp'=4,'kv_0'=8,'kv_1'=4,'tp'=2] {'kv_0','kv_1'}, dimensions={0} | all-to-all | bytes 262144 | tf_op jit(solution)/shard_map/all_to_all | solution.py:21
  59.3 0.0 collective-permute-start.2
  59.3 1.3 %collective-permute-done.2.other = bf16[32,16,128]{2,1,0:T(8,128)(2,1)S(1)} collective-permute-done((bf16[32,16,128]{2,1,0:T(8,128)(2,1)S(1)}, bf16[32,16,128]{2,1,0:T(8,128)(2,1)S(1)}, u32[]{:S(2)}, u32[]{:S(2)}) %collective-permute-start.2) | collective-permute-done | bytes 131104 | tf_op jit(solution)/shard_map/ppermute | solution.py:267
  60.6 0.0 copy-done.1
  60.6 0.0 copy-done
  60.6 2.9 %feed.1 = (f32[32,16,128]{2,1,0:T(8,128)S(1)}, bf16[32,16,128]{2,1,0:T(8,128)(2,1)S(1)}, f32[8,128,128]{2,1,0:T(8,128)}) custom-call(bf16[32,16,128]{2,1,0:T(8,128)(2,1)S(1)} %all_to_all.22.own, bf16[32,16,128]{2,1,0:T(8,128)(2,1)S(1)} %collective-permute-done.2.other, f32[32,128]{1,0:T(8,128)S(1)} %get-tuple-element.27.gain, bf16[176,4096]{1,0:T(8,128)(2,1)S(1)} %bitcast.9, ...), custom_call_target="tpu_custom_call" | custom-call | tf_op jit(solution)/shard_map/feed/pallas_call | solution.py:268
  63.5 0.2 collective-permute-start.3
  63.7 1.2 %collective-permute-done.3.theirs = bf16[32,16,128]{2,1,0:T(8,128)(2,1)S(1)} collective-permute-done((bf16[32,16,128]{2,1,0:T(8,128)(2,1)S(1)}, bf16[32,16,128]{2,1,0:T(8,128)(2,1)S(1)}, u32[]{:S(2)}, u32[]{:S(2)}) %collective-permute-start.3) | collective-permute-done | bytes 131104 | tf_op jit(solution)/shard_map/ppermute | solution.py:287
  65.0 14.1 %all_to_all.23.pieces = bf16[32,16,128]{2,1,0:T(8,128)(2,1)S(1)} all-to-all(bf16[32,16,128]{2,1,0:T(8,128)(2,1)S(1)} %chip_sum.1), channel_id=1, replica_groups=mesh['dp'=4,'kv_0'=8,'kv_1'=4,'tp'=2] {'kv_0','kv_1'}, dimensions={0} | all-to-all | bytes 262144 | tf_op jit(solution)/shard_map/all_to_all | solution.py:21
  79.1 0.8 finish.1
  (1 shorter events, 0.0 us)
Async XLA Ops:
  0.6 1.6 %collective-permute-start = (bf16[32,64]{1,0:T(8,128)(2,1)}, bf16[32,64]{1,0:T(8,128)(2,1)S(1)}, u32[]{:S(2)}, u32[]{:S(2)}) collective-permute-start(bf16[32,64]{1,0:T(8,128)(2,1)} %refs_0_.1), channel_id=1, source_target_pairs={{0,1},{1,0},{2,3},{3,2},{4,5},{5,4},{6,7},{7,6},{8,9},{9,8},{10,11... | collective-permute-start | bytes 12296 | tf_op jit(solution)/shard_map/ppermute | solution.py:207
  0.7 28.2 %copy-start.2 = (f32[1,8,128,128]{3,2,1,0:T(8,128)S(1)}, f32[1,8,128,128]{3,2,1,0:T(8,128)}, u32[]{:S(2)}) copy-start(f32[1,8,128,128]{3,2,1,0:T(8,128)} %param.15) | copy-start | bytes 1572868
  2.3 58.3 %copy-start.1 = (bf16[4096,176]{0,1:T(8,128)(2,1)S(1)}, bf16[4096,176]{0,1:T(8,128)(2,1)}, u32[]{:S(2)}) copy-start(bf16[4096,176]{0,1:T(8,128)(2,1)} %param.26) | copy-start | bytes 4325380
  2.7 57.9 %copy-start = (bf16[4096,176]{0,1:T(8,128)(2,1)S(1)}, bf16[4096,176]{0,1:T(8,128)(2,1)}, u32[]{:S(2)}) copy-start(bf16[4096,176]{0,1:T(8,128)(2,1)} %param.25) | copy-start | bytes 4325380
  43.5 1.3 %collective-permute-start.1 = (bf16[32,8,128]{2,1,0:T(8,128)(2,1)S(1)}, bf16[32,8,128]{2,1,0:T(8,128)(2,1)S(1)}, u32[]{:S(2)}, u32[]{:S(2)}) collective-permute-start(bf16[32,8,128]{2,1,0:T(8,128)(2,1)S(1)} %all_to_all.21.own), channel_id=1, source_target_pairs={{0,1},{1,0},{2,3},{3,2},{4,5},{5,4},{6,7},{7,6},{8,9},{9,8},{10,11... | collective-permute-start | bytes 196616 | tf_op jit(solution)/shard_map/ppermute | solution.py:252
  59.3 1.3 %collective-permute-start.2 = (bf16[32,16,128]{2,1,0:T(8,128)(2,1)S(1)}, bf16[32,16,128]{2,1,0:T(8,128)(2,1)S(1)}, u32[]{:S(2)}, u32[]{:S(2)}) collective-permute-start(bf16[32,16,128]{2,1,0:T(8,128)(2,1)S(1)} %all_to_all.22.own), channel_id=1, source_target_pairs={{0,1},{1,0},{2,3},{3,2},{4,5},{5,4},{6,7},{7,6},{8,9},{9,8},{10,11... | collective-permute-start | bytes 393224 | tf_op jit(solution)/shard_map/ppermute | solution.py:267
  63.5 1.4 %collective-permute-start.3 = (bf16[32,16,128]{2,1,0:T(8,128)(2,1)S(1)}, bf16[32,16,128]{2,1,0:T(8,128)(2,1)S(1)}, u32[]{:S(2)}, u32[]{:S(2)}) collective-permute-start(bf16[32,16,128]{2,1,0:T(8,128)(2,1)S(1)} %get-tuple-element.30), channel_id=1, source_target_pairs={{0,1},{1,0},{2,3},{3,2},{4,5},{5,4},{6,7},{7,6},{8,9},{9,8},{10,11... | collective-permute-start | bytes 393224 | tf_op jit(solution)/shard_map/ppermute | solution.py:287

commit v5 on v4

--- a/solution.py
+++ b/solution.py
@@ -21,9 +21,8 @@
     return lax.all_to_all(pieces, axis, split_axis=0, concat_axis=0, tiled=True)
 
 
-def lanes_below(core, shape):
-    lane = lax.broadcasted_iota(jnp.int32, shape, len(shape) - 1)
-    return (lane < LANES // 2) == (core == 0)
+def low_lanes(shape):
+    return lax.broadcasted_iota(jnp.int32, shape, len(shape) - 1) < LANES // 2
 
 
 def half_turn(x):
@@ -70,7 +69,7 @@
     extra = jnp.where(lane == 0, high, jnp.where(lane == 1, squares - high, 0.0))
     scaled = (block * gain[pl.ds(kv, 1), :]).astype(bf16)
     heads = wq.shape[1] // LANES
-    step = out.shape[1]
+    step = out.shape[1] * out.shape[2]
     for index, weight in enumerate((wq, wf, wi, wg)):
         part = jnp.dot(scaled, weight[...], preferred_element_type=f32)
         for head in range(heads):
@@ -80,12 +79,14 @@
     for row in range(4 * heads, step):
         rows_scr[pl.ds(row, rows, stride=step), :] = extra
     for row in range(rows):
-        out[row] = rows_scr[pl.ds(row * step, step), :].astype(bf16)
+        piece = rows_scr[pl.ds(row * step, step), :].reshape(out.shape[1:])
+        out[row] = piece.astype(bf16)
 
 
 def recur_kernel(pieces, state, bound, gain, gated, new_state, width):
     heads = state.shape[0]
     total = jnp.sum(pieces[...].astype(f32), axis=0)
+    total = total.reshape(total.shape[0] * total.shape[1], LANES)
     squares = total[4 * heads : 4 * heads + 1, 0:1] + total[4 * heads : 4 * heads + 1, 1:2]
     row_scale = lax.rsqrt(squares / width + epsilon)
     query_pre, forget_pre, value_in, gate_pre = [
@@ -131,39 +132,94 @@
         out[peer] = packed
 
 
-def feed_kernel(
-    own, other, gain, w_gate, w_up, state, w_down_hbm, mine, theirs, state_hbm, scr, w_down, sems
+def part(index):
+    return slice(index * LANES, (index + 1) * LANES)
+
+
+def split_lanes(low, left, right):
+    return jnp.where(low, left, half_turn(right)), jnp.where(low, half_turn(left), right)
+
+
+def arrange_in_kernel(w_gate, w_up, gain, ins, gains):
+    units = w_gate.shape[0]
+    low = low_lanes((units, LANES))
+    for pair in range(w_gate.shape[1] // (2 * LANES)):
+        left, right = part(2 * pair), part(2 * pair + 1)
+        for index, weight in enumerate((w_gate, w_up)):
+            first, second = split_lanes(low, weight[:, left], weight[:, right])
+            ins[0, index * units : (index + 1) * units, part(pair)] = first
+            ins[1, index * units : (index + 1) * units, part(pair)] = second
+        first, second = split_lanes(
+            low[:1], gain[2 * pair : 2 * pair + 1, :], gain[2 * pair + 1 : 2 * pair + 2, :]
+        )
+        gains[0, pair : pair + 1, :] = first
+        gains[1, pair : pair + 1, :] = second
+
+
+def arrange_out_kernel(w_down, outs):
+    low = low_lanes((w_down.shape[0], LANES))
+    for pair in range(w_down.shape[1] // (2 * LANES)):
+        first, second = split_lanes(low, w_down[:, part(2 * pair)], w_down[:, part(2 * pair + 1)])
+        outs[0, :, part(pair)] = first
+        outs[1, :, part(pair)] = second
+
+
+def half_feed(core, chunk, gains, ins, scr):
+    blocks, half, _ = chunk.shape
+    low = low_lanes((half, LANES))
+    squares = jnp.zeros((2 * half, LANES), f32)
+    for pair in range(blocks // 2):
+        first, second = split_lanes(
+            low, chunk[2 * pair].astype(f32), chunk[2 * pair + 1].astype(f32)
+        )
+        value = jnp.concatenate([first, second], axis=0)
+        squares = squares + value * value
+        scr[:, part(pair)] = (value * gains[core, pair : pair + 1, :]).astype(bf16)
+    products = lax.dot_general(scr[...], ins[core], NT, preferred_element_type=f32)
+    return products, squares
+
+
+def own_kernel(chunk, gains, ins, products, squares, scr):
+    products[...], squares[...] = half_feed(lax.axis_index("tp"), chunk, gains, ins, scr)
+
+
+def packed_rows(low, block, turned):
+    half = block.shape[0] // 2
+    first, second = block[:half], block[half:]
+    if turned:
+        first, second = second, first
+    return split_lanes(low, first, second)
+
+
+def other_kernel(
+    chunk, gains, ins, products, squares, outs, state, theirs, hidden_out, state_hbm, scr, sem
 ):
-    fetch = pltpu.make_async_copy(w_down_hbm, w_down, sems.at[0])
-    fetch.start()
-    store = pltpu.make_async_copy(state, state_hbm, sems.at[1])
+    store = pltpu.make_async_copy(state, state_hbm, sem)
     store.start()
     core = lax.axis_index("tp")
-    blocks, half, _ = own.shape
-    rows = 2 * half
-    mask = lanes_below(core, (half, LANES))
-    squares = jnp.zeros((rows, LANES), f32)
-    for block in range(blocks):
-        a, b = own[block].astype(f32), other[block].astype(f32)
-        top = jnp.where(mask, a, b)
-        bottom = half_turn(jnp.where(mask, b, a))
-        value = jnp.concatenate([top, bottom], axis=0)
-        squares = squares + value * value
-        scr[:, block * LANES : (block + 1) * LANES] = (value * gain[pl.ds(block, 1), :]).astype(bf16)
-    mean = jnp.sum(squares, axis=1, keepdims=True) / (blocks * LANES)
-    scale = lax.rsqrt(mean + epsilon)
-    normed = scr[...]
-    gate = scale * lax.dot_general(normed, w_gate[...], NT, preferred_element_type=f32)
-    up = scale * lax.dot_general(normed, w_up[...], NT, preferred_element_type=f32)
-    hidden = (jax.nn.silu(gate) * up).astype(bf16)
-    fetch.wait()
-    terms = jnp.dot(hidden, w_down[...], preferred_element_type=f32)
-    for block in range(blocks):
-        term = terms[:, block * LANES : (block + 1) * LANES]
-        top, bottom = term[:half], half_turn(term[half:])
-        mine[block] = jnp.where(mask, top, bottom)
-        theirs[block] = jnp.where(mask, bottom, top).astype(bf16)
+    half = chunk.shape[1]
+    more, more_squares = half_feed(1 - core, chunk, gains, ins, scr)
+    totals = products[...] + jnp.concatenate([more[half:], more[:half]], axis=0)
+    both = squares[...] + jnp.concatenate([more_squares[half:], more_squares[:half]], axis=0)
+    mean = jnp.sum(both, axis=1, keepdims=True) / (chunk.shape[0] * LANES)
+    totals = totals * lax.rsqrt(mean + epsilon)
+    units = totals.shape[1] // 2
+    hidden = (jax.nn.silu(totals[:, :units]) * totals[:, units:]).astype(bf16)
+    hidden_out[...] = hidden
+    terms = jnp.dot(hidden, outs[1 - core], preferred_element_type=f32)
+    low = low_lanes((half, LANES))
+    for pair in range(chunk.shape[0] // 2):
+        left, right = packed_rows(low, terms[:, part(pair)], True)
+        theirs[2 * pair] = left.astype(bf16)
+        theirs[2 * pair + 1] = right.astype(bf16)
     store.wait()
+
+
+def mine_kernel(hidden, outs, mine):
+    terms = jnp.dot(hidden[...], outs[lax.axis_index("tp")], preferred_element_type=f32)
+    low = low_lanes(mine.shape[1:])
+    for pair in range(mine.shape[0] // 2):
+        mine[2 * pair], mine[2 * pair + 1] = packed_rows(low, terms[:, part(pair)], False)
 
 
 def sum_kernel(mine, theirs, out):
@@ -202,7 +258,7 @@
     half = rows // 2
     blocks = width // LANES
     shape = pltpu.VMEM
-    piece_rows = 5 * heads
+    piece_rows = 4 * heads + 4
 
     other = lax.ppermute(tokens, "tp", SWAP)
     loads = (
@@ -212,30 +268,27 @@
         head_gain.reshape(heads, LANES),
         mixer_gain.reshape(blocks, LANES),
         w_heads_out.T,
-        w_query,
-        w_forget,
-        w_input,
-        w_outgate,
     )
-    tokens_here, first_gain, bound, gain, second_gain, heads_out, *projections = pl.pallas_call(
+    tokens_here, first_gain, bound, gain, second_gain, heads_out = pl.pallas_call(
         load_kernel,
         out_shape=tuple(shape(x.shape, x.dtype) for x in loads),
         in_specs=[IN_HBM] * len(loads),
         out_specs=tuple(in_vmem(len(loads))),
         scratch_shapes=[pltpu.SemaphoreType.DMA((len(loads),))],
         compiler_params=LIMIT,
+        cost_estimate=pl.CostEstimate(flops=4000000000, bytes_accessed=20000000, transcendentals=0),
         name="load",
     )(*far(*loads))
     pieces = pl.pallas_call(
         project_kernel,
-        out_shape=shape((rows, piece_rows, LANES), bf16),
+        out_shape=shape((rows, piece_rows // 4, 4, LANES), bf16),
         in_specs=in_vmem(7),
         out_specs=in_vmem(1)[0],
         scratch_shapes=[pltpu.VMEM((rows * piece_rows, LANES), f32)],
         compiler_params=LIMIT,
         name="project",
     )(
-        *held(tokens_here, other, first_gain, *projections)
+        *held(tokens_here, other, first_gain, w_query, w_forget, w_input, w_outgate)
     )
     pieces = exchanged(pieces, KV)
 
@@ -263,27 +316,60 @@
         name="mix",
     )(*held(own, other, tokens_here, heads_out))
 
+    units = w_gate.shape[1]
+    ins, gains = pl.pallas_call(
+        arrange_in_kernel,
+        out_shape=(
+            shape((2, 2 * units, width // 2), bf16),
+            shape((2, blocks // 2, LANES), f32),
+        ),
+        in_specs=in_vmem(3),
+        out_specs=tuple(in_vmem(2)),
+        compiler_params=LIMIT,
+        name="arrange_in",
+    )(*held(w_gate.T, w_up.T, second_gain))
+    outs = pl.pallas_call(
+        arrange_out_kernel,
+        out_shape=shape((2, units, width // 2), bf16),
+        in_specs=in_vmem(1),
+        out_specs=in_vmem(1)[0],
+        compiler_params=LIMIT,
+        name="arrange_out",
+    )(*held(w_down))
+
     own = exchanged(mixed, KV)
     other = lax.ppermute(own, "tp", SWAP)
-    mine, theirs, new_state = pl.pallas_call(
-        feed_kernel,
+    chunks = (kv_count, half, LANES)
+    products, squares = pl.pallas_call(
+        own_kernel,
+        out_shape=(shape((rows, 2 * units), f32), shape((rows, LANES), f32)),
+        in_specs=in_vmem(3),
+        out_specs=tuple(in_vmem(2)),
+        scratch_shapes=[pltpu.VMEM((rows, width // 2), bf16)],
+        compiler_params=LIMIT,
+        name="own",
+    )(*held(own, gains, ins))
+    theirs, hidden, new_state = pl.pallas_call(
+        other_kernel,
         out_shape=(
-            shape((kv_count, half, LANES), f32),
-            shape((kv_count, half, LANES), bf16),
+            shape(chunks, bf16),
+            shape((rows, units), bf16),
             pltpu.HBM(new_state.shape, f32),
         ),
-        in_specs=in_vmem(6) + [IN_HBM],
+        in_specs=in_vmem(7),
         out_specs=tuple(in_vmem(2) + [IN_HBM]),
-        scratch_shapes=[
-            pltpu.VMEM((rows, width), bf16),
-            pltpu.VMEM(w_down.shape, bf16),
-            pltpu.SemaphoreType.DMA((2,)),
-        ],
-        compiler_params=LIMIT,
-        name="feed",
-    )(
-        *held(own, other, second_gain, w_gate.T, w_up.T, new_state), *far(w_down)
-    )
+        scratch_shapes=[pltpu.VMEM((rows, width // 2), bf16), pltpu.SemaphoreType.DMA],
+        compiler_params=LIMIT,
+        name="other",
+    )(*held(other, gains, ins, products, squares, outs, new_state))
+    mine = pl.pallas_call(
+        mine_kernel,
+        out_shape=shape(chunks, f32),
+        in_specs=in_vmem(2),
+        out_specs=in_vmem(1)[0],
+        compiler_params=LIMIT,
+        name="mine",
+    )(*held(hidden, outs))
     theirs = lax.ppermute(theirs, "tp", SWAP)
     chip_sum = pl.pallas_call(
         sum_kernel,
@@ -326,4 +412,6 @@
         P(KV_TP, None),
     )
     out_specs = (P("dp", KV_TP), P(DP_KV, "tp", None, None))
+
+
     return jax.shard_map(local, mesh=torus, in_specs=in_specs, out_specs=out_specs, check_vma=False)

time: 80.2 us -> 79.5 us (level)
  waiting for transfers between devices: 3.8 us -> 2.43 us
  local copies, waits for them, and re-layouts: 0.02 us -> 1.31 us
    ppermute x2, waiting for transfers between devices: 2.6 us -> 1.29 us  [local(): other = lax.ppermute(own, 'tp', SWAP)]
    unnamed x6 -> x16, local copies, waits for them, and re-layouts: 0.02 us -> 1.31 us
    pallas_call x2 -> x6, Pallas kernels: 3.31 us -> 3.82 us  [the longest x1 1.08 us: local(): pl.pallas_call(other_kernel, out_shape=(shape(chunks, bf16), shape((rows,...]
  transfers between devices with their start and end apart: 4 -> 4, of which waited for: 3 -> 3; matrix products, arithmetic and copies ran while one was open for 0% -> 0% of each run, Pallas kernels for 2% -> 4%
where the time goes in v5:
time: 79.5 us; the launch traced here: 79.2 us
  blocking collectives  67.5 us (85%)
  Pallas kernels  6.95 us (9%)
  waiting for transfers between devices  2.43 us (3%)
  local copies, waits for them, and re-layouts  1.31 us (2%)
    all_to_all x4, blocking collectives, exchanged(): return lax.all_to_all(pieces, axis, split_axis=0, concat_axis=0, tiled=True)  67.5 us
  transfers between devices with their start and end apart: 4, of which 3 were waited for; matrix products, arithmetic and copies ran while one was open for 0% of the time, Pallas kernels for 4%

profile of v5, /device:TPU:6, one launch (start us, length us, event | category | flops | bytes accessed | tf_op | source)
XLA Modules:
  0.0 79.2 jit_solution(15949269850581236988)
XLA Ops:
  0.6 0.1 collective-permute-start
  0.8 1.2 %load.1 = (bf16[32,64]{1,0:T(8,128)(2,1)S(1)}, f32[32,128]{1,0:T(8,128)S(1)}, f32[8,128]{1,0:T(8,128)S(1)}, f32[8,128]{1,0:T(8,128)S(1)}, f32[32,128]{1,0:T(8,128)S(1)}, /*index=5*/bf16[64,2048]{1,0:T(8,128)(2,1)S(1)}) custom-call(bf16[32,64]{1,0:T(8,128)(2,1)} %refs_0_.1, f32[32,128]{1,0:T(8,128)} %bitcast.14, f32[8,128]{1,0:T(8,128)} %bitcast.16, ...), custom_call_target="tpu_custom_call" | custom-call | flops 4000000000 | bytes 20000000 | tf_op jit(solution)/shard_map/load/pallas_call | solution.py:272
  1.9 0.0 copy-start.3
  2.0 0.2 collective-permute-done.other
  2.1 0.4 project.1
  2.6 0.0 copy-start
  2.6 25.7 %all_to_all.20.refs_0_ = bf16[32,9,4,128]{3,2,1,0:T(4,128)(2,1)S(1)} all-to-all(bf16[32,9,4,128]{3,2,1,0:T(4,128)(2,1)S(1)} %project.1), channel_id=1, replica_groups=mesh['dp'=4,'kv_0'=8,'kv_1'=4,'tp'=2] {'kv_0','kv_1'}, dimensions={0} | all-to-all | bytes 589824 | tf_op jit(solution)/shard_map/all_to_all | solution.py:21
  28.2 0.8 %recur.1 = (bf16[32,8,128]{2,1,0:T(8,128)(2,1)S(1)}, f32[8,128,128]{2,1,0:T(8,128)S(1)}) custom-call(bf16[32,9,4,128]{3,2,1,0:T(4,128)(2,1)S(1)} %all_to_all.20.refs_0_, f32[8,128,128]{2,1,0:T(8,128)S(1)} %bitcast.11, f32[8,128]{1,0:T(8,128)S(1)} %get-tuple-element.19.refs_2_, f32[8,128]{1,0:T(8,128)S(1)} %get-tuple-element.20.refs_3_), custom_call_target="tpu_custom_call" | custom-call | tf_op jit(solution)/shard_map/recur/pallas_call | solution.py:295
  29.0 13.6 %all_to_all.21.own = bf16[32,8,128]{2,1,0:T(8,128)(2,1)S(1)} all-to-all(bf16[32,8,128]{2,1,0:T(8,128)(2,1)S(1)} %get-tuple-element.21), channel_id=1, replica_groups=mesh['dp'=4,'kv_0'=8,'kv_1'=4,'tp'=2] {'kv_0','kv_1'}, dimensions={0} | all-to-all | bytes 131072 | tf_op jit(solution)/shard_map/all_to_all | solution.py:21
  42.7 1.3 %collective-permute-done.1.other = bf16[32,8,128]{2,1,0:T(8,128)(2,1)S(1)} collective-permute-done((bf16[32,8,128]{2,1,0:T(8,128)(2,1)S(1)}, bf16[32,8,128]{2,1,0:T(8,128)(2,1)S(1)}, u32[]{:S(2)}, u32[]{:S(2)}) %collective-permute-start.1) | collective-permute-done | bytes 65568 | tf_op jit(solution)/shard_map/ppermute | solution.py:305
  43.9 0.4 mix.1.mixed
  44.3 14.1 %all_to_all.22.chunk = bf16[32,16,128]{2,1,0:T(8,128)(2,1)S(1)} all-to-all(bf16[32,16,128]{2,1,0:T(8,128)(2,1)S(1)} %mix.1.mixed), channel_id=1, replica_groups=mesh['dp'=4,'kv_0'=8,'kv_1'=4,'tp'=2] {'kv_0','kv_1'}, dimensions={0} | all-to-all | bytes 262144 | tf_op jit(solution)/shard_map/all_to_all | solution.py:21
  58.4 0.5 arrange_out.1.outs
  58.9 0.8 %copy-done.1 = bf16[4096,176]{0,1:T(8,128)(2,1)S(1)} copy-done((bf16[4096,176]{0,1:T(8,128)(2,1)S(1)}, bf16[4096,176]{0,1:T(8,128)(2,1)}, u32[]{:S(2)}) %copy-start.1) | copy-done | bytes 1441816
  59.8 0.4 copy-done.2
  60.2 1.0 %arrange_in.1 = (bf16[2,352,2048]{2,1,0:T(8,128)(2,1)S(1)}, f32[2,16,128]{2,1,0:T(8,128)S(1)}) custom-call(bf16[176,4096]{1,0:T(8,128)(2,1)S(1)} %bitcast.9, bf16[176,4096]{1,0:T(8,128)(2,1)S(1)} %bitcast.10, f32[32,128]{1,0:T(8,128)S(1)} %get-tuple-element.23.gain), custom_call_target="tpu_custom_call" | custom-call | tf_op jit(solution)/shard_map/arrange_in/pallas_call | solution.py:320
  61.2 0.5 own.1
  61.7 0.0 collective-permute-done.2.chunk
  61.8 1.1 %other.1 = (bf16[32,16,128]{2,1,0:T(8,128)(2,1)S(1)}, bf16[32,176]{1,0:T(8,128)(2,1)S(1)}, f32[8,128,128]{2,1,0:T(8,128)}) custom-call(bf16[32,16,128]{2,1,0:T(8,128)(2,1)S(1)} %collective-permute-done.2.chunk, f32[2,16,128]{2,1,0:T(8,128)S(1)} %get-tuple-element.24.gains, bf16[2,352,2048]{2,1,0:T(8,128)(2,1)S(1)} %get-tuple-element.25.ins, ...), custom_call_target="tpu_custom_call" | custom-call | tf_op jit(solution)/shard_map/other/pallas_call | solution.py:352
  62.8 0.1 collective-permute-start.3
  62.9 0.3 mine.1
  63.3 1.0 %collective-permute-done.3.theirs = bf16[32,16,128]{2,1,0:T(8,128)(2,1)S(1)} collective-permute-done((bf16[32,16,128]{2,1,0:T(8,128)(2,1)S(1)}, bf16[32,16,128]{2,1,0:T(8,128)(2,1)S(1)}, u32[]{:S(2)}, u32[]{:S(2)}) %collective-permute-start.3) | collective-permute-done | bytes 131104 | tf_op jit(solution)/shard_map/ppermute | solution.py:373
  64.3 14.1 %all_to_all.23.pieces = bf16[32,16,128]{2,1,0:T(8,128)(2,1)S(1)} all-to-all(bf16[32,16,128]{2,1,0:T(8,128)(2,1)S(1)} %chip_sum.1), channel_id=1, replica_groups=mesh['dp'=4,'kv_0'=8,'kv_1'=4,'tp'=2] {'kv_0','kv_1'}, dimensions={0} | all-to-all | bytes 262144 | tf_op jit(solution)/shard_map/all_to_all | solution.py:21
  78.4 0.8 finish.1
  (15 shorter events, 0.1 us)
Async XLA Ops:
  0.6 1.5 %collective-permute-start = (bf16[32,64]{1,0:T(8,128)(2,1)}, bf16[32,64]{1,0:T(8,128)(2,1)S(1)}, u32[]{:S(2)}, u32[]{:S(2)}) collective-permute-start(bf16[32,64]{1,0:T(8,128)(2,1)} %refs_0_.1), channel_id=1, source_target_pairs={{0,1},{1,0},{2,3},{3,2},{4,5},{5,4},{6,7},{7,6},{8,9},{9,8},{10,11... | collective-permute-start | bytes 12296 | tf_op jit(solution)/shard_map/ppermute | solution.py:263
  0.7 1.4 %copy-start.4 = (bf16[128,1024]{1,0:T(8,128)(2,1)S(1)}, bf16[128,1024]{1,0:T(8,128)(2,1)}, u32[]{:S(2)}) copy-start(bf16[128,1024]{1,0:T(8,128)(2,1)} %wq.1) | copy-start | bytes 786436
  0.7 1.4 %copy-start.5 = (bf16[128,1024]{1,0:T(8,128)(2,1)S(1)}, bf16[128,1024]{1,0:T(8,128)(2,1)}, u32[]{:S(2)}) copy-start(bf16[128,1024]{1,0:T(8,128)(2,1)} %wf.1) | copy-start | bytes 786436
  0.8 1.4 %copy-start.6 = (bf16[128,1024]{1,0:T(8,128)(2,1)S(1)}, bf16[128,1024]{1,0:T(8,128)(2,1)}, u32[]{:S(2)}) copy-start(bf16[128,1024]{1,0:T(8,128)(2,1)} %wi.1) | copy-start | bytes 786436
  0.8 1.4 %copy-start.7 = (bf16[128,1024]{1,0:T(8,128)(2,1)S(1)}, bf16[128,1024]{1,0:T(8,128)(2,1)}, u32[]{:S(2)}) copy-start(bf16[128,1024]{1,0:T(8,128)(2,1)} %wg.1) | copy-start | bytes 786436
  1.9 26.3 %copy-start.3 = (f32[1,8,128,128]{3,2,1,0:T(8,128)S(1)}, f32[1,8,128,128]{3,2,1,0:T(8,128)}, u32[]{:S(2)}) copy-start(f32[1,8,128,128]{3,2,1,0:T(8,128)} %param.15) | copy-start | bytes 1572868
  2.6 55.9 %copy-start = (bf16[176,4096]{1,0:T(8,128)(2,1)S(1)}, bf16[176,4096]{1,0:T(8,128)(2,1)}, u32[]{:S(2)}) copy-start(bf16[176,4096]{1,0:T(8,128)(2,1)} %w_down.1) | copy-start | bytes 4325380
  42.7 1.3 %collective-permute-start.1 = (bf16[32,8,128]{2,1,0:T(8,128)(2,1)S(1)}, bf16[32,8,128]{2,1,0:T(8,128)(2,1)S(1)}, u32[]{:S(2)}, u32[]{:S(2)}) collective-permute-start(bf16[32,8,128]{2,1,0:T(8,128)(2,1)S(1)} %all_to_all.21.own), channel_id=1, source_target_pairs={{0,1},{1,0},{2,3},{3,2},{4,5},{5,4},{6,7},{7,6},{8,9},{9,8},{10,11... | collective-permute-start | bytes 196616 | tf_op jit(solution)/shard_map/ppermute | solution.py:305
  58.4 1.4 %copy-start.1 = (bf16[4096,176]{0,1:T(8,128)(2,1)S(1)}, bf16[4096,176]{0,1:T(8,128)(2,1)}, u32[]{:S(2)}) copy-start(bf16[4096,176]{0,1:T(8,128)(2,1)} %param.25) | copy-start | bytes 4325380
  58.4 1.8 %copy-start.2 = (bf16[4096,176]{0,1:T(8,128)(2,1)S(1)}, bf16[4096,176]{0,1:T(8,128)(2,1)}, u32[]{:S(2)}) copy-start(bf16[4096,176]{0,1:T(8,128)(2,1)} %param.26) | copy-start | bytes 4325380
  58.4 3.3 %collective-permute-start.2 = (bf16[32,16,128]{2,1,0:T(8,128)(2,1)S(1)}, bf16[32,16,128]{2,1,0:T(8,128)(2,1)S(1)}, u32[]{:S(2)}, u32[]{:S(2)}) collective-permute-start(bf16[32,16,128]{2,1,0:T(8,128)(2,1)S(1)} %all_to_all.22.chunk), channel_id=1, source_target_pairs={{0,1},{1,0},{2,3},{3,2},{4,5},{5,4},{6,7},{7,6},{8,9},{9,8},{10,11... | collective-permute-start | bytes 393224 | tf_op jit(solution)/shard_map/ppermute | solution.py:341
  62.8 1.4 %collective-permute-start.3 = (bf16[32,16,128]{2,1,0:T(8,128)(2,1)S(1)}, bf16[32,16,128]{2,1,0:T(8,128)(2,1)S(1)}, u32[]{:S(2)}, u32[]{:S(2)}) collective-permute-start(bf16[32,16,128]{2,1,0:T(8,128)(2,1)S(1)} %get-tuple-element.30), channel_id=1, source_target_pairs={{0,1},{1,0},{2,3},{3,2},{4,5},{5,4},{6,7},{7,6},{8,9},{9,8},{10,11... | collective-permute-start | bytes 393224 | tf_op jit(solution)/shard_map/ppermute | solution.py:373

commit v6 on v5

--- a/solution.py
+++ b/solution.py
@@ -17,8 +17,16 @@
 bf16, f32 = jnp.bfloat16, jnp.float32
 
 
-def exchanged(pieces, axis):
-    return lax.all_to_all(pieces, axis, split_axis=0, concat_axis=0, tiled=True)
+FIRST = 22
+COUNT = 32
+MEMBERS = [(FIRST + slot) % COUNT for slot in range(COUNT)]
+SLOTS = [MEMBERS.index(place) for place in range(COUNT)]
+
+
+def exchanged(pieces):
+    return lax.all_to_all(
+        pieces, KV, split_axis=0, concat_axis=0, axis_index_groups=[MEMBERS], tiled=True
+    )
 
 
 def low_lanes(shape):
@@ -80,7 +88,7 @@
         rows_scr[pl.ds(row, rows, stride=step), :] = extra
     for row in range(rows):
         piece = rows_scr[pl.ds(row * step, step), :].reshape(out.shape[1:])
-        out[row] = piece.astype(bf16)
+        out[SLOTS[row]] = piece.astype(bf16)
 
 
 def recur_kernel(pieces, state, bound, gain, gated, new_state, width):
@@ -114,8 +122,9 @@
     core = lax.axis_index("tp")
     rows = tokens.shape[0]
     heads = own.shape[1]
-    rows_scr[0] = own[...].astype(f32).reshape(rows * heads, LANES)
-    rows_scr[1] = other[...].astype(f32).reshape(rows * heads, LANES)
+    for row in range(rows):
+        rows_scr[0, row * heads : (row + 1) * heads, :] = own[SLOTS[row]].astype(f32)
+        rows_scr[1, row * heads : (row + 1) * heads, :] = other[SLOTS[row]].astype(f32)
     for side in range(2):
         source = (core + side) % 2
         for head in range(heads):
@@ -170,7 +179,7 @@
     squares = jnp.zeros((2 * half, LANES), f32)
     for pair in range(blocks // 2):
         first, second = split_lanes(
-            low, chunk[2 * pair].astype(f32), chunk[2 * pair + 1].astype(f32)
+            low, chunk[SLOTS[2 * pair]].astype(f32), chunk[SLOTS[2 * pair + 1]].astype(f32)
         )
         value = jnp.concatenate([first, second], axis=0)
         squares = squares + value * value
@@ -210,8 +219,8 @@
     low = low_lanes((half, LANES))
     for pair in range(chunk.shape[0] // 2):
         left, right = packed_rows(low, terms[:, part(pair)], True)
-        theirs[2 * pair] = left.astype(bf16)
-        theirs[2 * pair + 1] = right.astype(bf16)
+        theirs[SLOTS[2 * pair]] = left.astype(bf16)
+        theirs[SLOTS[2 * pair + 1]] = right.astype(bf16)
     store.wait()
 
 
@@ -219,7 +228,9 @@
     terms = jnp.dot(hidden[...], outs[lax.axis_index("tp")], preferred_element_type=f32)
     low = low_lanes(mine.shape[1:])
     for pair in range(mine.shape[0] // 2):
-        mine[2 * pair], mine[2 * pair + 1] = packed_rows(low, terms[:, part(pair)], False)
+        left, right = packed_rows(low, terms[:, part(pair)], False)
+        mine[SLOTS[2 * pair]] = left
+        mine[SLOTS[2 * pair + 1]] = right
 
 
 def sum_kernel(mine, theirs, out):
@@ -290,7 +301,7 @@
     )(
         *held(tokens_here, other, first_gain, w_query, w_forget, w_input, w_outgate)
     )
-    pieces = exchanged(pieces, KV)
+    pieces = exchanged(pieces)
 
     gated, new_state = pl.pallas_call(
         lambda *refs: recur_kernel(*refs, width),
@@ -301,7 +312,7 @@
         name="recur",
     )(*held(pieces, rec_state[0], bound, gain))
 
-    own = exchanged(gated, KV)
+    own = exchanged(gated)
     other = lax.ppermute(own, "tp", SWAP)
     mixed = pl.pallas_call(
         mix_kernel,
@@ -337,7 +348,7 @@
         name="arrange_out",
     )(*held(w_down))
 
-    own = exchanged(mixed, KV)
+    own = exchanged(mixed)
     other = lax.ppermute(own, "tp", SWAP)
     chunks = (kv_count, half, LANES)
     products, squares = pl.pallas_call(
@@ -379,7 +390,7 @@
         compiler_params=LIMIT,
         name="chip_sum",
     )(*held(mine, theirs))
-    down = exchanged(chip_sum, KV)
+    down = exchanged(chip_sum)
     result = pl.pallas_call(
         finish_kernel,
         out_shape=jax.ShapeDtypeStruct((rows, cols), bf16),

time: 79.5 us -> 74.8 us (0.941)
  blocking collectives: 67.5 us -> 62.8 us
    all_to_all x4, blocking collectives: 67.5 us -> 62.8 us  [exchanged(): lax.all_to_all(pieces, KV, split_axis=0, concat_axis=0, axis_index_groups...]
  transfers between devices with their start and end apart: 4 -> 4, of which waited for: 3 -> 3; matrix products, arithmetic and copies ran while one was open for 0% -> 0% of each run, Pallas kernels for 4% -> 5%
where the time goes in v6:
time: 74.8 us; the launch traced here: 74.5 us
  blocking collectives  62.8 us (84%)
  Pallas kernels  6.95 us (9%)
  waiting for transfers between devices  2.43 us (3%)
  local copies, waits for them, and re-layouts  1.31 us (2%)
  between operations  0.79 us (1%)
    all_to_all x4, blocking collectives, exchanged(): lax.all_to_all(pieces, KV, split_axis=0, concat_axis=0, axis_index_groups...  62.8 us
  transfers between devices with their start and end apart: 4, of which 3 were waited for; matrix products, arithmetic and copies ran while one was open for 0% of the time, Pallas kernels for 5%

profile of v6, /device:TPU:6, one launch (start us, length us, event | category | flops | bytes accessed | tf_op | source)
XLA Modules:
  0.0 74.5 jit_solution(15563198800557199733)
XLA Ops:
  0.6 0.1 collective-permute-start
  0.8 1.2 %load.1 = (bf16[32,64]{1,0:T(8,128)(2,1)S(1)}, f32[32,128]{1,0:T(8,128)S(1)}, f32[8,128]{1,0:T(8,128)S(1)}, f32[8,128]{1,0:T(8,128)S(1)}, f32[32,128]{1,0:T(8,128)S(1)}, /*index=5*/bf16[64,2048]{1,0:T(8,128)(2,1)S(1)}) custom-call(bf16[32,64]{1,0:T(8,128)(2,1)} %refs_0_.1, f32[32,128]{1,0:T(8,128)} %bitcast.14, f32[8,128]{1,0:T(8,128)} %bitcast.16, ...), custom_call_target="tpu_custom_call" | custom-call | flops 4000000000 | bytes 20000000 | tf_op jit(solution)/shard_map/load/pallas_call | solution.py:283
  1.9 0.0 copy-start.3
  2.0 0.2 collective-permute-done.other
  2.1 0.4 project.1
  2.6 0.0 copy-start
  2.6 21.5 %all_to_all.20.refs_0_ = bf16[32,9,4,128]{3,2,1,0:T(4,128)(2,1)S(1)} all-to-all(bf16[32,9,4,128]{3,2,1,0:T(4,128)(2,1)S(1)} %project.1), channel_id=1, replica_groups={{44,46,48,50,52,54,56,58,60,62,0,2,4,6,8,10,12,14,16,18,20,22,24,26,28,..., dimensions={0} | all-to-all | bytes 589824 | tf_op jit(solution)/shard_map/all_to_all | solution.py:27
  24.0 0.8 %recur.1 = (bf16[32,8,128]{2,1,0:T(8,128)(2,1)S(1)}, f32[8,128,128]{2,1,0:T(8,128)S(1)}) custom-call(bf16[32,9,4,128]{3,2,1,0:T(4,128)(2,1)S(1)} %all_to_all.20.refs_0_, f32[8,128,128]{2,1,0:T(8,128)S(1)} %bitcast.11, f32[8,128]{1,0:T(8,128)S(1)} %get-tuple-element.19.refs_2_, f32[8,128]{1,0:T(8,128)S(1)} %get-tuple-element.20.refs_3_), custom_call_target="tpu_custom_call" | custom-call | tf_op jit(solution)/shard_map/recur/pallas_call | solution.py:306
  24.8 12.7 %all_to_all.21.own = bf16[32,8,128]{2,1,0:T(8,128)(2,1)S(1)} all-to-all(bf16[32,8,128]{2,1,0:T(8,128)(2,1)S(1)} %get-tuple-element.21), channel_id=1, replica_groups={{44,46,48,50,52,54,56,58,60,62,0,2,4,6,8,10,12,14,16,18,20,22,24,26,28,..., dimensions={0} | all-to-all | bytes 131072 | tf_op jit(solution)/shard_map/all_to_all | solution.py:27
  37.5 1.3 %collective-permute-done.1.other = bf16[32,8,128]{2,1,0:T(8,128)(2,1)S(1)} collective-permute-done((bf16[32,8,128]{2,1,0:T(8,128)(2,1)S(1)}, bf16[32,8,128]{2,1,0:T(8,128)(2,1)S(1)}, u32[]{:S(2)}, u32[]{:S(2)}) %collective-permute-start.1) | collective-permute-done | bytes 65568 | tf_op jit(solution)/shard_map/ppermute | solution.py:316
  38.8 0.4 mix.1.mixed
  39.2 14.5 %all_to_all.22.chunk = bf16[32,16,128]{2,1,0:T(8,128)(2,1)S(1)} all-to-all(bf16[32,16,128]{2,1,0:T(8,128)(2,1)S(1)} %mix.1.mixed), channel_id=1, replica_groups={{44,46,48,50,52,54,56,58,60,62,0,2,4,6,8,10,12,14,16,18,20,22,24,26,28,..., dimensions={0} | all-to-all | bytes 262144 | tf_op jit(solution)/shard_map/all_to_all | solution.py:27
  53.6 0.5 arrange_out.1.outs
  54.2 0.8 %copy-done.1 = bf16[4096,176]{0,1:T(8,128)(2,1)S(1)} copy-done((bf16[4096,176]{0,1:T(8,128)(2,1)S(1)}, bf16[4096,176]{0,1:T(8,128)(2,1)}, u32[]{:S(2)}) %copy-start.1) | copy-done | bytes 1441816
  55.0 0.4 copy-done.2
  55.4 1.0 %arrange_in.1 = (bf16[2,352,2048]{2,1,0:T(8,128)(2,1)S(1)}, f32[2,16,128]{2,1,0:T(8,128)S(1)}) custom-call(bf16[176,4096]{1,0:T(8,128)(2,1)S(1)} %bitcast.9, bf16[176,4096]{1,0:T(8,128)(2,1)S(1)} %bitcast.10, f32[32,128]{1,0:T(8,128)S(1)} %get-tuple-element.23.gain), custom_call_target="tpu_custom_call" | custom-call | tf_op jit(solution)/shard_map/arrange_in/pallas_call | solution.py:331
  56.4 0.5 own.1
  56.9 0.0 collective-permute-done.2.chunk
  57.0 1.1 %other.1 = (bf16[32,16,128]{2,1,0:T(8,128)(2,1)S(1)}, bf16[32,176]{1,0:T(8,128)(2,1)S(1)}, f32[8,128,128]{2,1,0:T(8,128)}) custom-call(bf16[32,16,128]{2,1,0:T(8,128)(2,1)S(1)} %collective-permute-done.2.chunk, f32[2,16,128]{2,1,0:T(8,128)S(1)} %get-tuple-element.24.gains, bf16[2,352,2048]{2,1,0:T(8,128)(2,1)S(1)} %get-tuple-element.25.ins, ...), custom_call_target="tpu_custom_call" | custom-call | tf_op jit(solution)/shard_map/other/pallas_call | solution.py:363
  58.1 0.1 collective-permute-start.3
  58.2 0.3 mine.1
  58.5 1.0 %collective-permute-done.3.theirs = bf16[32,16,128]{2,1,0:T(8,128)(2,1)S(1)} collective-permute-done((bf16[32,16,128]{2,1,0:T(8,128)(2,1)S(1)}, bf16[32,16,128]{2,1,0:T(8,128)(2,1)S(1)}, u32[]{:S(2)}, u32[]{:S(2)}) %collective-permute-start.3) | collective-permute-done | bytes 131104 | tf_op jit(solution)/shard_map/ppermute | solution.py:384
  59.5 14.2 %all_to_all.23.pieces = bf16[32,16,128]{2,1,0:T(8,128)(2,1)S(1)} all-to-all(bf16[32,16,128]{2,1,0:T(8,128)(2,1)S(1)} %chip_sum.1), channel_id=1, replica_groups={{44,46,48,50,52,54,56,58,60,62,0,2,4,6,8,10,12,14,16,18,20,22,24,26,28,..., dimensions={0} | all-to-all | bytes 262144 | tf_op jit(solution)/shard_map/all_to_all | solution.py:27
  73.7 0.8 %finish.1 = bf16[32,64]{1,0:T(8,128)(2,1)} custom-call(bf16[32,16,128]{2,1,0:T(8,128)(2,1)S(1)} %all_to_all.23.pieces, bf16[32,16,128]{2,1,0:T(8,128)(2,1)S(1)} %mix.1.mixed), custom_call_target="tpu_custom_call" | custom-call | tf_op jit(solution)/shard_map/finish/pallas_call | solution.py:394
  (15 shorter events, 0.1 us)
Async XLA Ops:
  0.6 1.5 %collective-permute-start = (bf16[32,64]{1,0:T(8,128)(2,1)}, bf16[32,64]{1,0:T(8,128)(2,1)S(1)}, u32[]{:S(2)}, u32[]{:S(2)}) collective-permute-start(bf16[32,64]{1,0:T(8,128)(2,1)} %refs_0_.1), channel_id=1, source_target_pairs={{0,1},{1,0},{2,3},{3,2},{4,5},{5,4},{6,7},{7,6},{8,9},{9,8},{10,11... | collective-permute-start | bytes 12296 | tf_op jit(solution)/shard_map/ppermute | solution.py:274
  0.7 1.4 %copy-start.4 = (bf16[128,1024]{1,0:T(8,128)(2,1)S(1)}, bf16[128,1024]{1,0:T(8,128)(2,1)}, u32[]{:S(2)}) copy-start(bf16[128,1024]{1,0:T(8,128)(2,1)} %wq.1) | copy-start | bytes 786436
  0.7 1.4 %copy-start.5 = (bf16[128,1024]{1,0:T(8,128)(2,1)S(1)}, bf16[128,1024]{1,0:T(8,128)(2,1)}, u32[]{:S(2)}) copy-start(bf16[128,1024]{1,0:T(8,128)(2,1)} %wf.1) | copy-start | bytes 786436
  0.8 1.4 %copy-start.6 = (bf16[128,1024]{1,0:T(8,128)(2,1)S(1)}, bf16[128,1024]{1,0:T(8,128)(2,1)}, u32[]{:S(2)}) copy-start(bf16[128,1024]{1,0:T(8,128)(2,1)} %wi.1) | copy-start | bytes 786436
  0.8 1.4 %copy-start.7 = (bf16[128,1024]{1,0:T(8,128)(2,1)S(1)}, bf16[128,1024]{1,0:T(8,128)(2,1)}, u32[]{:S(2)}) copy-start(bf16[128,1024]{1,0:T(8,128)(2,1)} %wg.1) | copy-start | bytes 786436
  1.9 22.1 %copy-start.3 = (f32[1,8,128,128]{3,2,1,0:T(8,128)S(1)}, f32[1,8,128,128]{3,2,1,0:T(8,128)}, u32[]{:S(2)}) copy-start(f32[1,8,128,128]{3,2,1,0:T(8,128)} %param.15) | copy-start | bytes 1572868
  2.6 51.1 %copy-start = (bf16[176,4096]{1,0:T(8,128)(2,1)S(1)}, bf16[176,4096]{1,0:T(8,128)(2,1)}, u32[]{:S(2)}) copy-start(bf16[176,4096]{1,0:T(8,128)(2,1)} %w_down.1) | copy-start | bytes 4325380
  37.5 1.3 %collective-permute-start.1 = (bf16[32,8,128]{2,1,0:T(8,128)(2,1)S(1)}, bf16[32,8,128]{2,1,0:T(8,128)(2,1)S(1)}, u32[]{:S(2)}, u32[]{:S(2)}) collective-permute-start(bf16[32,8,128]{2,1,0:T(8,128)(2,1)S(1)} %all_to_all.21.own), channel_id=1, source_target_pairs={{0,1},{1,0},{2,3},{3,2},{4,5},{5,4},{6,7},{7,6},{8,9},{9,8},{10,11... | collective-permute-start | bytes 196616 | tf_op jit(solution)/shard_map/ppermute | solution.py:316
  53.6 1.4 %copy-start.1 = (bf16[4096,176]{0,1:T(8,128)(2,1)S(1)}, bf16[4096,176]{0,1:T(8,128)(2,1)}, u32[]{:S(2)}) copy-start(bf16[4096,176]{0,1:T(8,128)(2,1)} %param.25) | copy-start | bytes 4325380
  53.6 1.8 %copy-start.2 = (bf16[4096,176]{0,1:T(8,128)(2,1)S(1)}, bf16[4096,176]{0,1:T(8,128)(2,1)}, u32[]{:S(2)}) copy-start(bf16[4096,176]{0,1:T(8,128)(2,1)} %param.26) | copy-start | bytes 4325380
  53.6 3.3 %collective-permute-start.2 = (bf16[32,16,128]{2,1,0:T(8,128)(2,1)S(1)}, bf16[32,16,128]{2,1,0:T(8,128)(2,1)S(1)}, u32[]{:S(2)}, u32[]{:S(2)}) collective-permute-start(bf16[32,16,128]{2,1,0:T(8,128)(2,1)S(1)} %all_to_all.22.chunk), channel_id=1, source_target_pairs={{0,1},{1,0},{2,3},{3,2},{4,5},{5,4},{6,7},{7,6},{8,9},{9,8},{10,11... | collective-permute-start | bytes 393224 | tf_op jit(solution)/shard_map/ppermute | solution.py:352
  58.1 1.4 %collective-permute-start.3 = (bf16[32,16,128]{2,1,0:T(8,128)(2,1)S(1)}, bf16[32,16,128]{2,1,0:T(8,128)(2,1)S(1)}, u32[]{:S(2)}, u32[]{:S(2)}) collective-permute-start(bf16[32,16,128]{2,1,0:T(8,128)(2,1)S(1)} %get-tuple-element.30), channel_id=1, source_target_pairs={{0,1},{1,0},{2,3},{3,2},{4,5},{5,4},{6,7},{7,6},{8,9},{9,8},{10,11... | collective-permute-start | bytes 393224 | tf_op jit(solution)/shard_map/ppermute | solution.py:384

commit v7 on v5

--- a/solution.py
+++ b/solution.py
@@ -17,8 +17,39 @@
 bf16, f32 = jnp.bfloat16, jnp.float32
 
 
-def exchanged(pieces, axis):
-    return lax.all_to_all(pieces, axis, split_axis=0, concat_axis=0, tiled=True)
+COUNT = 32
+OWNERS = [22, 23, 24, 25, 26, 27, 28, 29, 30, 31, 0, 1, 2, 3, 4, 5, 6, 7, 8, 9, 10, 11, 12, 13, 14, 15, 16, 17, 18, 19, 20, 21]
+ORDERS = [
+    [22, 23, 24, 25, 26, 27, 28, 29, 30, 31, 0, 1, 2, 3, 4, 5, 6, 7, 8, 9, 10, 11, 12, 13, 14, 15, 16, 17, 18, 19, 20, 21],
+    [18, 19, 20, 21, 22, 23, 24, 25, 26, 27, 28, 29, 30, 31, 0, 1, 2, 3, 4, 5, 6, 7, 8, 9, 10, 11, 12, 13, 14, 15, 16, 17],
+]
+LAST_ORDERS = [
+    [22, 11, 24, 8, 21, 14, 16, 29, 9, 31, 20, 12, 25, 13, 19, 28, 4, 2, 10, 15, 1, 5, 23, 3, 18, 0, 30, 17, 7, 27, 6, 26],
+    [18, 20, 25, 14, 28, 30, 12, 27, 6, 31, 26, 8, 23, 5, 11, 21, 4, 16, 1, 9, 7, 0, 13, 15, 29, 19, 3, 10, 2, 22, 17, 24],
+]
+FIRST_PLANE = 5
+TURNED = [(place // 4 - FIRST_PLANE) % 8 < 4 for place in range(COUNT)]
+
+
+def teams(orders):
+    return [[2 * place + (team ^ TURNED[place]) for place in orders[team]] for team in range(2)]
+
+
+def exchanged(pieces, axes, groups):
+    return lax.all_to_all(
+        pieces, axes, split_axis=0, concat_axis=0, axis_index_groups=groups, tiled=True
+    )
+
+
+def my_team():
+    plane, core = lax.axis_index("kv_0"), lax.axis_index("tp")
+    return jnp.where((plane + 8 - FIRST_PLANE) % 8 < 4, 1 - core, core)
+
+
+def for_my_team(body):
+    mine = my_team()
+    for team in range(2):
+        pl.when(mine == team)(lambda team=team: body(team))
 
 
 def low_lanes(shape):
@@ -80,7 +111,7 @@
         rows_scr[pl.ds(row, rows, stride=step), :] = extra
     for row in range(rows):
         piece = rows_scr[pl.ds(row * step, step), :].reshape(out.shape[1:])
-        out[row] = piece.astype(bf16)
+        out[OWNERS.index(row)] = piece.astype(bf16)
 
 
 def recur_kernel(pieces, state, bound, gain, gated, new_state, width):
@@ -111,25 +142,29 @@
 
 
 def mix_kernel(own, other, tokens, weight, out, rows_scr, whole_scr):
-    core = lax.axis_index("tp")
-    rows = tokens.shape[0]
-    heads = own.shape[1]
-    rows_scr[0] = own[...].astype(f32).reshape(rows * heads, LANES)
-    rows_scr[1] = other[...].astype(f32).reshape(rows * heads, LANES)
-    for side in range(2):
-        source = (core + side) % 2
-        for head in range(heads):
-            column = (side * heads + head) * LANES
-            whole_scr[:, column : column + LANES] = rows_scr[
-                source, pl.ds(head, rows, stride=heads), :
-            ].astype(bf16)
-    added = lax.dot_general(whole_scr[...], weight[...], NT, preferred_element_type=f32)
-    mixed = tokens[...].astype(f32) + added
-    half = rows // 2
-    packed = jnp.concatenate([mixed[:half], mixed[half:]], axis=1)
-    packed = jnp.where(core == 0, packed, half_turn(packed)).astype(bf16)
-    for peer in range(out.shape[0]):
-        out[peer] = packed
+    def body(team):
+        rows = tokens.shape[0]
+        heads = own.shape[1]
+        for row in range(rows):
+            place = slice(row * heads, (row + 1) * heads)
+            side = 1 - team if TURNED[row] else team
+            rows_scr[side, place, :] = own[ORDERS[team].index(row)].astype(f32)
+            rows_scr[1 - side, place, :] = other[ORDERS[1 - team].index(row)].astype(f32)
+        for side in range(2):
+            for head in range(heads):
+                column = (side * heads + head) * LANES
+                whole_scr[:, column : column + LANES] = rows_scr[
+                    side, pl.ds(head, rows, stride=heads), :
+                ].astype(bf16)
+        added = lax.dot_general(whole_scr[...], weight[...], NT, preferred_element_type=f32)
+        mixed = tokens[...].astype(f32) + added
+        half = rows // 2
+        packed = jnp.concatenate([mixed[:half], mixed[half:]], axis=1)
+        packed = (half_turn(packed) if team else packed).astype(bf16)
+        for peer in range(out.shape[0]):
+            out[peer] = packed
+
+    for_my_team(body)
 
 
 def part(index):
@@ -138,6 +173,10 @@
 
 def split_lanes(low, left, right):
     return jnp.where(low, left, half_turn(right)), jnp.where(low, half_turn(left), right)
+
+
+def by_team(pair, halves):
+    return halves[::-1] if TURNED[2 * pair] else halves
 
 
 def arrange_in_kernel(w_gate, w_up, gain, ins, gains):
@@ -146,11 +185,14 @@
     for pair in range(w_gate.shape[1] // (2 * LANES)):
         left, right = part(2 * pair), part(2 * pair + 1)
         for index, weight in enumerate((w_gate, w_up)):
-            first, second = split_lanes(low, weight[:, left], weight[:, right])
+            first, second = by_team(pair, split_lanes(low, weight[:, left], weight[:, right]))
             ins[0, index * units : (index + 1) * units, part(pair)] = first
             ins[1, index * units : (index + 1) * units, part(pair)] = second
-        first, second = split_lanes(
-            low[:1], gain[2 * pair : 2 * pair + 1, :], gain[2 * pair + 1 : 2 * pair + 2, :]
+        first, second = by_team(
+            pair,
+            split_lanes(
+                low[:1], gain[2 * pair : 2 * pair + 1, :], gain[2 * pair + 1 : 2 * pair + 2, :]
+            ),
         )
         gains[0, pair : pair + 1, :] = first
         gains[1, pair : pair + 1, :] = second
@@ -159,28 +201,35 @@
 def arrange_out_kernel(w_down, outs):
     low = low_lanes((w_down.shape[0], LANES))
     for pair in range(w_down.shape[1] // (2 * LANES)):
-        first, second = split_lanes(low, w_down[:, part(2 * pair)], w_down[:, part(2 * pair + 1)])
+        first, second = by_team(
+            pair, split_lanes(low, w_down[:, part(2 * pair)], w_down[:, part(2 * pair + 1)])
+        )
         outs[0, :, part(pair)] = first
         outs[1, :, part(pair)] = second
 
 
-def half_feed(core, chunk, gains, ins, scr):
+def half_feed(team, chunk, gains, ins, scr):
     blocks, half, _ = chunk.shape
     low = low_lanes((half, LANES))
     squares = jnp.zeros((2 * half, LANES), f32)
     for pair in range(blocks // 2):
         first, second = split_lanes(
-            low, chunk[2 * pair].astype(f32), chunk[2 * pair + 1].astype(f32)
+            low,
+            chunk[ORDERS[team].index(2 * pair)].astype(f32),
+            chunk[ORDERS[team].index(2 * pair + 1)].astype(f32),
         )
         value = jnp.concatenate([first, second], axis=0)
         squares = squares + value * value
-        scr[:, part(pair)] = (value * gains[core, pair : pair + 1, :]).astype(bf16)
-    products = lax.dot_general(scr[...], ins[core], NT, preferred_element_type=f32)
+        scr[:, part(pair)] = (value * gains[team, pair : pair + 1, :]).astype(bf16)
+    products = lax.dot_general(scr[...], ins[team], NT, preferred_element_type=f32)
     return products, squares
 
 
 def own_kernel(chunk, gains, ins, products, squares, scr):
-    products[...], squares[...] = half_feed(lax.axis_index("tp"), chunk, gains, ins, scr)
+    def body(team):
+        products[...], squares[...] = half_feed(team, chunk, gains, ins, scr)
+
+    for_my_team(body)
 
 
 def packed_rows(low, block, turned):
@@ -196,30 +245,38 @@
 ):
     store = pltpu.make_async_copy(state, state_hbm, sem)
     store.start()
-    core = lax.axis_index("tp")
-    half = chunk.shape[1]
-    more, more_squares = half_feed(1 - core, chunk, gains, ins, scr)
-    totals = products[...] + jnp.concatenate([more[half:], more[:half]], axis=0)
-    both = squares[...] + jnp.concatenate([more_squares[half:], more_squares[:half]], axis=0)
-    mean = jnp.sum(both, axis=1, keepdims=True) / (chunk.shape[0] * LANES)
-    totals = totals * lax.rsqrt(mean + epsilon)
-    units = totals.shape[1] // 2
-    hidden = (jax.nn.silu(totals[:, :units]) * totals[:, units:]).astype(bf16)
-    hidden_out[...] = hidden
-    terms = jnp.dot(hidden, outs[1 - core], preferred_element_type=f32)
-    low = low_lanes((half, LANES))
-    for pair in range(chunk.shape[0] // 2):
-        left, right = packed_rows(low, terms[:, part(pair)], True)
-        theirs[2 * pair] = left.astype(bf16)
-        theirs[2 * pair + 1] = right.astype(bf16)
+
+    def body(team):
+        half = chunk.shape[1]
+        more, more_squares = half_feed(1 - team, chunk, gains, ins, scr)
+        totals = products[...] + jnp.concatenate([more[half:], more[:half]], axis=0)
+        both = squares[...] + jnp.concatenate([more_squares[half:], more_squares[:half]], axis=0)
+        mean = jnp.sum(both, axis=1, keepdims=True) / (chunk.shape[0] * LANES)
+        totals = totals * lax.rsqrt(mean + epsilon)
+        units = totals.shape[1] // 2
+        hidden = (jax.nn.silu(totals[:, :units]) * totals[:, units:]).astype(bf16)
+        hidden_out[...] = hidden
+        terms = jnp.dot(hidden, outs[1 - team], preferred_element_type=f32)
+        low = low_lanes((half, LANES))
+        for pair in range(chunk.shape[0] // 2):
+            left, right = packed_rows(low, terms[:, part(pair)], True)
+            theirs[LAST_ORDERS[1 - team].index(2 * pair)] = left.astype(bf16)
+            theirs[LAST_ORDERS[1 - team].index(2 * pair + 1)] = right.astype(bf16)
+
+    for_my_team(body)
     store.wait()
 
 
 def mine_kernel(hidden, outs, mine):
-    terms = jnp.dot(hidden[...], outs[lax.axis_index("tp")], preferred_element_type=f32)
-    low = low_lanes(mine.shape[1:])
-    for pair in range(mine.shape[0] // 2):
-        mine[2 * pair], mine[2 * pair + 1] = packed_rows(low, terms[:, part(pair)], False)
+    def body(team):
+        terms = jnp.dot(hidden[...], outs[team], preferred_element_type=f32)
+        low = low_lanes(mine.shape[1:])
+        for pair in range(mine.shape[0] // 2):
+            left, right = packed_rows(low, terms[:, part(pair)], False)
+            mine[LAST_ORDERS[team].index(2 * pair)] = left
+            mine[LAST_ORDERS[team].index(2 * pair + 1)] = right
+
+    for_my_team(body)
 
 
 def sum_kernel(mine, theirs, out):
@@ -227,10 +284,9 @@
 
 
 def finish_kernel(pieces, mixed, out):
-    core = lax.axis_index("tp")
     half = mixed.shape[1]
     total = mixed[0].astype(f32) + jnp.sum(pieces[...].astype(f32), axis=0)
-    total = jnp.where(core == 0, total, half_turn(total))
+    total = jnp.where(my_team() == 0, total, half_turn(total))
     out[:half] = total[:, : LANES // 2].astype(bf16)
     out[half:] = half_turn(total)[:, : LANES // 2].astype(bf16)
 
@@ -290,7 +346,7 @@
     )(
         *held(tokens_here, other, first_gain, w_query, w_forget, w_input, w_outgate)
     )
-    pieces = exchanged(pieces, KV)
+    pieces = exchanged(pieces, KV, [OWNERS])
 
     gated, new_state = pl.pallas_call(
         lambda *refs: recur_kernel(*refs, width),
@@ -301,7 +357,7 @@
         name="recur",
     )(*held(pieces, rec_state[0], bound, gain))
 
-    own = exchanged(gated, KV)
+    own = exchanged(gated, KV_TP, teams(ORDERS))
     other = lax.ppermute(own, "tp", SWAP)
     mixed = pl.pallas_call(
         mix_kernel,
@@ -337,7 +393,7 @@
         name="arrange_out",
     )(*held(w_down))
 
-    own = exchanged(mixed, KV)
+    own = exchanged(mixed, KV_TP, teams(ORDERS))
     other = lax.ppermute(own, "tp", SWAP)
     chunks = (kv_count, half, LANES)
     products, squares = pl.pallas_call(
@@ -379,7 +435,7 @@
         compiler_params=LIMIT,
         name="chip_sum",
     )(*held(mine, theirs))
-    down = exchanged(chip_sum, KV)
+    down = exchanged(chip_sum, KV_TP, teams(LAST_ORDERS))
     result = pl.pallas_call(
         finish_kernel,
         out_shape=jax.ShapeDtypeStruct((rows, cols), bf16),

time: 79.5 us -> 73.8 us (0.928); the launches traced: 79.2 us -> 72.6 us
  blocking collectives: 67.5 us -> 60.8 us
  starting transfers between devices: 0.19 us -> 1.17 us
    all_to_all x4, blocking collectives: 67.5 us -> 60.8 us  [exchanged(): lax.all_to_all(pieces, axes, split_axis=0, concat_axis=0, axis_index_grou...]
  transfers between devices with their start and end apart: 4 -> 4, of which waited for: 3 -> 3; matrix products, arithmetic and copies ran while one was open for 0% -> 0% of each run, Pallas kernels for 4% -> 5%
where the time goes in v7:
time: 73.8 us; the launch traced here: 72.6 us
  blocking collectives  60.8 us (82%)
  Pallas kernels  6.98 us (9%)
  waiting for transfers between devices  2.05 us (3%)
  starting transfers between devices  1.17 us (2%)
  local copies, waits for them, and re-layouts  0.84 us (1%)
  between operations  0.78 us (1%)
    all_to_all x4, blocking collectives, exchanged(): lax.all_to_all(pieces, axes, split_axis=0, concat_axis=0, axis_index_grou...  60.8 us
  transfers between devices with their start and end apart: 4, of which 3 were waited for; matrix products, arithmetic and copies ran while one was open for 0% of the time, Pallas kernels for 5%

profile of v7, /device:TPU:6, one launch (start us, length us, event | category | flops | bytes accessed | tf_op | source)
XLA Modules:
  0.0 72.6 jit_solution(14251770281665640902)
XLA Ops:
  0.6 0.1 collective-permute-start
  0.8 1.2 %load.1 = (bf16[32,64]{1,0:T(8,128)(2,1)S(1)}, f32[32,128]{1,0:T(8,128)S(1)}, f32[8,128]{1,0:T(8,128)S(1)}, f32[8,128]{1,0:T(8,128)S(1)}, f32[32,128]{1,0:T(8,128)S(1)}, /*index=5*/bf16[64,2048]{1,0:T(8,128)(2,1)S(1)}) custom-call(bf16[32,64]{1,0:T(8,128)(2,1)} %refs_0_.1, f32[32,128]{1,0:T(8,128)} %bitcast.14, f32[8,128]{1,0:T(8,128)} %bitcast.16, ...), custom_call_target="tpu_custom_call" | custom-call | flops 4000000000 | bytes 20000000 | tf_op jit(solution)/shard_map/load/pallas_call | solution.py:328
  2.0 0.2 collective-permute-done.other
  2.1 0.4 project.1
  2.6 21.5 %all_to_all.20.refs_0_ = bf16[32,9,4,128]{3,2,1,0:T(4,128)(2,1)S(1)} all-to-all(bf16[32,9,4,128]{3,2,1,0:T(4,128)(2,1)S(1)} %project.1), channel_id=1, replica_groups={{44,46,48,50,52,54,56,58,60,62,0,2,4,6,8,10,12,14,16,18,20,22,24,26,28,..., dimensions={0} | all-to-all | bytes 589824 | tf_op jit(solution)/shard_map/all_to_all | solution.py:39
  24.0 0.8 %recur.1 = (bf16[32,8,128]{2,1,0:T(8,128)(2,1)S(1)}, f32[8,128,128]{2,1,0:T(8,128)S(1)}) custom-call(bf16[32,9,4,128]{3,2,1,0:T(4,128)(2,1)S(1)} %all_to_all.20.refs_0_, f32[8,128,128]{2,1,0:T(8,128)S(1)} %bitcast.11, f32[8,128]{1,0:T(8,128)S(1)} %get-tuple-element.19.refs_2_, f32[8,128]{1,0:T(8,128)S(1)} %get-tuple-element.20.refs_3_), custom_call_target="tpu_custom_call" | custom-call | tf_op jit(solution)/shard_map/recur/pallas_call | solution.py:351
  24.8 12.2 %all_to_all.21.own = bf16[32,8,128]{2,1,0:T(8,128)(2,1)S(1)} all-to-all(bf16[32,8,128]{2,1,0:T(8,128)(2,1)S(1)} %get-tuple-element.21), channel_id=1, replica_groups={{45,47,49,51,53,55,57,59,61,63,1,3,5,7,8,10,12,14,16,18,20,22,24,26,28,..., dimensions={0} | all-to-all | bytes 131072 | tf_op jit(solution)/shard_map/all_to_all | solution.py:39
  37.1 0.0 collective-permute-start.1
  37.1 1.2 %collective-permute-done.1.other = bf16[32,8,128]{2,1,0:T(8,128)(2,1)S(1)} collective-permute-done((bf16[32,8,128]{2,1,0:T(8,128)(2,1)S(1)}, bf16[32,8,128]{2,1,0:T(8,128)(2,1)S(1)}, u32[]{:S(2)}, u32[]{:S(2)}) %collective-permute-start.1) | collective-permute-done | bytes 65568 | tf_op jit(solution)/shard_map/ppermute | solution.py:361
  38.3 0.4 mix.1.mixed
  38.7 13.6 %all_to_all.22.chunk = bf16[32,16,128]{2,1,0:T(8,128)(2,1)S(1)} all-to-all(bf16[32,16,128]{2,1,0:T(8,128)(2,1)S(1)} %mix.1.mixed), channel_id=1, replica_groups={{45,47,49,51,53,55,57,59,61,63,1,3,5,7,8,10,12,14,16,18,20,22,24,26,28,..., dimensions={0} | all-to-all | bytes 262144 | tf_op jit(solution)/shard_map/all_to_all | solution.py:39
  52.3 0.5 collective-permute-start.2
  52.8 0.5 arrange_out.1.outs
  53.3 0.4 copy-done.1
  53.6 0.4 copy-done.2
  54.1 1.0 %arrange_in.1 = (bf16[2,352,2048]{2,1,0:T(8,128)(2,1)S(1)}, f32[2,16,128]{2,1,0:T(8,128)S(1)}) custom-call(bf16[176,4096]{1,0:T(8,128)(2,1)S(1)} %bitcast.9, bf16[176,4096]{1,0:T(8,128)(2,1)S(1)} %bitcast.10, f32[32,128]{1,0:T(8,128)S(1)} %get-tuple-element.23.gain), custom_call_target="tpu_custom_call" | custom-call | tf_op jit(solution)/shard_map/arrange_in/pallas_call | solution.py:376
  55.0 0.6 own.1
  55.6 0.0 collective-permute-done.2.chunk
  55.6 1.1 %other.1 = (bf16[32,16,128]{2,1,0:T(8,128)(2,1)S(1)}, bf16[32,176]{1,0:T(8,128)(2,1)S(1)}, f32[8,128,128]{2,1,0:T(8,128)}) custom-call(bf16[32,16,128]{2,1,0:T(8,128)(2,1)S(1)} %collective-permute-done.2.chunk, f32[2,16,128]{2,1,0:T(8,128)S(1)} %get-tuple-element.24.gains, bf16[2,352,2048]{2,1,0:T(8,128)(2,1)S(1)} %get-tuple-element.25.ins, ...), custom_call_target="tpu_custom_call" | custom-call | tf_op jit(solution)/shard_map/other/pallas_call | solution.py:408
  56.7 0.6 collective-permute-start.3
  57.3 0.3 mine.1
  57.6 0.7 collective-permute-done.3.theirs
  58.3 13.5 %all_to_all.23.pieces = bf16[32,16,128]{2,1,0:T(8,128)(2,1)S(1)} all-to-all(bf16[32,16,128]{2,1,0:T(8,128)(2,1)S(1)} %chip_sum.1), channel_id=1, replica_groups={{45,22,49,16,43,28,32,59,18,63,41,24,51,26,38,57,8,5,20,30,3,10,47,7,36..., dimensions={0} | all-to-all | bytes 262144 | tf_op jit(solution)/shard_map/all_to_all | solution.py:39
  71.8 0.8 %finish.1 = bf16[32,64]{1,0:T(8,128)(2,1)} custom-call(bf16[32,16,128]{2,1,0:T(8,128)(2,1)S(1)} %all_to_all.23.pieces, bf16[32,16,128]{2,1,0:T(8,128)(2,1)S(1)} %mix.1.mixed), custom_call_target="tpu_custom_call" | custom-call | tf_op jit(solution)/shard_map/finish/pallas_call | solution.py:439
  (15 shorter events, 0.1 us)
Async XLA Ops:
  0.6 1.5 %collective-permute-start = (bf16[32,64]{1,0:T(8,128)(2,1)}, bf16[32,64]{1,0:T(8,128)(2,1)S(1)}, u32[]{:S(2)}, u32[]{:S(2)}) collective-permute-start(bf16[32,64]{1,0:T(8,128)(2,1)} %refs_0_.1), channel_id=1, source_target_pairs={{0,1},{1,0},{2,3},{3,2},{4,5},{5,4},{6,7},{7,6},{8,9},{9,8},{10,11... | collective-permute-start | bytes 12296 | tf_op jit(solution)/shard_map/ppermute | solution.py:319
  0.7 1.4 %copy-start.4 = (bf16[128,1024]{1,0:T(8,128)(2,1)S(1)}, bf16[128,1024]{1,0:T(8,128)(2,1)}, u32[]{:S(2)}) copy-start(bf16[128,1024]{1,0:T(8,128)(2,1)} %wq.1) | copy-start | bytes 786436
  0.7 1.4 %copy-start.5 = (bf16[128,1024]{1,0:T(8,128)(2,1)S(1)}, bf16[128,1024]{1,0:T(8,128)(2,1)}, u32[]{:S(2)}) copy-start(bf16[128,1024]{1,0:T(8,128)(2,1)} %wf.1) | copy-start | bytes 786436
  0.8 1.4 %copy-start.6 = (bf16[128,1024]{1,0:T(8,128)(2,1)S(1)}, bf16[128,1024]{1,0:T(8,128)(2,1)}, u32[]{:S(2)}) copy-start(bf16[128,1024]{1,0:T(8,128)(2,1)} %wi.1) | copy-start | bytes 786436
  0.8 1.4 %copy-start.7 = (bf16[128,1024]{1,0:T(8,128)(2,1)S(1)}, bf16[128,1024]{1,0:T(8,128)(2,1)}, u32[]{:S(2)}) copy-start(bf16[128,1024]{1,0:T(8,128)(2,1)} %wg.1) | copy-start | bytes 786436
  1.9 22.1 %copy-start.3 = (f32[1,8,128,128]{3,2,1,0:T(8,128)S(1)}, f32[1,8,128,128]{3,2,1,0:T(8,128)}, u32[]{:S(2)}) copy-start(f32[1,8,128,128]{3,2,1,0:T(8,128)} %param.15) | copy-start | bytes 1572868
  2.6 50.2 %copy-start = (bf16[176,4096]{1,0:T(8,128)(2,1)S(1)}, bf16[176,4096]{1,0:T(8,128)(2,1)}, u32[]{:S(2)}) copy-start(bf16[176,4096]{1,0:T(8,128)(2,1)} %w_down.1) | copy-start | bytes 4325380
  37.1 1.3 %collective-permute-start.1 = (bf16[32,8,128]{2,1,0:T(8,128)(2,1)S(1)}, bf16[32,8,128]{2,1,0:T(8,128)(2,1)S(1)}, u32[]{:S(2)}, u32[]{:S(2)}) collective-permute-start(bf16[32,8,128]{2,1,0:T(8,128)(2,1)S(1)} %all_to_all.21.own), channel_id=1, source_target_pairs={{0,1},{1,0},{2,3},{3,2},{4,5},{5,4},{6,7},{7,6},{8,9},{9,8},{10,11... | collective-permute-start | bytes 196616 | tf_op jit(solution)/shard_map/ppermute | solution.py:361
  52.3 1.4 %copy-start.1 = (bf16[4096,176]{0,1:T(8,128)(2,1)S(1)}, bf16[4096,176]{0,1:T(8,128)(2,1)}, u32[]{:S(2)}) copy-start(bf16[4096,176]{0,1:T(8,128)(2,1)} %param.25) | copy-start | bytes 4325380
  52.3 1.8 %copy-start.2 = (bf16[4096,176]{0,1:T(8,128)(2,1)S(1)}, bf16[4096,176]{0,1:T(8,128)(2,1)}, u32[]{:S(2)}) copy-start(bf16[4096,176]{0,1:T(8,128)(2,1)} %param.26) | copy-start | bytes 4325380
  52.3 3.3 %collective-permute-start.2 = (bf16[32,16,128]{2,1,0:T(8,128)(2,1)S(1)}, bf16[32,16,128]{2,1,0:T(8,128)(2,1)S(1)}, u32[]{:S(2)}, u32[]{:S(2)}) collective-permute-start(bf16[32,16,128]{2,1,0:T(8,128)(2,1)S(1)} %all_to_all.22.chunk), channel_id=1, source_target_pairs={{0,1},{1,0},{2,3},{3,2},{4,5},{5,4},{6,7},{7,6},{8,9},{9,8},{10,11... | collective-permute-start | bytes 393224 | tf_op jit(solution)/shard_map/ppermute | solution.py:397
  56.7 1.5 %collective-permute-start.3 = (bf16[32,16,128]{2,1,0:T(8,128)(2,1)S(1)}, bf16[32,16,128]{2,1,0:T(8,128)(2,1)S(1)}, u32[]{:S(2)}, u32[]{:S(2)}) collective-permute-start(bf16[32,16,128]{2,1,0:T(8,128)(2,1)S(1)} %get-tuple-element.30), channel_id=1, source_target_pairs={{0,1},{1,0},{2,3},{3,2},{4,5},{5,4},{6,7},{7,6},{8,9},{9,8},{10,11... | collective-permute-start | bytes 393224 | tf_op jit(solution)/shard_map/ppermute | solution.py:429

commit v8 on v7

--- a/solution.py
+++ b/solution.py
@@ -24,8 +24,8 @@
     [18, 19, 20, 21, 22, 23, 24, 25, 26, 27, 28, 29, 30, 31, 0, 1, 2, 3, 4, 5, 6, 7, 8, 9, 10, 11, 12, 13, 14, 15, 16, 17],
 ]
 LAST_ORDERS = [
-    [22, 11, 24, 8, 21, 14, 16, 29, 9, 31, 20, 12, 25, 13, 19, 28, 4, 2, 10, 15, 1, 5, 23, 3, 18, 0, 30, 17, 7, 27, 6, 26],
-    [18, 20, 25, 14, 28, 30, 12, 27, 6, 31, 26, 8, 23, 5, 11, 21, 4, 16, 1, 9, 7, 0, 13, 15, 29, 19, 3, 10, 2, 22, 17, 24],
+    [22, 8, 2, 14, 7, 1, 5, 21, 20, 6, 0, 31, 9, 11, 28, 16, 29, 17, 15, 27, 13, 3, 26, 4, 30, 10, 23, 24, 12, 25, 18, 19],
+    [18, 29, 20, 16, 28, 12, 25, 21, 7, 2, 8, 15, 24, 9, 22, 31, 19, 1, 14, 6, 27, 17, 0, 10, 5, 26, 4, 13, 30, 23, 11, 3],
 ]
 FIRST_PLANE = 5
 TURNED = [(place // 4 - FIRST_PLANE) % 8 < 4 for place in range(COUNT)]
@@ -198,16 +198,6 @@
         gains[1, pair : pair + 1, :] = second
 
 
-def arrange_out_kernel(w_down, outs):
-    low = low_lanes((w_down.shape[0], LANES))
-    for pair in range(w_down.shape[1] // (2 * LANES)):
-        first, second = by_team(
-            pair, split_lanes(low, w_down[:, part(2 * pair)], w_down[:, part(2 * pair + 1)])
-        )
-        outs[0, :, part(pair)] = first
-        outs[1, :, part(pair)] = second
-
-
 def half_feed(team, chunk, gains, ins, scr):
     blocks, half, _ = chunk.shape
     low = low_lanes((half, LANES))
@@ -225,11 +215,24 @@
     return products, squares
 
 
-def own_kernel(chunk, gains, ins, products, squares, scr):
+def own_kernel(
+    chunk, gains, ins, w_down, state, products, squares, outs, state_hbm, scr, sem
+):
+    store = pltpu.make_async_copy(state, state_hbm, sem)
+    store.start()
+
     def body(team):
         products[...], squares[...] = half_feed(team, chunk, gains, ins, scr)
 
     for_my_team(body)
+    low = low_lanes((w_down.shape[0], LANES))
+    for pair in range(w_down.shape[1] // (2 * LANES)):
+        first, second = by_team(
+            pair, split_lanes(low, w_down[:, part(2 * pair)], w_down[:, part(2 * pair + 1)])
+        )
+        outs[0, :, part(pair)] = first
+        outs[1, :, part(pair)] = second
+    store.wait()
 
 
 def packed_rows(low, block, turned):
@@ -240,12 +243,7 @@
     return split_lanes(low, first, second)
 
 
-def other_kernel(
-    chunk, gains, ins, products, squares, outs, state, theirs, hidden_out, state_hbm, scr, sem
-):
-    store = pltpu.make_async_copy(state, state_hbm, sem)
-    store.start()
-
+def other_kernel(chunk, gains, ins, products, squares, outs, theirs, hidden_out, scr):
     def body(team):
         half = chunk.shape[1]
         more, more_squares = half_feed(1 - team, chunk, gains, ins, scr)
@@ -264,7 +262,6 @@
             theirs[LAST_ORDERS[1 - team].index(2 * pair + 1)] = right.astype(bf16)
 
     for_my_team(body)
-    store.wait()
 
 
 def mine_kernel(hidden, outs, mine):
@@ -384,40 +381,33 @@
         compiler_params=LIMIT,
         name="arrange_in",
     )(*held(w_gate.T, w_up.T, second_gain))
-    outs = pl.pallas_call(
-        arrange_out_kernel,
-        out_shape=shape((2, units, width // 2), bf16),
-        in_specs=in_vmem(1),
-        out_specs=in_vmem(1)[0],
-        compiler_params=LIMIT,
-        name="arrange_out",
-    )(*held(w_down))
 
     own = exchanged(mixed, KV_TP, teams(ORDERS))
     other = lax.ppermute(own, "tp", SWAP)
     chunks = (kv_count, half, LANES)
-    products, squares = pl.pallas_call(
+    products, squares, outs, new_state = pl.pallas_call(
         own_kernel,
-        out_shape=(shape((rows, 2 * units), f32), shape((rows, LANES), f32)),
-        in_specs=in_vmem(3),
+        out_shape=(
+            shape((rows, 2 * units), f32),
+            shape((rows, LANES), f32),
+            shape((2, units, width // 2), bf16),
+            pltpu.HBM(new_state.shape, f32),
+        ),
+        in_specs=in_vmem(5),
+        out_specs=tuple(in_vmem(3) + [IN_HBM]),
+        scratch_shapes=[pltpu.VMEM((rows, width // 2), bf16), pltpu.SemaphoreType.DMA],
+        compiler_params=LIMIT,
+        name="own",
+    )(*held(own, gains, ins, w_down, new_state))
+    theirs, hidden = pl.pallas_call(
+        other_kernel,
+        out_shape=(shape(chunks, bf16), shape((rows, units), bf16)),
+        in_specs=in_vmem(6),
         out_specs=tuple(in_vmem(2)),
         scratch_shapes=[pltpu.VMEM((rows, width // 2), bf16)],
         compiler_params=LIMIT,
-        name="own",
-    )(*held(own, gains, ins))
-    theirs, hidden, new_state = pl.pallas_call(
-        other_kernel,
-        out_shape=(
-            shape(chunks, bf16),
-            shape((rows, units), bf16),
-            pltpu.HBM(new_state.shape, f32),
-        ),
-        in_specs=in_vmem(7),
-        out_specs=tuple(in_vmem(2) + [IN_HBM]),
-        scratch_shapes=[pltpu.VMEM((rows, width // 2), bf16), pltpu.SemaphoreType.DMA],
-        compiler_params=LIMIT,
         name="other",
-    )(*held(other, gains, ins, products, squares, outs, new_state))
+    )(*held(other, gains, ins, products, squares, outs))
     mine = pl.pallas_call(
         mine_kernel,
         out_shape=shape(chunks, f32),

time: 73.8 us -> 73 us (0.989)
  no operation moved by 1% of the time
where the time goes in v8:
time: 73 us; the launch traced here: 72 us
  blocking collectives  60.7 us (83%)
  Pallas kernels  6.97 us (10%)
  waiting for transfers between devices  2.34 us (3%)
  between operations  0.78 us (1%)
  starting transfers between devices  0.73 us (1%)
    all_to_all x4, blocking collectives, exchanged(): lax.all_to_all(pieces, axes, split_axis=0, concat_axis=0, axis_index_grou...  60.7 us
  transfers between devices with their start and end apart: 4, of which 3 were waited for; matrix products, arithmetic and copies ran while one was open for 0% of the time, Pallas kernels for 5%

profile of v8, /device:TPU:6, one launch (start us, length us, event | category | flops | bytes accessed | tf_op | source)
XLA Modules:
  0.0 72.0 jit_solution(8376542916209160577)
XLA Ops:
  0.6 0.1 collective-permute-start
  0.8 1.2 %load.1 = (bf16[32,64]{1,0:T(8,128)(2,1)S(1)}, f32[32,128]{1,0:T(8,128)S(1)}, f32[8,128]{1,0:T(8,128)S(1)}, f32[8,128]{1,0:T(8,128)S(1)}, f32[32,128]{1,0:T(8,128)S(1)}, /*index=5*/bf16[64,2048]{1,0:T(8,128)(2,1)S(1)}) custom-call(bf16[32,64]{1,0:T(8,128)(2,1)} %refs_0_.1, f32[32,128]{1,0:T(8,128)} %bitcast.14, f32[8,128]{1,0:T(8,128)} %bitcast.16, ...), custom_call_target="tpu_custom_call" | custom-call | flops 4000000000 | bytes 20000000 | tf_op jit(solution)/shard_map/load/pallas_call | solution.py:325
  1.9 0.0 copy-start.3
  2.0 0.2 collective-permute-done.other
  2.1 0.0 copy-start.1
  2.1 0.4 project.1
  2.6 0.0 copy-start
  2.6 21.5 %all_to_all.20.refs_0_ = bf16[32,9,4,128]{3,2,1,0:T(4,128)(2,1)S(1)} all-to-all(bf16[32,9,4,128]{3,2,1,0:T(4,128)(2,1)S(1)} %project.1), channel_id=1, replica_groups={{44,46,48,50,52,54,56,58,60,62,0,2,4,6,8,10,12,14,16,18,20,22,24,26,28,..., dimensions={0} | all-to-all | bytes 589824 | tf_op jit(solution)/shard_map/all_to_all | solution.py:39
  24.0 0.8 %recur.1 = (bf16[32,8,128]{2,1,0:T(8,128)(2,1)S(1)}, f32[8,128,128]{2,1,0:T(8,128)S(1)}) custom-call(bf16[32,9,4,128]{3,2,1,0:T(4,128)(2,1)S(1)} %all_to_all.20.refs_0_, f32[8,128,128]{2,1,0:T(8,128)S(1)} %bitcast.11, f32[8,128]{1,0:T(8,128)S(1)} %get-tuple-element.20.refs_2_, f32[8,128]{1,0:T(8,128)S(1)} %get-tuple-element.21.refs_3_), custom_call_target="tpu_custom_call" | custom-call | tf_op jit(solution)/shard_map/recur/pallas_call | solution.py:348
  24.8 12.2 %all_to_all.21.own = bf16[32,8,128]{2,1,0:T(8,128)(2,1)S(1)} all-to-all(bf16[32,8,128]{2,1,0:T(8,128)(2,1)S(1)} %get-tuple-element.22), channel_id=1, replica_groups={{45,47,49,51,53,55,57,59,61,63,1,3,5,7,8,10,12,14,16,18,20,22,24,26,28,..., dimensions={0} | all-to-all | bytes 131072 | tf_op jit(solution)/shard_map/all_to_all | solution.py:39
  37.1 0.0 collective-permute-start.1
  37.1 1.2 %collective-permute-done.1.other = bf16[32,8,128]{2,1,0:T(8,128)(2,1)S(1)} collective-permute-done((bf16[32,8,128]{2,1,0:T(8,128)(2,1)S(1)}, bf16[32,8,128]{2,1,0:T(8,128)(2,1)S(1)}, u32[]{:S(2)}, u32[]{:S(2)}) %collective-permute-start.1) | collective-permute-done | bytes 65568 | tf_op jit(solution)/shard_map/ppermute | solution.py:358
  38.3 0.4 mix.1.mixed
  38.7 13.6 %all_to_all.22.chunk = bf16[32,16,128]{2,1,0:T(8,128)(2,1)S(1)} all-to-all(bf16[32,16,128]{2,1,0:T(8,128)(2,1)S(1)} %mix.1.mixed), channel_id=1, replica_groups={{45,47,49,51,53,55,57,59,61,63,1,3,5,7,8,10,12,14,16,18,20,22,24,26,28,..., dimensions={0} | all-to-all | bytes 262144 | tf_op jit(solution)/shard_map/all_to_all | solution.py:39
  52.3 0.5 collective-permute-start.2
  52.8 0.9 %arrange_in.1 = (bf16[2,352,2048]{2,1,0:T(8,128)(2,1)S(1)}, f32[2,16,128]{2,1,0:T(8,128)S(1)}) custom-call(bf16[176,4096]{1,0:T(8,128)(2,1)S(1)} %bitcast.9, bf16[176,4096]{1,0:T(8,128)(2,1)S(1)} %bitcast.10, f32[32,128]{1,0:T(8,128)S(1)} %get-tuple-element.24.gain), custom_call_target="tpu_custom_call" | custom-call | tf_op jit(solution)/shard_map/arrange_in/pallas_call | solution.py:373
  53.7 0.4 copy-done.2
  54.1 1.1 %own.1 = (f32[32,352]{1,0:T(8,128)S(1)}, f32[32,128]{1,0:T(8,128)S(1)}, bf16[2,176,2048]{2,1,0:T(8,128)(2,1)S(1)}, f32[8,128,128]{2,1,0:T(8,128)}) custom-call(bf16[32,16,128]{2,1,0:T(8,128)(2,1)S(1)} %all_to_all.22.chunk, f32[2,16,128]{2,1,0:T(8,128)S(1)} %get-tuple-element.25.gains, bf16[2,352,2048]{2,1,0:T(8,128)(2,1)S(1)} %get-tuple-element.26.ins, ...), custom_call_target="tpu_custom_call" | custom-call | tf_op jit(solution)/shard_map/own/pallas_call | solution.py:388
  55.2 1.1 %other.1 = (bf16[32,16,128]{2,1,0:T(8,128)(2,1)S(1)}, bf16[32,176]{1,0:T(8,128)(2,1)S(1)}) custom-call(bf16[32,16,128]{2,1,0:T(8,128)(2,1)S(1)} %collective-permute-done.2.chunk, f32[2,16,128]{2,1,0:T(8,128)S(1)} %get-tuple-element.25.gains, bf16[2,352,2048]{2,1,0:T(8,128)(2,1)S(1)} %get-tuple-element.26.ins, f32[32,352]{1,0:T(8,128)S(1)} %get-tuple-element.28.products, ...), custom_call_target="tpu_custom_call" | custom-call | tf_op jit(solution)/shard_map/other/pallas_call | solution.py:402
  56.3 0.1 collective-permute-start.3
  56.4 0.3 mine.1
  56.8 1.0 %collective-permute-done.3.theirs = bf16[32,16,128]{2,1,0:T(8,128)(2,1)S(1)} collective-permute-done((bf16[32,16,128]{2,1,0:T(8,128)(2,1)S(1)}, bf16[32,16,128]{2,1,0:T(8,128)(2,1)S(1)}, u32[]{:S(2)}, u32[]{:S(2)}) %collective-permute-start.3) | collective-permute-done | bytes 131104 | tf_op jit(solution)/shard_map/ppermute | solution.py:419
  57.8 13.4 %all_to_all.23.pieces = bf16[32,16,128]{2,1,0:T(8,128)(2,1)S(1)} all-to-all(bf16[32,16,128]{2,1,0:T(8,128)(2,1)S(1)} %chip_sum.1), channel_id=1, replica_groups={{45,16,5,28,14,3,10,43,41,12,1,63,18,22,57,32,59,34,30,55,26,7,53,8,61,..., dimensions={0} | all-to-all | bytes 262144 | tf_op jit(solution)/shard_map/all_to_all | solution.py:39
  71.2 0.8 %finish.1 = bf16[32,64]{1,0:T(8,128)(2,1)} custom-call(bf16[32,16,128]{2,1,0:T(8,128)(2,1)S(1)} %all_to_all.23.pieces, bf16[32,16,128]{2,1,0:T(8,128)(2,1)S(1)} %mix.1.mixed), custom_call_target="tpu_custom_call" | custom-call | tf_op jit(solution)/shard_map/finish/pallas_call | solution.py:429
  (14 shorter events, 0.1 us)
Async XLA Ops:
  0.6 1.5 %collective-permute-start = (bf16[32,64]{1,0:T(8,128)(2,1)}, bf16[32,64]{1,0:T(8,128)(2,1)S(1)}, u32[]{:S(2)}, u32[]{:S(2)}) collective-permute-start(bf16[32,64]{1,0:T(8,128)(2,1)} %refs_0_.1), channel_id=1, source_target_pairs={{0,1},{1,0},{2,3},{3,2},{4,5},{5,4},{6,7},{7,6},{8,9},{9,8},{10,11... | collective-permute-start | bytes 12296 | tf_op jit(solution)/shard_map/ppermute | solution.py:316
  0.7 1.4 %copy-start.4 = (bf16[128,1024]{1,0:T(8,128)(2,1)S(1)}, bf16[128,1024]{1,0:T(8,128)(2,1)}, u32[]{:S(2)}) copy-start(bf16[128,1024]{1,0:T(8,128)(2,1)} %wq.1) | copy-start | bytes 786436
  0.7 1.4 %copy-start.5 = (bf16[128,1024]{1,0:T(8,128)(2,1)S(1)}, bf16[128,1024]{1,0:T(8,128)(2,1)}, u32[]{:S(2)}) copy-start(bf16[128,1024]{1,0:T(8,128)(2,1)} %wf.1) | copy-start | bytes 786436
  0.8 1.4 %copy-start.6 = (bf16[128,1024]{1,0:T(8,128)(2,1)S(1)}, bf16[128,1024]{1,0:T(8,128)(2,1)}, u32[]{:S(2)}) copy-start(bf16[128,1024]{1,0:T(8,128)(2,1)} %wi.1) | copy-start | bytes 786436
  0.8 1.4 %copy-start.7 = (bf16[128,1024]{1,0:T(8,128)(2,1)S(1)}, bf16[128,1024]{1,0:T(8,128)(2,1)}, u32[]{:S(2)}) copy-start(bf16[128,1024]{1,0:T(8,128)(2,1)} %wg.1) | copy-start | bytes 786436
  1.9 22.1 %copy-start.3 = (f32[1,8,128,128]{3,2,1,0:T(8,128)S(1)}, f32[1,8,128,128]{3,2,1,0:T(8,128)}, u32[]{:S(2)}) copy-start(f32[1,8,128,128]{3,2,1,0:T(8,128)} %param.15) | copy-start | bytes 1572868
  2.1 50.6 %copy-start.1 = (bf16[4096,176]{0,1:T(8,128)(2,1)S(1)}, bf16[4096,176]{0,1:T(8,128)(2,1)}, u32[]{:S(2)}) copy-start(bf16[4096,176]{0,1:T(8,128)(2,1)} %param.26) | copy-start | bytes 4325380
  2.6 50.2 %copy-start = (bf16[4096,176]{0,1:T(8,128)(2,1)S(1)}, bf16[4096,176]{0,1:T(8,128)(2,1)}, u32[]{:S(2)}) copy-start(bf16[4096,176]{0,1:T(8,128)(2,1)} %param.25) | copy-start | bytes 4325380
  37.1 1.3 %collective-permute-start.1 = (bf16[32,8,128]{2,1,0:T(8,128)(2,1)S(1)}, bf16[32,8,128]{2,1,0:T(8,128)(2,1)S(1)}, u32[]{:S(2)}, u32[]{:S(2)}) collective-permute-start(bf16[32,8,128]{2,1,0:T(8,128)(2,1)S(1)} %all_to_all.21.own), channel_id=1, source_target_pairs={{0,1},{1,0},{2,3},{3,2},{4,5},{5,4},{6,7},{7,6},{8,9},{9,8},{10,11... | collective-permute-start | bytes 196616 | tf_op jit(solution)/shard_map/ppermute | solution.py:358
  52.3 2.9 %collective-permute-start.2 = (bf16[32,16,128]{2,1,0:T(8,128)(2,1)S(1)}, bf16[32,16,128]{2,1,0:T(8,128)(2,1)S(1)}, u32[]{:S(2)}, u32[]{:S(2)}) collective-permute-start(bf16[32,16,128]{2,1,0:T(8,128)(2,1)S(1)} %all_to_all.22.chunk), channel_id=1, source_target_pairs={{0,1},{1,0},{2,3},{3,2},{4,5},{5,4},{6,7},{7,6},{8,9},{9,8},{10,11... | collective-permute-start | bytes 393224 | tf_op jit(solution)/shard_map/ppermute | solution.py:386
  52.8 1.4 %copy-start.2 = (bf16[176,4096]{1,0:T(8,128)(2,1)S(1)}, bf16[176,4096]{1,0:T(8,128)(2,1)}, u32[]{:S(2)}) copy-start(bf16[176,4096]{1,0:T(8,128)(2,1)} %w_down.1) | copy-start | bytes 4325380
  56.3 1.4 %collective-permute-start.3 = (bf16[32,16,128]{2,1,0:T(8,128)(2,1)S(1)}, bf16[32,16,128]{2,1,0:T(8,128)(2,1)S(1)}, u32[]{:S(2)}, u32[]{:S(2)}) collective-permute-start(bf16[32,16,128]{2,1,0:T(8,128)(2,1)S(1)} %get-tuple-element.32), channel_id=1, source_target_pairs={{0,1},{1,0},{2,3},{3,2},{4,5},{5,4},{6,7},{7,6},{8,9},{9,8},{10,11... | collective-permute-start | bytes 393224 | tf_op jit(solution)/shard_map/ppermute | solution.py:419

commit v9 on v8

--- a/solution.py
+++ b/solution.py
@@ -114,7 +114,7 @@
         out[OWNERS.index(row)] = piece.astype(bf16)
 
 
-def recur_kernel(pieces, state, bound, gain, gated, new_state, width):
+def recur_kernel(pieces, state, bound, gain, gated, forget_out, value_out, width):
     heads = state.shape[0]
     total = jnp.sum(pieces[...].astype(f32), axis=0)
     total = total.reshape(total.shape[0] * total.shape[1], LANES)
@@ -124,15 +124,16 @@
         row_scale * total[i * heads : (i + 1) * heads] for i in range(4)
     ]
     forget = bound[...] + (1.0 - bound[...]) * jax.nn.sigmoid(forget_pre)
-    forget_down = jnp.transpose(forget)
-    query_down = jnp.transpose(jax.nn.silu(query_pre))
-    reads = []
-    for head in range(heads):
-        keep = jnp.broadcast_to(forget_down[:, head : head + 1], state.shape[1:])
-        fresh = keep * state[head] + (1.0 - keep) * value_in[head : head + 1]
-        new_state[head] = fresh
-        reads.append(jnp.sum(query_down[:, head : head + 1] * fresh, axis=0, keepdims=True))
-    head_out = jnp.concatenate(reads, axis=0)
+    query_act = jax.nn.silu(query_pre)
+    forget_out[...] = forget
+    value_out[...] = value_in
+    fresh = jnp.sum(query_act * (1.0 - forget), axis=1, keepdims=True) * value_in
+    down = jnp.transpose(query_act * forget)
+    reads = [
+        jnp.sum(down[:, head : head + 1] * state[head], axis=0, keepdims=True)
+        for head in range(heads)
+    ]
+    head_out = jnp.concatenate(reads, axis=0) + fresh
     head_out = head_out * lax.rsqrt(
         jnp.mean(head_out * head_out, axis=1, keepdims=True) + epsilon
     )
@@ -179,7 +180,7 @@
     return halves[::-1] if TURNED[2 * pair] else halves
 
 
-def arrange_in_kernel(w_gate, w_up, gain, ins, gains):
+def arrange_in_kernel(w_gate, w_up, gain, forget, value, state, ins, gains, new_state):
     units = w_gate.shape[0]
     low = low_lanes((units, LANES))
     for pair in range(w_gate.shape[1] // (2 * LANES)):
@@ -196,6 +197,10 @@
         )
         gains[0, pair : pair + 1, :] = first
         gains[1, pair : pair + 1, :] = second
+    down = jnp.transpose(forget[...])
+    for head in range(state.shape[0]):
+        keep = jnp.broadcast_to(down[:, head : head + 1], state.shape[1:])
+        new_state[head] = keep * state[head] + (1.0 - keep) * value[head : head + 1, :]
 
 
 def half_feed(team, chunk, gains, ins, scr):
@@ -320,9 +325,8 @@
         lower_bound.reshape(heads, LANES),
         head_gain.reshape(heads, LANES),
         mixer_gain.reshape(blocks, LANES),
-        w_heads_out.T,
-    )
-    tokens_here, first_gain, bound, gain, second_gain, heads_out = pl.pallas_call(
+    )
+    tokens_here, first_gain, bound, gain, second_gain = pl.pallas_call(
         load_kernel,
         out_shape=tuple(shape(x.shape, x.dtype) for x in loads),
         in_specs=[IN_HBM] * len(loads),
@@ -345,11 +349,12 @@
     )
     pieces = exchanged(pieces, KV, [OWNERS])
 
-    gated, new_state = pl.pallas_call(
+    per_head = shape((heads, LANES), f32)
+    gated, forget, value_in = pl.pallas_call(
         lambda *refs: recur_kernel(*refs, width),
-        out_shape=(shape((kv_count, heads, LANES), bf16), shape(rec_state.shape[1:], f32)),
+        out_shape=(shape((kv_count, heads, LANES), bf16), per_head, per_head),
         in_specs=in_vmem(4),
-        out_specs=tuple(in_vmem(2)),
+        out_specs=tuple(in_vmem(3)),
         compiler_params=LIMIT,
         name="recur",
     )(*held(pieces, rec_state[0], bound, gain))
@@ -367,20 +372,21 @@
         ],
         compiler_params=LIMIT,
         name="mix",
-    )(*held(own, other, tokens_here, heads_out))
+    )(*held(own, other, tokens_here, w_heads_out.T))
 
     units = w_gate.shape[1]
-    ins, gains = pl.pallas_call(
+    ins, gains, new_state = pl.pallas_call(
         arrange_in_kernel,
         out_shape=(
             shape((2, 2 * units, width // 2), bf16),
             shape((2, blocks // 2, LANES), f32),
+            shape(rec_state.shape[1:], f32),
         ),
-        in_specs=in_vmem(3),
-        out_specs=tuple(in_vmem(2)),
+        in_specs=in_vmem(6),
+        out_specs=tuple(in_vmem(3)),
         compiler_params=LIMIT,
         name="arrange_in",
-    )(*held(w_gate.T, w_up.T, second_gain))
+    )(*held(w_gate.T, w_up.T, second_gain, forget, value_in, rec_state[0]))
 
     own = exchanged(mixed, KV_TP, teams(ORDERS))
     other = lax.ppermute(own, "tp", SWAP)

time: 73 us -> 72.8 us (level)
  no operation moved by 1% of the time
where the time goes in v9:
time: 72.8 us; the launch traced here: 71.7 us
  blocking collectives  60.6 us (83%)
  Pallas kernels  6.65 us (9%)
  waiting for transfers between devices  2.59 us (4%)
  between operations  0.78 us (1%)
  starting transfers between devices  0.73 us (1%)
    all_to_all x4, blocking collectives, exchanged(): lax.all_to_all(pieces, axes, split_axis=0, concat_axis=0, axis_index_grou...  60.6 us
  transfers between devices with their start and end apart: 4, of which 3 were waited for; matrix products, arithmetic and copies ran while one was open for 0% of the time, Pallas kernels for 5%

profile of v9, /device:TPU:6, one launch (start us, length us, event | category | flops | bytes accessed | tf_op | source)
XLA Modules:
  0.0 71.7 jit_solution(10463539088663074635)
XLA Ops:
  0.6 0.1 collective-permute-start
  0.8 0.9 %load.1 = (bf16[32,64]{1,0:T(8,128)(2,1)S(1)}, f32[32,128]{1,0:T(8,128)S(1)}, f32[8,128]{1,0:T(8,128)S(1)}, f32[8,128]{1,0:T(8,128)S(1)}, f32[32,128]{1,0:T(8,128)S(1)}) custom-call(bf16[32,64]{1,0:T(8,128)(2,1)} %refs_0_.1, f32[32,128]{1,0:T(8,128)} %bitcast.15, f32[8,128]{1,0:T(8,128)} %bitcast.17, f32[8,128]{1,0:T(8,128)} %bitcast.18, f32[32,128]{1,0:T(8,128)} %bitcast.16), custom_call_target="tpu_custom_call" | custom-call | flops 4000000000 | bytes 20000000 | tf_op jit(solution)/shard_map/load/pallas_call | solution.py:329
  1.7 0.0 copy-start
  1.7 0.4 collective-permute-done.other
  2.1 0.0 copy-start.4
  2.1 0.4 project.1
  2.6 0.0 copy-start.1
  2.6 21.3 %all_to_all.20.refs_0_ = bf16[32,9,4,128]{3,2,1,0:T(4,128)(2,1)S(1)} all-to-all(bf16[32,9,4,128]{3,2,1,0:T(4,128)(2,1)S(1)} %project.1), channel_id=1, replica_groups={{44,46,48,50,52,54,56,58,60,62,0,2,4,6,8,10,12,14,16,18,20,22,24,26,28,..., dimensions={0} | all-to-all | bytes 589824 | tf_op jit(solution)/shard_map/all_to_all | solution.py:39
  23.9 0.6 recur.1
  24.5 12.3 %all_to_all.21.own = bf16[32,8,128]{2,1,0:T(8,128)(2,1)S(1)} all-to-all(bf16[32,8,128]{2,1,0:T(8,128)(2,1)S(1)} %get-tuple-element.23), channel_id=1, replica_groups={{45,47,49,51,53,55,57,59,61,63,1,3,5,7,8,10,12,14,16,18,20,22,24,26,28,..., dimensions={0} | all-to-all | bytes 131072 | tf_op jit(solution)/shard_map/all_to_all | solution.py:39
  36.8 0.0 collective-permute-start.1
  36.8 1.2 %collective-permute-done.1.other = bf16[32,8,128]{2,1,0:T(8,128)(2,1)S(1)} collective-permute-done((bf16[32,8,128]{2,1,0:T(8,128)(2,1)S(1)}, bf16[32,8,128]{2,1,0:T(8,128)(2,1)S(1)}, u32[]{:S(2)}, u32[]{:S(2)}) %collective-permute-start.1) | collective-permute-done | bytes 65568 | tf_op jit(solution)/shard_map/ppermute | solution.py:363
  38.0 0.4 mix.1.mixed
  38.4 13.6 %all_to_all.22.chunk = bf16[32,16,128]{2,1,0:T(8,128)(2,1)S(1)} all-to-all(bf16[32,16,128]{2,1,0:T(8,128)(2,1)S(1)} %mix.1.mixed), channel_id=1, replica_groups={{45,47,49,51,53,55,57,59,61,63,1,3,5,7,8,10,12,14,16,18,20,22,24,26,28,..., dimensions={0} | all-to-all | bytes 262144 | tf_op jit(solution)/shard_map/all_to_all | solution.py:39
  52.0 0.5 collective-permute-start.2
  52.5 1.1 %arrange_in.1 = (bf16[2,352,2048]{2,1,0:T(8,128)(2,1)S(1)}, f32[2,16,128]{2,1,0:T(8,128)S(1)}, f32[8,128,128]{2,1,0:T(8,128)S(1)}) custom-call(bf16[176,4096]{1,0:T(8,128)(2,1)S(1)} %bitcast.11, bf16[176,4096]{1,0:T(8,128)(2,1)S(1)} %bitcast.12, f32[32,128]{1,0:T(8,128)S(1)} %get-tuple-element.24.gain, f32[8,128]{1,0:T(8,128)S(1)} %get-tuple-element.25.forget, ...), custom_call_target="tpu_custom_call" | custom-call | tf_op jit(solution)/shard_map/arrange_in/pallas_call | solution.py:378
  53.5 0.3 copy-done.3
  53.8 1.1 %own.1 = (f32[32,352]{1,0:T(8,128)S(1)}, f32[32,128]{1,0:T(8,128)S(1)}, bf16[2,176,2048]{2,1,0:T(8,128)(2,1)S(1)}, f32[8,128,128]{2,1,0:T(8,128)}) custom-call(bf16[32,16,128]{2,1,0:T(8,128)(2,1)S(1)} %all_to_all.22.chunk, f32[2,16,128]{2,1,0:T(8,128)S(1)} %get-tuple-element.27.gains, bf16[2,352,2048]{2,1,0:T(8,128)(2,1)S(1)} %get-tuple-element.28.ins, ...), custom_call_target="tpu_custom_call" | custom-call | tf_op jit(solution)/shard_map/own/pallas_call | solution.py:394
  54.9 1.1 %other.1 = (bf16[32,16,128]{2,1,0:T(8,128)(2,1)S(1)}, bf16[32,176]{1,0:T(8,128)(2,1)S(1)}) custom-call(bf16[32,16,128]{2,1,0:T(8,128)(2,1)S(1)} %collective-permute-done.2.chunk, f32[2,16,128]{2,1,0:T(8,128)S(1)} %get-tuple-element.27.gains, bf16[2,352,2048]{2,1,0:T(8,128)(2,1)S(1)} %get-tuple-element.28.ins, f32[32,352]{1,0:T(8,128)S(1)} %get-tuple-element.30.products, ...), custom_call_target="tpu_custom_call" | custom-call | tf_op jit(solution)/shard_map/other/pallas_call | solution.py:408
  56.0 0.1 collective-permute-start.3
  56.1 0.3 mine.1
  56.5 1.0 %collective-permute-done.3.theirs = bf16[32,16,128]{2,1,0:T(8,128)(2,1)S(1)} collective-permute-done((bf16[32,16,128]{2,1,0:T(8,128)(2,1)S(1)}, bf16[32,16,128]{2,1,0:T(8,128)(2,1)S(1)}, u32[]{:S(2)}, u32[]{:S(2)}) %collective-permute-start.3) | collective-permute-done | bytes 131104 | tf_op jit(solution)/shard_map/ppermute | solution.py:425
  57.5 13.4 %all_to_all.23.pieces = bf16[32,16,128]{2,1,0:T(8,128)(2,1)S(1)} all-to-all(bf16[32,16,128]{2,1,0:T(8,128)(2,1)S(1)} %chip_sum.1), channel_id=1, replica_groups={{45,16,5,28,14,3,10,43,41,12,1,63,18,22,57,32,59,34,30,55,26,7,53,8,61,..., dimensions={0} | all-to-all | bytes 262144 | tf_op jit(solution)/shard_map/all_to_all | solution.py:39
  70.9 0.8 %finish.1 = bf16[32,64]{1,0:T(8,128)(2,1)} custom-call(bf16[32,16,128]{2,1,0:T(8,128)(2,1)S(1)} %all_to_all.23.pieces, bf16[32,16,128]{2,1,0:T(8,128)(2,1)S(1)} %mix.1.mixed), custom_call_target="tpu_custom_call" | custom-call | tf_op jit(solution)/shard_map/finish/pallas_call | solution.py:435
  (16 shorter events, 0.1 us)
Async XLA Ops:
  0.6 1.5 %collective-permute-start = (bf16[32,64]{1,0:T(8,128)(2,1)}, bf16[32,64]{1,0:T(8,128)(2,1)S(1)}, u32[]{:S(2)}, u32[]{:S(2)}) collective-permute-start(bf16[32,64]{1,0:T(8,128)(2,1)} %refs_0_.1), channel_id=1, source_target_pairs={{0,1},{1,0},{2,3},{3,2},{4,5},{5,4},{6,7},{7,6},{8,9},{9,8},{10,11... | collective-permute-start | bytes 12296 | tf_op jit(solution)/shard_map/ppermute | solution.py:321
  0.7 1.4 %copy-start.5 = (bf16[128,1024]{1,0:T(8,128)(2,1)S(1)}, bf16[128,1024]{1,0:T(8,128)(2,1)}, u32[]{:S(2)}) copy-start(bf16[128,1024]{1,0:T(8,128)(2,1)} %wq.1) | copy-start | bytes 786436
  0.7 1.4 %copy-start.6 = (bf16[128,1024]{1,0:T(8,128)(2,1)S(1)}, bf16[128,1024]{1,0:T(8,128)(2,1)}, u32[]{:S(2)}) copy-start(bf16[128,1024]{1,0:T(8,128)(2,1)} %wf.1) | copy-start | bytes 786436
  0.8 1.4 %copy-start.7 = (bf16[128,1024]{1,0:T(8,128)(2,1)S(1)}, bf16[128,1024]{1,0:T(8,128)(2,1)}, u32[]{:S(2)}) copy-start(bf16[128,1024]{1,0:T(8,128)(2,1)} %wi.1) | copy-start | bytes 786436
  0.8 1.4 %copy-start.8 = (bf16[128,1024]{1,0:T(8,128)(2,1)S(1)}, bf16[128,1024]{1,0:T(8,128)(2,1)}, u32[]{:S(2)}) copy-start(bf16[128,1024]{1,0:T(8,128)(2,1)} %wg.1) | copy-start | bytes 786436
  1.7 22.2 %copy-start = (f32[1,8,128,128]{3,2,1,0:T(8,128)S(1)}, f32[1,8,128,128]{3,2,1,0:T(8,128)}, u32[]{:S(2)}) copy-start(f32[1,8,128,128]{3,2,1,0:T(8,128)} %param.15) | copy-start | bytes 1572868
  2.1 35.9 %copy-start.4 = (bf16[2048,64]{0,1:T(8,128)(2,1)S(1)}, bf16[2048,64]{0,1:T(8,128)(2,1)}, u32[]{:S(2)}) copy-start(bf16[2048,64]{0,1:T(8,128)(2,1)} %param.23) | copy-start | bytes 786436
  2.1 50.3 %copy-start.2 = (bf16[4096,176]{0,1:T(8,128)(2,1)S(1)}, bf16[4096,176]{0,1:T(8,128)(2,1)}, u32[]{:S(2)}) copy-start(bf16[4096,176]{0,1:T(8,128)(2,1)} %param.26) | copy-start | bytes 4325380
  2.6 49.9 %copy-start.1 = (bf16[4096,176]{0,1:T(8,128)(2,1)S(1)}, bf16[4096,176]{0,1:T(8,128)(2,1)}, u32[]{:S(2)}) copy-start(bf16[4096,176]{0,1:T(8,128)(2,1)} %param.25) | copy-start | bytes 4325380
  36.8 1.3 %collective-permute-start.1 = (bf16[32,8,128]{2,1,0:T(8,128)(2,1)S(1)}, bf16[32,8,128]{2,1,0:T(8,128)(2,1)S(1)}, u32[]{:S(2)}, u32[]{:S(2)}) collective-permute-start(bf16[32,8,128]{2,1,0:T(8,128)(2,1)S(1)} %all_to_all.21.own), channel_id=1, source_target_pairs={{0,1},{1,0},{2,3},{3,2},{4,5},{5,4},{6,7},{7,6},{8,9},{9,8},{10,11... | collective-permute-start | bytes 196616 | tf_op jit(solution)/shard_map/ppermute | solution.py:363
  52.0 2.9 %collective-permute-start.2 = (bf16[32,16,128]{2,1,0:T(8,128)(2,1)S(1)}, bf16[32,16,128]{2,1,0:T(8,128)(2,1)S(1)}, u32[]{:S(2)}, u32[]{:S(2)}) collective-permute-start(bf16[32,16,128]{2,1,0:T(8,128)(2,1)S(1)} %all_to_all.22.chunk), channel_id=1, source_target_pairs={{0,1},{1,0},{2,3},{3,2},{4,5},{5,4},{6,7},{7,6},{8,9},{9,8},{10,11... | collective-permute-start | bytes 393224 | tf_op jit(solution)/shard_map/ppermute | solution.py:392
  52.5 1.4 %copy-start.3 = (bf16[176,4096]{1,0:T(8,128)(2,1)S(1)}, bf16[176,4096]{1,0:T(8,128)(2,1)}, u32[]{:S(2)}) copy-start(bf16[176,4096]{1,0:T(8,128)(2,1)} %w_down.1) | copy-start | bytes 4325380
  56.0 1.4 %collective-permute-start.3 = (bf16[32,16,128]{2,1,0:T(8,128)(2,1)S(1)}, bf16[32,16,128]{2,1,0:T(8,128)(2,1)S(1)}, u32[]{:S(2)}, u32[]{:S(2)}) collective-permute-start(bf16[32,16,128]{2,1,0:T(8,128)(2,1)S(1)} %get-tuple-element.34), channel_id=1, source_target_pairs={{0,1},{1,0},{2,3},{3,2},{4,5},{5,4},{6,7},{7,6},{8,9},{9,8},{10,11... | collective-permute-start | bytes 393224 | tf_op jit(solution)/shard_map/ppermute | solution.py:425
